TPU v7x, 512 devices: a whole 4x4x16 slice. The times are simulated.
512 devices in a mesh: sp: 64 (over z, y), tp: 8 (over x, core).
Axes of the slice: x: 4, y: 4, z: 16, core: 2. Of those that a mesh axis runs over, the one named last changes fastest.
Arguments:
- skip_stream_entering: bfloat16 [8192, 2048], P(('sp', 'tp')), may hold values from -6 to 6
- content_signal_matrix: bfloat16 [8192, 4096], P('sp', 'tp'), may hold values from -6 to 6
- writer_signal_matrix: bfloat16 [8192, 1024], P('sp', 'tp'), may hold values from -6 to 6
- reader_signal_matrix: bfloat16 [8192, 1024], P('sp', 'tp'), may hold values from -6 to 6
- multiplier_signal: bfloat16 [8192, 4096], P('sp', 'tp'), may hold values from -6 to 6
- interval_before_softplus: float32 [64, 8192], P('tp', 'sp'), may hold values from -7.5 to 0.5
- extra_log_shrink: float32 [64, 8192], P('tp', 'sp'), may hold values from -2.8 to 0
- log_forget_speed: float32 [64], P('tp'), may hold values from -12 to 0
- content_filter_coefs: bfloat16 [4, 4096], P(None, 'tp'), may hold values from -3 to 3
- writer_filter_coefs: bfloat16 [4, 1024], P(None, 'tp'), may hold values from -3 to 3
- reader_filter_coefs: bfloat16 [4, 1024], P(None, 'tp'), may hold values from -3 to 3
- skip_path_factor: float32 [64], P('tp'), may hold values from 0.25 to 2
- cluster_scaling_vector: float32 [4096], P('tp'), may hold values from 0.1 to 1.9
- blend_result_matrix: bfloat16 [4096, 2048], P('tp'), may hold values from -0.09375 to 0.09375
- feature_blend_scaling: float32 [2048], replicated, may hold values from 0.1 to 1.9
- widening_matrix: bfloat16 [2048, 8192], P('sp', 'tp'), may hold values from -0.125 to 0.125
- narrowing_matrix: bfloat16 [8192, 2048], P('tp', 'sp'), may hold values from -0.0625 to 0.0625
Outputs:
- layer_out: bfloat16 [8192, 2048], P(('sp', 'tp'))
All inputs are finite; a program needn't handle non-finite values.
Results may differ from a plain program's by a relative error of at most 0.02.
Values may be sent and summed in bfloat16 or wider, within the bound.
No kernel may reach another device: no remote copies, remote signals or barrier semaphores. Data moves between devices by JAX's collectives and lax.ppermute only.
A program may use at most 64 MiB of HBM per device.

v0:
```python
import jax
import jax.numpy as jnp
from jax import lax
from jax.sharding import Mesh
from jax.sharding import PartitionSpec as P

HEAD_DIM = 64
STATE = 128
BLOCK = 128
SP = ("sp_0", "sp_1")
SP_TP = ("sp_0", "sp_1", "tp")


epsilon = 1e-05


def turned_gather(arrays, axis, dims):
    turned = [jnp.moveaxis(a, dim, 0) for a, dim in zip(arrays, dims)]
    widths = [t[0].size for t in turned]
    both = jnp.concatenate([t.reshape(-1, w) for t, w in zip(turned, widths)], axis=1)
    out = lax.all_gather(both, axis, axis=0, tiled=True)
    blocks = jnp.split(out, [sum(widths[:k]) for k in range(1, len(widths))], axis=1)
    return tuple(
        (
            jnp.moveaxis(b.reshape(-1, *t.shape[1:]), 0, dim)
            for b, t, dim in zip(blocks, turned, dims)
        )
    )


def shifted(value, axis, steps):
    count = lax.axis_size(axis)
    initial, last = (max(0, -steps), min(count, count - steps))
    return lax.ppermute(value, axis, [(source, source + steps) for source in range(initial, last)])


def nothing_yet(value, identity):
    return jax.tree.map(
        lambda part, zero: jnp.zeros_like(part) + jnp.asarray(zero, part.dtype), value, identity
    )


def entering_2(value, axes, combine, identity):
    before = start = nothing_yet(value, identity)
    running = value
    for axis in reversed(axes):
        peers, mine = (lax.axis_size(axis), lax.axis_index(axis))
        pieces = jax.tree.map(
            lambda part, kind: lax.all_gather(part.astype(kind), axis),
            running,
            (jnp.bfloat16, jnp.bfloat16),
        )
        inside, running = (start, start)
        for k in range(peers):
            passed = k < mine
            running = combine(
                running, jax.tree.map(lambda part, own: part[k].astype(own.dtype), pieces, value)
            )
            inside = jax.tree.map(lambda new, old: jnp.where(passed, new, old), running, inside)
        before = combine(inside, before)
    return before


def in_blocks(value, dim, peers):
    dims = value.shape
    blocks = value.reshape(*dims[:dim], peers, dims[dim] // peers, *dims[dim + 1 :])
    return jnp.moveaxis(blocks, dim, 0)


def sum_at_owner(value, axis, dim):
    blocks = in_blocks(value, dim, lax.axis_size(axis))
    arrived = lax.all_to_all(blocks, axis, split_axis=0, concat_axis=0, tiled=True)
    return arrived.astype(jnp.float32).sum(axis=0)


def copy_for_each(value, axis):
    copies = jnp.broadcast_to(value, (lax.axis_size(axis), *value.shape))
    return lax.all_to_all(copies, axis, split_axis=0, concat_axis=0, tiled=True)


def laid_out(blocks, dim):
    dims = list(blocks.shape[1:])
    dims[dim] *= blocks.shape[0]
    return jnp.moveaxis(blocks, 0, dim).reshape(dims)


def gathered_copies(value, axis, dim):
    blocks = copy_for_each(value, axis)
    return laid_out(blocks, dim)


def convolve(inputs, rim_rows, conv_taps):
    width = conv_taps.shape[0]
    length = inputs.shape[0]
    extended = jnp.concatenate([rim_rows, inputs], axis=0)
    summed = extended[0:length].astype(jnp.float32) * conv_taps[0].astype(jnp.float32)
    for offset in range(1, width):
        summed = summed + extended[offset : offset + length].astype(jnp.float32) * conv_taps[
            offset
        ].astype(jnp.float32)
    return jax.nn.silu(summed)


def advance(carried, pair):
    block_state, block_factor = pair
    return (carried * block_factor[..., None, None] + block_state, carried)


def combine_states(earlier, following):
    return (earlier[0] * following[0], earlier[1] * following[0][..., None, None] + following[1])


def blockwise(values, interval_lengths, log_forgetting, key_rows, query_rows):
    length, groups, per_group, width = values.shape
    blocks = length // BLOCK
    value_blocks = values.reshape(blocks, BLOCK, groups, per_group, width)
    step_blocks = jnp.transpose(
        interval_lengths.reshape(groups, per_group, blocks, BLOCK), (2, 3, 0, 1)
    )
    weighted = value_blocks * step_blocks[..., None]
    cumulative = jnp.cumsum(
        jnp.transpose(log_forgetting.reshape(groups, per_group, blocks, BLOCK), (2, 0, 1, 3)),
        axis=-1,
    )
    key_blocks = key_rows.reshape(blocks, BLOCK, groups, -1)
    query_blocks = query_rows.reshape(blocks, BLOCK, groups, -1)
    causal = jnp.tril(jnp.ones((BLOCK, BLOCK), dtype=bool))
    decay_mask = jnp.exp(
        jnp.where(causal, cumulative[..., :, None] - cumulative[..., None, :], -jnp.inf)
    )
    scores = jnp.einsum("clgn,csgn->cgls", query_blocks, key_blocks)
    within = jnp.einsum("cgls,cgrls,csgrp->clgrp", scores, decay_mask, weighted)
    to_end = jnp.exp(cumulative[..., -1:] - cumulative)
    states = jnp.einsum("clgn,cgrl,clgrp->cgrpn", key_blocks, to_end, weighted)
    block_totals = cumulative[..., -1]
    initial = jnp.zeros(states.shape[1:], jnp.float32)
    final, entering = lax.scan(advance, initial, (states, jnp.exp(block_totals)))
    carried = jnp.einsum("clgn,cgrpn,cgrl->clgrp", query_blocks, entering, jnp.exp(cumulative))
    from_start = (jnp.cumsum(block_totals, axis=0) - block_totals)[..., None] + cumulative
    return (within + carried, final, from_start, jnp.sum(block_totals, axis=0))


def normalize(rows, gain):
    widened = rows.astype(jnp.float32)
    scaled = widened * lax.rsqrt(jnp.mean(widened * widened, axis=-1, keepdims=True) + epsilon)
    return (scaled * gain).astype(jnp.bfloat16)


def per_device(
    skip_stream_entering,
    content_signal_matrix,
    writer_signal_matrix,
    reader_signal_matrix,
    multiplier_signal,
    interval_before_softplus,
    extra_log_shrink,
    log_forget_speed,
    content_filter_coefs,
    writer_filter_coefs,
    reader_filter_coefs,
    skip_path_factor,
    cluster_scaling_vector,
    blend_result_matrix,
    feature_blend_scaling,
    widening_matrix,
    narrowing_matrix,
):
    up_whole, down_whole = turned_gather((widening_matrix, narrowing_matrix), SP, (0, 1))
    rim_width = content_filter_coefs.shape[0] - 1
    length = content_signal_matrix.shape[0]
    rims = shifted(
        (
            content_signal_matrix[length - rim_width :],
            writer_signal_matrix[length - rim_width :],
            reader_signal_matrix[length - rim_width :],
        ),
        SP,
        1,
    )
    values = convolve(content_signal_matrix, rims[0], content_filter_coefs)
    key_rows = convolve(writer_signal_matrix, rims[1], writer_filter_coefs)
    query_rows = convolve(reader_signal_matrix, rims[2], reader_filter_coefs)
    local_heads = interval_before_softplus.shape[0]
    local_groups = writer_signal_matrix.shape[1] // STATE
    per_group = local_heads // local_groups
    interval_lengths = jax.nn.softplus(interval_before_softplus)
    log_forgetting = extra_log_shrink - jnp.exp(log_forget_speed)[:, None] * interval_lengths
    shaped = values.reshape(length, local_groups, per_group, HEAD_DIM)
    local_out, end_state, from_start, device_total = blockwise(
        shaped,
        interval_lengths.reshape(local_groups, per_group, length),
        log_forgetting.reshape(local_groups, per_group, length),
        key_rows,
        query_rows,
    )
    identity = (jnp.ones_like(device_total), jnp.zeros_like(end_state))
    incoming = entering_2((jnp.exp(device_total), end_state), SP, combine_states, identity)[1]
    query_blocks = query_rows.reshape(length // BLOCK, BLOCK, local_groups, STATE)
    arriving = jnp.einsum("clgn,grpn,cgrl->clgrp", query_blocks, incoming, jnp.exp(from_start))
    scan_out = (local_out + arriving).reshape(length, local_heads * HEAD_DIM)
    gated = (scan_out + jnp.repeat(skip_path_factor, HEAD_DIM) * values) * jax.nn.silu(
        multiplier_signal.astype(jnp.float32)
    )
    grouped = gated.reshape(length, local_groups, -1)
    grouped = grouped * lax.rsqrt(jnp.mean(grouped * grouped, axis=-1, keepdims=True) + epsilon)
    heads_out = (grouped.reshape(length, -1) * cluster_scaling_vector).astype(jnp.bfloat16)
    mixer_rows = sum_at_owner(
        jnp.dot(heads_out, blend_result_matrix, preferred_element_type=jnp.float32).astype(
            jnp.bfloat16
        ),
        "tp",
        0,
    ).astype(jnp.bfloat16)
    own_rows = (skip_stream_entering.astype(jnp.float32) + mixer_rows.astype(jnp.float32)).astype(
        jnp.bfloat16
    )
    normed_all = gathered_copies(normalize(own_rows, feature_blend_scaling), "tp", 0)
    lifted = jnp.dot(normed_all, up_whole, preferred_element_type=jnp.float32)
    lifted = jax.nn.relu(lifted)
    hidden = (lifted * lifted).astype(jnp.bfloat16)
    mlp_rows = sum_at_owner(
        jnp.dot(hidden, down_whole, preferred_element_type=jnp.float32).astype(jnp.bfloat16),
        "tp",
        0,
    ).astype(jnp.bfloat16)
    return (own_rows.astype(jnp.float32) + mlp_rows.astype(jnp.float32)).astype(jnp.bfloat16)


def solution(mesh):
    torus = Mesh(mesh.devices.reshape(16, 4, mesh.shape["tp"]), ("sp_0", "sp_1", "tp"))
    placed = (
        P(SP_TP, None),
        P(SP, "tp"),
        P(SP, "tp"),
        P(SP, "tp"),
        P(SP, "tp"),
        P("tp", SP),
        P("tp", SP),
        P("tp"),
        P(None, "tp"),
        P(None, "tp"),
        P(None, "tp"),
        P("tp"),
        P("tp"),
        P("tp", None),
        P(),
        P(SP, "tp"),
        P("tp", SP),
    )
    return jax.shard_map(
        per_device, mesh=torus, in_specs=placed, out_specs=P(SP_TP, None), check_vma=False
    )
```

profile of v0, /device:TPU:1, one launch (start us, length us, event | category | flops | bytes accessed | tf_op | source)
XLA Modules:
  0.0 304.0 jit_solution(4290324773650001404)
XLA Ops:
  6.5 0.0 copy-start
  6.5 0.0 all-gather.5.cloned.1.call-start
  6.5 0.9 slice.212
  7.4 0.2 copy.24
  7.6 4.0 %collective-permute-start.2 = (bf16[3,512]{0,1:T(8,128)(2,1)S(1)}, bf16[3,512]{0,1:T(8,128)(2,1)S(1)}, u32[]{:S(2)}, u32[]{:S(2)}) collective-permute-start(bf16[3,512]{0,1:T(8,128)(2,1)S(1)} %copy.24), channel_id=1, source_target_pairs={{0,8},{8,16},{16,24},{24,32},{32,40},{40,48},{48,56},{56,64},{64,7... | collective-permute-start | bytes 9224 | tf_op jit(solution)/shard_map/ppermute | solution.py:34
  11.6 0.7 slice.204
  12.3 3.2 %collective-permute-start.1 = (bf16[3,128]{1,0:T(4,128)(2,1)S(1)}, bf16[3,128]{1,0:T(4,128)(2,1)S(1)}, u32[]{:S(2)}, u32[]{:S(2)}) collective-permute-start(bf16[3,128]{1,0:T(4,128)(2,1)S(1)} %slice.204), channel_id=1, source_target_pairs={{0,8},{8,16},{16,24},{24,32},{32,40},{40,48},{48,56},{56,64},{64,7... | collective-permute-start | bytes 2312 | tf_op jit(solution)/shard_map/ppermute | solution.py:34
  15.5 0.7 exp.73
  16.2 0.8 fusion.190
  16.9 0.3 reduce_window_sum.17
  17.2 0.2 subtract_reduce_fusion
  17.4 0.1 slice_exponential_fusion
  17.5 0.9 slice_convert_fusion.3
  18.3 0.8 bitcast_convert_fusion.3
  19.2 0.1 copy.27
  19.3 8.0 %all-gather = bf16[4,1,8,1]{2,3,1,0:T(2,128)(2,1)S(1)} all-gather(bf16[1,1,8,1]{2,3,1,0:T(2,128)(2,1)S(1)} %copy.27), channel_id=2, replica_groups=mesh['sp_0'=16,'sp_1'=4,'tp'=8] {'sp_1'}, dimensions={0}, use_global_device_ids=true | all-gather | bytes 80 | tf_op jit(solution)/shard_map/all_gather | solution.py:49
  27.2 0.1 exponential_bitcast_fusion.2
  27.3 1.0 copy.25
  28.3 0.0 collective-permute-done.1
  28.3 1.0 divide_multiply_fusion.1
  29.3 0.0 collective-permute-done.2
  29.3 0.5 divide_multiply_fusion
  29.9 0.2 fusion.22
  30.0 11.4 %all-gather.1 = bf16[32,64,128]{2,1,0:T(8,128)(2,1)S(1)} all-gather(bf16[8,64,128]{2,1,0:T(8,128)(2,1)S(1)} %fusion.22), channel_id=3, replica_groups=mesh['sp_0'=16,'sp_1'=4,'tp'=8] {'sp_1'}, dimensions={0}, use_global_device_ids=true | all-gather | bytes 655360 | tf_op jit(solution)/shard_map/all_gather | solution.py:49
  41.4 0.9 fusion.104
  42.3 0.0 all-gather.5.cloned.1.call-update
  42.3 0.0 all-gather.7.cloned.1.call-start
  42.4 1.6 pad_maximum_fusion.1
  43.9 0.0 all-gather.7.cloned.1.call-update
  43.9 0.7 slice.196
  44.6 1.3 collective-permute-start
  45.9 27.0 %all_gather.22 = bf16[16,1,8]{2,1,0:T(2,128)(2,1)S(1)} all-gather(bf16[1,1,8]{2,1,0:T(2,128)(2,1)S(1)} %convert_bitcast_fusion), channel_id=1, replica_groups=mesh['sp_0'=16,'sp_1'=4,'tp'=8] {'sp_0'}, dimensions={0}, use_global_device_ids=true | all-gather | bytes 272 | tf_op jit(solution)/shard_map/all_gather | solution.py:49
  73.0 0.8 bitcast_convert_fusion.7
  73.8 1.0 copy.28
  74.9 0.7 broadcast_in_dim.20
  75.6 0.1 mul.651
  75.7 0.0 collective-permute-done
  75.7 1.0 divide_multiply_fusion.2
  76.6 0.2 fusion.19
  76.8 0.2 fusion.216
  77.0 34.8 %all-gather.5.cloned.1.call-done = bf16[16,1,8,64,128]{4,3,2,1,0:T(8,128)(2,1)} async-done(((bf16[1,1,8,64,128]{4,3,2,1,0:T(8,128)(2,1)}), bf16[16,1,8,64,128]{4,3,2,1,0:T(8,128)(2,1)}) %all-gather.5.cloned.1.call-update) | async-done | bytes 2097168 | tf_op jit(solution)/shard_map/all_gather | solution.py:49
  111.8 0.0 copy-start.3
  111.8 2.5 fusion.18
  114.3 0.0 copy-start.1
  114.3 0.0 copy-start.2
  114.4 0.4 fusion.21
  114.7 0.2 multiply_reduce_fusion
  114.9 0.0 copy-done
  114.9 0.0 copy-done.3
  114.9 0.6 convolution_convert_fusion
  115.5 23.3 %all_to_all.15 = bf16[8,16,2048]{2,1,0:T(8,128)(2,1)S(1)} all-to-all(bf16[8,16,2048]{2,1,0:T(8,128)(2,1)S(1)} %bitcast.221), channel_id=1, replica_groups=mesh['sp_0'=16,'sp_1'=4,'tp'=8] {'tp'}, dimensions={0} | all-to-all | bytes 1048576 | tf_op jit(solution)/shard_map/all_to_all | solution.py:72
  138.8 0.1 reduce_sum.47
  138.9 0.0 copy-done.1
  138.9 0.1 fusion.113
  139.0 0.0 copy-done.2
  139.0 0.1 fusion.115
  139.2 12.8 %all_to_all.16 = bf16[8,16,2048]{2,1,0:T(8,128)(2,1)S(1)} all-to-all(bf16[8,16,2048]{2,1,0:T(8,128)(2,1)S(1)} %broadcast_in_dim.21), channel_id=1, replica_groups=mesh['sp_0'=16,'sp_1'=4,'tp'=8] {'tp'}, dimensions={0} | all-to-all | bytes 1048576 | tf_op jit(solution)/shard_map/all_to_all | solution.py:78
  151.9 117.2 %all-gather.7.cloned.1.call-done = bf16[2048,2048]{1,0:T(8,128)(2,1)} async-done(((bf16[32,2048]{1,0:T(8,128)(2,1)}), bf16[2048,2048]{1,0:T(8,128)(2,1)}) %all-gather.7.cloned.1.call-update) | async-done | bytes 8388624 | tf_op jit(solution)/shard_map/all_gather | solution.py:21
  269.1 5.6 %fusion.4 = bf16[128,2048]{1,0:T(8,128)(2,1)S(1)} fusion(bf16[2048,2048]{1,0:T(8,128)(2,1)} %all-gather.7.cloned.1.call-done, bf16[128,2048]{1,0:T(8,128)(2,1)S(1)} %bitcast.222), kind=kOutput, calls=%fused_computation.4 | convolution fusion | flops 1074397184 | bytes 9437184 | tf_op jit(solution)/shard_map/dot_general | solution.py:222
  274.7 21.8 %all_to_all.17 = bf16[8,16,2048]{2,1,0:T(8,128)(2,1)S(1)} all-to-all(bf16[8,16,2048]{2,1,0:T(8,128)(2,1)S(1)} %bitcast.223), channel_id=1, replica_groups=mesh['sp_0'=16,'sp_1'=4,'tp'=8] {'tp'}, dimensions={0} | all-to-all | bytes 1048576 | tf_op jit(solution)/shard_map/all_to_all | solution.py:72
  296.5 0.1 reduce_sum.49
  296.5 0.7 fusion.116
  (10 shorter events, 0.1 us)
Async XLA Ops:
  6.5 108.4 %copy-start = (bf16[512,2048]{1,0:T(8,128)(2,1)S(1)}, bf16[512,2048]{1,0:T(8,128)(2,1)}, u32[]{:S(2)}) copy-start(bf16[512,2048]{1,0:T(8,128)(2,1)} %param.30) | copy-start | bytes 6291460
  6.5 105.3 %all-gather.5.cloned.1.call-start = ((), (), s32[]{:S(2)}) async-start(), calls=%async_computation.3 | async-start | bytes 2228224 | tf_op jit(solution)/shard_map/all_gather | solution.py:49
  7.6 21.8 %collective-permute-start.2 = (bf16[3,512]{0,1:T(8,128)(2,1)S(1)}, bf16[3,512]{0,1:T(8,128)(2,1)S(1)}, u32[]{:S(2)}, u32[]{:S(2)}) collective-permute-start(bf16[3,512]{0,1:T(8,128)(2,1)S(1)} %copy.24), channel_id=1, source_target_pairs={{0,8},{8,16},{16,24},{24,32},{32,40},{40,48},{48,56},{56,64},{64,7... | collective-permute-start | bytes 9224 | tf_op jit(solution)/shard_map/ppermute | solution.py:34
  12.3 16.0 %collective-permute-start.1 = (bf16[3,128]{1,0:T(4,128)(2,1)S(1)}, bf16[3,128]{1,0:T(4,128)(2,1)S(1)}, u32[]{:S(2)}, u32[]{:S(2)}) collective-permute-start(bf16[3,128]{1,0:T(4,128)(2,1)S(1)} %slice.204), channel_id=1, source_target_pairs={{0,8},{8,16},{16,24},{24,32},{32,40},{40,48},{48,56},{56,64},{64,7... | collective-permute-start | bytes 2312 | tf_op jit(solution)/shard_map/ppermute | solution.py:34
  42.3 226.8 %all-gather.7.cloned.1.call-start = ((), (), s32[]{:S(2)}) async-start(), calls=%async_computation.4 | async-start | bytes 8519680 | tf_op jit(solution)/shard_map/all_gather | solution.py:21
  44.6 31.1 %collective-permute-start = (bf16[3,128]{1,0:T(4,128)(2,1)S(1)}, bf16[3,128]{1,0:T(4,128)(2,1)S(1)}, u32[]{:S(2)}, u32[]{:S(2)}) collective-permute-start(bf16[3,128]{1,0:T(4,128)(2,1)S(1)} %slice.196), channel_id=1, source_target_pairs={{0,8},{8,16},{16,24},{24,32},{32,40},{40,48},{48,56},{56,64},{64,7... | collective-permute-start | bytes 2312 | tf_op jit(solution)/shard_map/ppermute | solution.py:34
  111.8 3.1 %copy-start.3 = (f32[512]{0:T(512)S(1)}, f32[512]{0:T(512)}, u32[]{:S(2)}) copy-start(f32[512]{0:T(512)} %param.29) | copy-start | bytes 6148
  114.3 24.5 %copy-start.1 = (bf16[16,2048]{1,0:T(8,128)(2,1)S(1)}, bf16[16,2048]{1,0:T(8,128)(2,1)}, u32[]{:S(2)}) copy-start(bf16[16,2048]{1,0:T(8,128)(2,1)} %param.17) | copy-start | bytes 196612
  114.3 24.7 %copy-start.2 = (f32[2048]{0:T(1024)S(1)}, f32[2048]{0:T(1024)}, u32[]{:S(2)}) copy-start(f32[2048]{0:T(1024)} %param.31) | copy-start | bytes 24580
Sparse Core Ops, SparseCore 0:
  42.4 69.3 all-gather.4
  114.8 154.2 all-gather.6
where the time goes:
time: 305 us; the launch traced here: 304 us
  waiting for transfers between devices  152 us (50%)
  blocking collectives  104 us (34%)
  between operations  13.7 us (4%)
  other arithmetic  10.1 us (3%)
  matrix products  9.51 us (3%)
  starting transfers between devices  8.53 us (3%)
  local copies, waits for them, and re-layouts  6.08 us (2%)
    all_gather x1, waiting for transfers between devices, turned_gather(): out = lax.all_gather(both, axis, axis=0, tiled=True)  117 us
    all_gather x3, blocking collectives, entering_2(): lax.all_gather(part.astype(kind), axis)  46.3 us
    all_to_all x2, blocking collectives, sum_at_owner(): lax.all_to_all(blocks, axis, split_axis=0, concat_axis=0, tiled=True)  45.1 us
    all_gather x1, waiting for transfers between devices, entering_2(): lax.all_gather(part.astype(kind), axis)  34.8 us
    all_to_all x1, blocking collectives, copy_for_each(): return lax.all_to_all(copies, axis, split_axis=0, concat_axis=0, tiled=True)  12.8 us
    ppermute x3, starting transfers between devices, shifted(): lax.ppermute(value, axis, [(source, source + steps) for source in range(i...  8.49 us
  transfers between devices with their start and end apart: 5, of which 2 were waited for; matrix products, arithmetic and copies ran while one was open for 6% of the time, Pallas kernels for 0%

commit v1 on v0

v1 whole, which is shorter than its diff:
```python
import jax
import jax.numpy as jnp
from jax import lax
from jax.experimental import pallas as pl
from jax.experimental.pallas import tpu as pltpu
from jax.sharding import Mesh
from jax.sharding import PartitionSpec as P

HEADS = 8
HEAD_DIM = 64
STATE = 128
BLOCK = 128
WIDTH = HEADS * HEAD_DIM
RIM = 8
SP = ("z", "y")
TP = ("x", "c")
ROWS = ("y", "x")
EPSILON = 1e-05
INTERPRET = False

f32 = jnp.float32
bf16 = jnp.bfloat16
VMEM = pl.BlockSpec(memory_space=pltpu.VMEM)
SMEM = pl.BlockSpec(memory_space=pltpu.SMEM)
HBM = pl.BlockSpec(memory_space=pl.ANY)


def call(kernel, outs, in_specs, scratch=(), **kw):
    single = not isinstance(outs, (list, tuple))
    return pl.pallas_call(
        kernel,
        out_shape=outs,
        in_specs=in_specs,
        out_specs=VMEM if single else [VMEM] * len(outs),
        scratch_shapes=list(scratch),
        interpret=INTERPRET,
        **kw,
    )


def shape(dims, kind):
    return jax.ShapeDtypeStruct(dims, kind)


def exchange(value, axes):
    return lax.all_to_all(value, axes, split_axis=0, concat_axis=0, tiled=True)


def dot(a, b, dims, **kw):
    return lax.dot_general(a, b, (dims, ((), ())), preferred_element_type=f32, **kw)


def spread(rows, width):
    head = lax.broadcasted_iota(jnp.int32, (HEADS, HEADS * width), 0)
    lane = lax.broadcasted_iota(jnp.int32, (HEADS, HEADS * width), 1)
    chosen = jnp.where(lane // width == head, 1.0, 0.0).astype(f32)
    return dot(rows, chosen, ((0,), (0,)), precision=lax.Precision.HIGHEST)


def silu(value):
    return value / (1.0 + jnp.exp(-value))


def convolve(src_ref, rim, taps_ref, room):
    room[0:RIM, :] = rim.astype(f32)
    room[RIM : RIM + BLOCK, :] = src_ref[...].astype(f32)
    taps = taps_ref[...].astype(f32)
    width = taps.shape[0]
    total = None
    for k in range(width):
        start = RIM - width + 1 + k
        term = room[start : start + BLOCK, :] * taps[k : k + 1, :]
        total = term if total is None else total + term
    return silu(total)


def local_kernel(
    x_ref, b_ref, c_ref, rim_ref, xt_ref, bt_ref, ct_ref, dt_ref, shrink_ref, speed_ref, skip_ref,
    pre_ref, query_ref, cum_ref, send_ref, x_room, b_room, c_room,
):
    values = convolve(x_ref, rim_ref[:, 0:WIDTH], xt_ref, x_room)
    keys = convolve(b_ref, rim_ref[:, WIDTH : WIDTH + STATE], bt_ref, b_room).astype(bf16)
    query = convolve(c_ref, rim_ref[:, WIDTH + STATE : WIDTH + 2 * STATE], ct_ref, c_room).astype(bf16)
    query_ref[...] = query
    before = dt_ref[...]
    steps = jnp.maximum(before, 0.0) + jnp.log1p(jnp.exp(-jnp.abs(before)))
    head = lax.broadcasted_iota(jnp.int32, (HEADS, BLOCK), 0)
    token = lax.broadcasted_iota(jnp.int32, (HEADS, BLOCK), 1)
    speed = jnp.zeros((HEADS, BLOCK), f32)
    for h in range(HEADS):
        speed = jnp.where(head == h, speed_ref[h], speed)
    cum = shrink_ref[...] - jnp.exp(speed) * steps
    reach = 1
    while reach < BLOCK:
        cum = cum + jnp.where(token >= reach, pltpu.roll(cum, reach, 1), 0.0)
        reach *= 2
    cum_ref[...] = cum
    last = cum[:, BLOCK - 1 : BLOCK]
    weight = steps * jnp.exp(last - cum)
    weighted = (values * spread(weight, HEAD_DIM)).astype(bf16)
    state = dot(weighted, keys, ((0,), (0,)))
    send_ref[:, 0:8, :] = state.reshape(WIDTH // 8, 8, STATE).astype(bf16)
    row = lax.broadcasted_iota(jnp.int32, (8, STATE), 0)
    for h in range(HEADS):
        whole = jnp.broadcast_to(last[h : h + 1, :], (8, STATE))
        high = whole.astype(bf16).astype(f32)
        both = jnp.where(row == 0, high, jnp.where(row == 1, whole - high, 0.0)).astype(bf16)
        for k in range(HEAD_DIM // 8):
            send_ref[h * (HEAD_DIM // 8) + k, 8:16, :] = both
    scores = dot(query, keys, ((1,), (1,)))
    columns = spread(cum, BLOCK)
    later = lax.broadcasted_iota(jnp.int32, (BLOCK, BLOCK), 0)
    earlier = lax.broadcasted_iota(jnp.int32, (BLOCK, BLOCK), 1)
    causal = later >= earlier
    first = lax.broadcasted_iota(jnp.int32, (BLOCK, 2 * HEAD_DIM), 1) < HEAD_DIM
    for pair in range(HEADS // 2):
        lanes = slice(pair * 2 * HEAD_DIM, (pair + 1) * 2 * HEAD_DIM)
        two = values[:, lanes]
        two_low = two.astype(bf16)
        parts = []
        for h in (2 * pair, 2 * pair + 1):
            away = columns[:, h * BLOCK : (h + 1) * BLOCK] - cum[h : h + 1, :]
            mixing = scores * jnp.exp(jnp.where(causal, away, -jnp.inf)) * steps[h : h + 1, :]
            parts.append(dot(mixing.astype(bf16), two_low, ((1,), (0,))))
        within = jnp.where(first, parts[0], parts[1])
        skip = jnp.where(first, skip_ref[2 * pair], skip_ref[2 * pair + 1])
        pre_ref[:, lanes] = within + skip * two


def scan_kernel(got_ref, out_ref):
    carried = jnp.zeros((8, STATE), f32)
    for k in range(got_ref.shape[0]):
        out_ref[k] = carried.astype(bf16)
        tile = got_ref[k].astype(f32)
        factor = jnp.exp(tile[8:9, :] + tile[9:10, :])
        carried = carried * factor + tile[0:8, :]


def gate_kernel(pre_ref, query_ref, cum_ref, inc_ref, gate_ref, gain_ref, w_ref, out_ref):
    inc = inc_ref[...].reshape(WIDTH, STATE)
    arriving = dot(query_ref[...], inc, ((1,), (1,))) * spread(jnp.exp(cum_ref[...]), HEAD_DIM)
    gated = (pre_ref[...] + arriving) * silu(gate_ref[...].astype(f32))
    scale = lax.rsqrt(jnp.mean(gated * gated, axis=-1, keepdims=True) + EPSILON)
    heads_out = (gated * scale * gain_ref[...]).astype(bf16)
    out = dot(heads_out, w_ref[...], ((1,), (0,))).astype(bf16)
    out_ref[...] = out.reshape(out_ref.shape)


def norm_kernel(got_ref, skip_ref, gain_ref, own_ref, copies_ref):
    total = got_ref[0].astype(f32)
    for k in range(1, got_ref.shape[0]):
        total = total + got_ref[k].astype(f32)
    own = (skip_ref[...].astype(f32) + total.astype(bf16).astype(f32)).astype(bf16)
    own_ref[...] = own
    wide = own.astype(f32)
    scale = lax.rsqrt(jnp.mean(wide * wide, axis=-1, keepdims=True) + EPSILON)
    normed = (wide * scale * gain_ref[...]).astype(bf16)
    for k in range(copies_ref.shape[0]):
        copies_ref[k] = normed


def mlp_kernel(rows_ref, w_ref, out_ref, w_vmem, sems):
    halves, depth, both = w_ref.shape
    units = both // 2
    pieces = sems.shape[1]
    size = depth // pieces
    copies = []
    for j in range(pieces):
        for k in range(halves):
            copy = pltpu.make_async_copy(
                w_ref.at[k, pl.ds(j * size, size)], w_vmem.at[k, pl.ds(j * size, size)], sems.at[k, j]
            )
            copy.start()
            copies.append(copy)
    count, each, _ = rows_ref.shape
    rows = rows_ref[...].reshape(count * each, depth)
    lifted = [None] * halves
    for j in range(pieces):
        for k in range(halves):
            copies[j * halves + k].wait()
            part = dot(rows[:, j * size : (j + 1) * size], w_vmem[k, j * size : (j + 1) * size, 0:units], ((1,), (0,)))
            lifted[k] = part if lifted[k] is None else lifted[k] + part
    hidden = []
    for k in range(halves):
        up = jnp.maximum(lifted[k], 0.0)
        hidden.append((up * up).astype(bf16))
    for j in range(pieces):
        total = None
        for k in range(halves):
            part = dot(hidden[k], w_vmem[k, j * size : (j + 1) * size, units:both], ((1,), (1,)))
            total = part if total is None else total + part
        out_ref[:, :, j * size : (j + 1) * size] = total.astype(bf16).reshape(count, each, size)


def final_kernel(got_ref, own_ref, out_ref):
    total = got_ref[0].astype(f32)
    for k in range(1, got_ref.shape[0]):
        total = total + got_ref[k].astype(f32)
    out_ref[...] = (own_ref[...].astype(f32) + total.astype(bf16).astype(f32)).astype(bf16)


def per_device(
    skip_stream_entering,
    content_signal_matrix,
    writer_signal_matrix,
    reader_signal_matrix,
    multiplier_signal,
    interval_before_softplus,
    extra_log_shrink,
    log_forget_speed,
    content_filter_coefs,
    writer_filter_coefs,
    reader_filter_coefs,
    skip_path_factor,
    cluster_scaling_vector,
    blend_result_matrix,
    feature_blend_scaling,
    widening_matrix,
    narrowing_matrix,
):
    ny = lax.axis_size("y")
    nsp = lax.axis_size("z") * ny
    ntp = lax.axis_size("x") * lax.axis_size("c")
    nrows = ny * lax.axis_size("x")
    width = skip_stream_entering.shape[1]
    own_count = skip_stream_entering.shape[0]

    rim = jnp.concatenate(
        [
            content_signal_matrix[BLOCK - RIM :],
            writer_signal_matrix[BLOCK - RIM :],
            reader_signal_matrix[BLOCK - RIM :],
        ],
        axis=1,
    )
    rim = lax.ppermute(rim, SP, [(k, k + 1) for k in range(nsp - 1)])

    depth, units = widening_matrix.shape
    slim = units // ny
    mine = jnp.concatenate(
        [widening_matrix.reshape(depth, ny, slim), narrowing_matrix.T.reshape(depth, ny, slim)], axis=2
    )
    mine = jnp.moveaxis(mine, 1, 0)
    parts = exchange(mine, "y").reshape(ny * depth, 2 * slim)
    weights = lax.all_gather(parts, ("c", "z"), axis=0, tiled=True).reshape(-1, width, 2 * slim)

    rim, content_signal_matrix, parts = lax.optimization_barrier((rim, content_signal_matrix, parts))
    pre, query, cum, send = call(
        local_kernel,
        [
            shape((BLOCK, WIDTH), f32),
            shape((BLOCK, STATE), bf16),
            shape((HEADS, BLOCK), f32),
            shape((nsp, 16, STATE), bf16),
        ],
        [VMEM] * 9 + [SMEM] * 2,
        [pltpu.VMEM((RIM + BLOCK, n), f32) for n in (WIDTH, STATE, STATE)],
    )(
        content_signal_matrix,
        writer_signal_matrix,
        reader_signal_matrix,
        rim,
        content_filter_coefs,
        writer_filter_coefs,
        reader_filter_coefs,
        interval_before_softplus,
        extra_log_shrink,
        log_forget_speed,
        skip_path_factor,
    )
    got = exchange(send, SP)
    before = call(scan_kernel, shape((nsp, 8, STATE), bf16), [VMEM])(got)
    incoming = exchange(before, SP)
    mixed = call(gate_kernel, shape((ntp, own_count, width), bf16), [VMEM] * 7)(
        pre,
        query,
        cum,
        incoming,
        multiplier_signal,
        cluster_scaling_vector.reshape(1, -1),
        blend_result_matrix,
    )
    mixed = exchange(mixed, TP)
    own, copies = call(
        norm_kernel,
        [shape((own_count, width), bf16), shape((nrows, own_count, width), bf16)],
        [VMEM] * 3,
    )(mixed, skip_stream_entering, feature_blend_scaling.reshape(1, -1))
    rows = exchange(copies, ROWS)
    out = call(
        mlp_kernel,
        shape((nrows, own_count, width), bf16),
        [VMEM, HBM],
        [pltpu.VMEM(weights.shape, bf16), pltpu.SemaphoreType.DMA((weights.shape[0], 4))],
    )(rows, weights)
    out = exchange(out, ROWS)
    return call(final_kernel, shape((own_count, width), bf16), [VMEM] * 2)(out, own)


def solution(mesh):
    torus = Mesh(mesh.devices.reshape(16, 4, 4, 2), ("z", "y", "x", "c"))
    placed = (
        P(SP + TP, None),
        P(SP, TP),
        P(SP, TP),
        P(SP, TP),
        P(SP, TP),
        P(TP, SP),
        P(TP, SP),
        P(TP),
        P(None, TP),
        P(None, TP),
        P(None, TP),
        P(TP),
        P(TP),
        P(TP, None),
        P(),
        P(SP, TP),
        P(TP, SP),
    )
    return jax.shard_map(
        per_device, mesh=torus, in_specs=placed, out_specs=P(SP + TP, None), check_vma=False
    )
```

time: 305 us -> 176 us (0.58)
  waiting for transfers between devices: 152 us -> 0.83 us
  blocking collectives: 104 us -> 135 us
  Pallas kernels: 0 us -> 19.1 us
  other arithmetic: 10.1 us -> 0.07 us
  matrix products: 9.51 us -> 0 us
  starting transfers between devices: 8.53 us -> 2.18 us
    all_gather x2 -> x1, waiting for transfers between devices: 152 us -> 0.01 us  [per_device(): lax.all_gather(parts, ('c', 'z'), axis=0, tiled=True)]
    all_to_all x3 -> x6, blocking collectives: 57.9 us -> 135 us  [exchange(): return lax.all_to_all(value, axes, split_axis=0, concat_axis=0, tiled=True)]
    all_gather x3 -> x0, blocking collectives: 46.3 us -> none  [entering_2(): lax.all_gather(part.astype(kind), axis)]
    pallas_call x0 -> x6, Pallas kernels: none -> 19.1 us  [the longest x1 5.8 us: per_device(): call(mlp_kernel, shape((nrows, own_count, width), bf16), [VMEM, HBM], [pl...]
    dot_general x7 -> x0, matrix products: 9.51 us -> none  [the longest x1 5.56 us: per_device(): jnp.dot(hidden, down_whole, preferred_element_type=jnp.float32)]
    ppermute x3 -> x1, starting transfers between devices: 8.49 us -> 2.18 us  [per_device(): rim = lax.ppermute(rim, SP, [(k, k + 1) for k in range(nsp - 1)])]
    mul x8 -> x0, other arithmetic: 5.77 us -> none  [the longest x3 2.52 us: convolve(): extended[0:length].astype(jnp.float32) * conv_taps[0].astype(jnp.float32)]
  transfers between devices with their start and end apart: 5 -> 2, of which waited for: 2 -> 1; matrix products, arithmetic and copies ran while one was open for 6% -> 1% of each run, Pallas kernels for 0% -> 6%
where the time goes in v1:
time: 176 us; the launch traced here: 175 us
  blocking collectives  135 us (77%)
  Pallas kernels  19.1 us (11%)
  between operations  13.4 us (8%)
  local copies, waits for them, and re-layouts  4.43 us (3%)
  starting transfers between devices  2.18 us (1%)
    all_to_all x6, blocking collectives, exchange(): return lax.all_to_all(value, axes, split_axis=0, concat_axis=0, tiled=True)  135 us
    pallas_call x1, Pallas kernels, per_device(): call(mlp_kernel, shape((nrows, own_count, width), bf16), [VMEM, HBM], [pl...  5.8 us
    pallas_call x1, Pallas kernels, per_device(): call(local_kernel, [shape((BLOCK, WIDTH), f32), shape((BLOCK, STATE), bf1...  3.65 us
    pallas_call x1, Pallas kernels, per_device(): call(gate_kernel, shape((ntp, own_count, width), bf16), [VMEM] * 7)  3.56 us
  transfers between devices with their start and end apart: 2, of which 1 were waited for; matrix products, arithmetic and copies ran while one was open for 1% of the time, Pallas kernels for 6%

profile of v1, /device:TPU:1, one launch (start us, length us, event | category | flops | bytes accessed | tf_op | source)
XLA Modules:
  0.0 174.8 jit_solution(16859867663804470748)
XLA Ops:
  6.5 0.0 all-gather.2.cloned.1.call-start
  6.5 0.9 reshape.18
  7.4 0.9 reshape.19
  8.3 0.1 maximum_bitcast_fusion
  8.4 9.7 %all_to_all.30 = bf16[4,32,512]{2,1,0:T(8,128)(2,1)} all-to-all(bf16[4,32,512]{2,1,0:T(8,128)(2,1)S(1)} %copy.19), channel_id=1, replica_groups=mesh['z'=16,'y'=4,'x'=4,'c'=2] {'y'}, dimensions={0} | all-to-all | bytes 262144 | tf_op jit(solution)/shard_map/all_to_all | solution.py:46
  18.1 0.0 all-gather.2.cloned.1.call-update
  18.2 0.7 slice.9
  18.9 0.7 slice.10
  19.5 0.7 slice.11
  20.2 2.2 %collective-permute-start = (bf16[8,768]{1,0:T(8,128)(2,1)S(1)}, bf16[8,768]{1,0:T(8,128)(2,1)S(1)}, u32[]{:S(2)}, u32[]{:S(2)}) collective-permute-start(bf16[8,768]{1,0:T(8,128)(2,1)S(1)} %pad_maximum_fusion), channel_id=1, source_target_pairs={{0,8},{8,16},{16,24},{24,32},{32,40},{40,48},{48,56},{56,64},{64,7... | collective-permute-start | bytes 36872 | tf_op jit(solution)/shard_map/ppermute | solution.py:236
  22.4 0.8 collective-permute-done.rim_ref
  23.2 0.0 copy-start
  23.2 0.6 copy-done
  23.8 3.6 %shard_map.163 = (f32[128,512]{1,0:T(8,128)}, bf16[128,128]{1,0:T(8,128)(2,1)}, f32[8,128]{1,0:T(8,128)}, bf16[64,16,128]{2,1,0:T(8,128)(2,1)}) custom-call(bf16[128,512]{1,0:T(8,128)(2,1)} %x_ref, bf16[128,128]{1,0:T(8,128)(2,1)} %b_ref.1, bf16[128,128]{1,0:T(8,128)(2,1)} %c_ref.1, bf16[8,768]{1,0:T(8,128)(2,1)} %copy-done, bf16[4,512]{1,0:T(4,128)(2,1)} %xt_ref.1, ...), custom_call_target="tpu_custom_call" | custom-call | tf_op jit(solution)/shard_map/pallas_call | solution.py:248
  27.5 42.4 %all_to_all.31.got_ref = bf16[64,16,128]{2,1,0:T(8,128)(2,1)} all-to-all(bf16[64,16,128]{2,1,0:T(8,128)(2,1)} %get-tuple-element.18), channel_id=1, replica_groups=mesh['z'=16,'y'=4,'x'=4,'c'=2] {'z','y'}, dimensions={0} | all-to-all | bytes 524288 | tf_op jit(solution)/shard_map/all_to_all | solution.py:46
  69.9 1.7 shard_map.164
  71.7 22.8 %all_to_all.32.inc_ref = bf16[64,8,128]{2,1,0:T(8,128)(2,1)} all-to-all(bf16[64,8,128]{2,1,0:T(8,128)(2,1)} %shard_map.164), channel_id=1, replica_groups=mesh['z'=16,'y'=4,'x'=4,'c'=2] {'z','y'}, dimensions={0} | all-to-all | bytes 262144 | tf_op jit(solution)/shard_map/all_to_all | solution.py:46
  94.5 3.6 %shard_map.165 = bf16[8,16,2048]{2,1,0:T(8,128)(2,1)} custom-call(f32[128,512]{1,0:T(8,128)} %get-tuple-element.15.pre_ref, bf16[128,128]{1,0:T(8,128)(2,1)} %get-tuple-element.16.query_ref, f32[8,128]{1,0:T(8,128)} %get-tuple-element.17.cum_ref, bf16[64,8,128]{2,1,0:T(8,128)(2,1)} %all_to_all.32.inc_ref, bf16[128,512]{1,0:T(8,128)(2,1)} %gate_ref.1, ...), custom_call_target="tpu_custom_call" | custom-call | tf_op jit(solution)/shard_map/pallas_call | solution.py:274
  98.0 19.6 %all_to_all.33.got_ref = bf16[8,16,2048]{2,1,0:T(8,128)(2,1)} all-to-all(bf16[8,16,2048]{2,1,0:T(8,128)(2,1)} %shard_map.165), channel_id=1, replica_groups=mesh['z'=16,'y'=4,'x'=4,'c'=2] {'x','c'}, dimensions={0} | all-to-all | bytes 1048576 | tf_op jit(solution)/shard_map/all_to_all | solution.py:46
  117.6 2.3 %shard_map.166 = (bf16[16,2048]{1,0:T(8,128)(2,1)}, bf16[16,16,2048]{2,1,0:T(8,128)(2,1)}) custom-call(bf16[8,16,2048]{2,1,0:T(8,128)(2,1)} %all_to_all.33.got_ref, bf16[16,2048]{1,0:T(8,128)(2,1)} %skip_ref.3, f32[1,2048]{1,0:T(1,128)} %bitcast.10), custom_call_target="tpu_custom_call" | custom-call | tf_op jit(solution)/shard_map/pallas_call | solution.py:284
  119.9 20.5 %all_to_all.34.rows_ref = bf16[16,16,2048]{2,1,0:T(8,128)(2,1)} all-to-all(bf16[16,16,2048]{2,1,0:T(8,128)(2,1)} %get-tuple-element.19), channel_id=1, replica_groups=mesh['z'=16,'y'=4,'x'=4,'c'=2] {'y','x'}, dimensions={0} | all-to-all | bytes 2097152 | tf_op jit(solution)/shard_map/all_to_all | solution.py:46
  140.4 0.0 all-gather.2.cloned.1.call-done
  140.4 5.8 %shard_map.167 = bf16[16,16,2048]{2,1,0:T(8,128)(2,1)} custom-call(bf16[16,16,2048]{2,1,0:T(8,128)(2,1)} %all_to_all.34.rows_ref, bf16[2,2048,512]{2,1,0:T(8,128)(2,1)} %bitcast.7), custom_call_target="tpu_custom_call" | custom-call | tf_op jit(solution)/shard_map/pallas_call | solution.py:290
  146.2 19.7 %all_to_all.35.got_ref = bf16[16,16,2048]{2,1,0:T(8,128)(2,1)} all-to-all(bf16[16,16,2048]{2,1,0:T(8,128)(2,1)} %shard_map.167), channel_id=1, replica_groups=mesh['z'=16,'y'=4,'x'=4,'c'=2] {'y','x'}, dimensions={0} | all-to-all | bytes 2097152 | tf_op jit(solution)/shard_map/all_to_all | solution.py:46
  166.0 2.0 %shard_map.168 = bf16[16,2048]{1,0:T(8,128)(2,1)} custom-call(bf16[16,16,2048]{2,1,0:T(8,128)(2,1)} %all_to_all.35.got_ref, bf16[16,2048]{1,0:T(8,128)(2,1)} %get-tuple-element.20.own_ref), custom_call_target="tpu_custom_call" | custom-call | tf_op jit(solution)/shard_map/pallas_call | solution.py:297
  (2 shorter events, 0.0 us)
Async XLA Ops:
  6.5 133.9 %all-gather.2.cloned.1.call-start = ((), (), s32[]{:S(2)}) async-start(), calls=%async_computation.6 | async-start | bytes 4325376 | tf_op jit(solution)/shard_map/all_gather | solution.py:245
  20.2 3.0 %collective-permute-start = (bf16[8,768]{1,0:T(8,128)(2,1)S(1)}, bf16[8,768]{1,0:T(8,128)(2,1)S(1)}, u32[]{:S(2)}, u32[]{:S(2)}) collective-permute-start(bf16[8,768]{1,0:T(8,128)(2,1)S(1)} %pad_maximum_fusion), channel_id=1, source_target_pairs={{0,8},{8,16},{16,24},{24,32},{32,40},{40,48},{48,56},{56,64},{64,7... | collective-permute-start | bytes 36872 | tf_op jit(solution)/shard_map/ppermute | solution.py:236
  23.2 0.6 copy-start
Sparse Core Ops, SparseCore 0:
  18.3 85.3 all-gather.1

commit v2 on v1

--- a/solution.py
+++ b/solution.py
@@ -39,7 +39,11 @@
 
 
 def shape(dims, kind):
-    return jax.ShapeDtypeStruct(dims, kind)
+    return jax.ShapeDtypeStruct(dims, kind) if INTERPRET else pltpu.VMEM(dims, kind)
+
+
+def near(value):
+    return value if INTERPRET else pltpu.with_memory_space_constraint(value, pltpu.VMEM)
 
 
 def exchange(value, axes):
@@ -72,6 +76,16 @@
         term = room[start : start + BLOCK, :] * taps[k : k + 1, :]
         total = term if total is None else total + term
     return silu(total)
+
+
+def first_kernel(x_ref, b_ref, c_ref, up_ref, down_ref, rim_ref, mine_ref):
+    rim_ref[:, 0:WIDTH] = x_ref[...]
+    rim_ref[:, WIDTH : WIDTH + STATE] = b_ref[...]
+    rim_ref[:, WIDTH + STATE : WIDTH + 2 * STATE] = c_ref[...]
+    slim = mine_ref.shape[2] // 2
+    for k in range(mine_ref.shape[0]):
+        mine_ref[k, :, 0:slim] = up_ref[:, k * slim : (k + 1) * slim]
+        mine_ref[k, :, slim : 2 * slim] = down_ref[:, k * slim : (k + 1) * slim]
 
 
 def local_kernel(
@@ -136,13 +150,16 @@
         carried = carried * factor + tile[0:8, :]
 
 
-def gate_kernel(pre_ref, query_ref, cum_ref, inc_ref, gate_ref, gain_ref, w_ref, out_ref):
+def gate_kernel(pre_ref, query_ref, cum_ref, inc_ref, gate_ref, gain_ref, w_ref, out_ref, w_room, sem):
+    copy = pltpu.make_async_copy(w_ref, w_room, sem)
+    copy.start()
     inc = inc_ref[...].reshape(WIDTH, STATE)
     arriving = dot(query_ref[...], inc, ((1,), (1,))) * spread(jnp.exp(cum_ref[...]), HEAD_DIM)
     gated = (pre_ref[...] + arriving) * silu(gate_ref[...].astype(f32))
     scale = lax.rsqrt(jnp.mean(gated * gated, axis=-1, keepdims=True) + EPSILON)
     heads_out = (gated * scale * gain_ref[...]).astype(bf16)
-    out = dot(heads_out, w_ref[...], ((1,), (0,))).astype(bf16)
+    copy.wait()
+    out = dot(heads_out, w_room[...], ((1,), (0,))).astype(bf16)
     out_ref[...] = out.reshape(out_ref.shape)
 
 
@@ -225,26 +242,25 @@
     width = skip_stream_entering.shape[1]
     own_count = skip_stream_entering.shape[0]
 
-    rim = jnp.concatenate(
-        [
-            content_signal_matrix[BLOCK - RIM :],
-            writer_signal_matrix[BLOCK - RIM :],
-            reader_signal_matrix[BLOCK - RIM :],
-        ],
-        axis=1,
-    )
-    rim = lax.ppermute(rim, SP, [(k, k + 1) for k in range(nsp - 1)])
-
     depth, units = widening_matrix.shape
     slim = units // ny
-    mine = jnp.concatenate(
-        [widening_matrix.reshape(depth, ny, slim), narrowing_matrix.T.reshape(depth, ny, slim)], axis=2
-    )
-    mine = jnp.moveaxis(mine, 1, 0)
+    rim, mine = pl.pallas_call(
+        first_kernel,
+        grid=(1,),
+        out_shape=[shape((RIM, WIDTH + 2 * STATE), bf16), shape((ny, depth, 2 * slim), bf16)],
+        in_specs=[pl.BlockSpec((RIM, n), lambda i: (BLOCK // RIM - 1, 0)) for n in (WIDTH, STATE, STATE)]
+        + [pl.BlockSpec((depth, units), lambda i: (0, 0))] * 2,
+        out_specs=[
+            pl.BlockSpec((RIM, WIDTH + 2 * STATE), lambda i: (0, 0)),
+            pl.BlockSpec((ny, depth, 2 * slim), lambda i: (0, 0, 0)),
+        ],
+        interpret=INTERPRET,
+    )(content_signal_matrix, writer_signal_matrix, reader_signal_matrix, widening_matrix, narrowing_matrix.T)
+    rim = lax.ppermute(rim, SP, [(k, k + 1) for k in range(nsp - 1)])
     parts = exchange(mine, "y").reshape(ny * depth, 2 * slim)
     weights = lax.all_gather(parts, ("c", "z"), axis=0, tiled=True).reshape(-1, width, 2 * slim)
 
-    rim, content_signal_matrix, parts = lax.optimization_barrier((rim, content_signal_matrix, parts))
+    rim, parts = lax.optimization_barrier((rim, parts))
     pre, query, cum, send = call(
         local_kernel,
         [
@@ -259,7 +275,7 @@
         content_signal_matrix,
         writer_signal_matrix,
         reader_signal_matrix,
-        rim,
+        near(rim),
         content_filter_coefs,
         writer_filter_coefs,
         reader_filter_coefs,
@@ -269,13 +285,18 @@
         skip_path_factor,
     )
     got = exchange(send, SP)
-    before = call(scan_kernel, shape((nsp, 8, STATE), bf16), [VMEM])(got)
+    before = call(scan_kernel, shape((nsp, 8, STATE), bf16), [VMEM])(near(got))
     incoming = exchange(before, SP)
-    mixed = call(gate_kernel, shape((ntp, own_count, width), bf16), [VMEM] * 7)(
-        pre,
-        query,
-        cum,
-        incoming,
+    mixed = call(
+        gate_kernel,
+        shape((ntp, own_count, width), bf16),
+        [VMEM] * 6 + [HBM],
+        [pltpu.VMEM(blend_result_matrix.shape, bf16), pltpu.SemaphoreType.DMA(())],
+    )(
+        near(pre),
+        near(query),
+        near(cum),
+        near(incoming),
         multiplier_signal,
         cluster_scaling_vector.reshape(1, -1),
         blend_result_matrix,
@@ -285,16 +306,16 @@
         norm_kernel,
         [shape((own_count, width), bf16), shape((nrows, own_count, width), bf16)],
         [VMEM] * 3,
-    )(mixed, skip_stream_entering, feature_blend_scaling.reshape(1, -1))
+    )(near(mixed), skip_stream_entering, feature_blend_scaling.reshape(1, -1))
     rows = exchange(copies, ROWS)
     out = call(
         mlp_kernel,
         shape((nrows, own_count, width), bf16),
         [VMEM, HBM],
         [pltpu.VMEM(weights.shape, bf16), pltpu.SemaphoreType.DMA((weights.shape[0], 4))],
-    )(rows, weights)
+    )(near(rows), weights)
     out = exchange(out, ROWS)
-    return call(final_kernel, shape((own_count, width), bf16), [VMEM] * 2)(out, own)
+    return call(final_kernel, jax.ShapeDtypeStruct((own_count, width), bf16), [VMEM] * 2)(near(out), near(own))
 
 
 def solution(mesh):

time: 176 us -> 160 us (0.909)
  Pallas kernels: 19.1 us -> 12.8 us
  blocking collectives: 135 us -> 129 us
  local copies, waits for them, and re-layouts: 4.43 us -> 0 us
    all_to_all x6, blocking collectives: 135 us -> 129 us  [exchange(): return lax.all_to_all(value, axes, split_axis=0, concat_axis=0, tiled=True)]
    pallas_call x1, Pallas kernels: 5.8 us -> 3.58 us  [per_device(): call(mlp_kernel, shape((nrows, own_count, width), bf16), [VMEM, HBM], [pl...]
    pallas_call x3 -> x4, Pallas kernels: 7.31 us -> 5.24 us  [the longest x1 3.38 us: per_device(): call(gate_kernel, shape((ntp, own_count, width), bf16), [VMEM] * 6 + [HBM...]
    slice x3 -> x0, local copies, waits for them, and re-layouts: 2.07 us -> none  [the longest x1 0.7 us: per_device(): content_signal_matrix[BLOCK - RIM:]]
  transfers between devices with their start and end apart: 2 -> 2, of which waited for: 1 -> 1; matrix products, arithmetic and copies ran while one was open for 1% -> 0% of each run, Pallas kernels for 6% -> 5%
where the time goes in v2:
time: 160 us; the launch traced here: 158 us
  blocking collectives  129 us (81%)
  between operations  13.4 us (8%)
  Pallas kernels  12.8 us (8%)
  starting transfers between devices  2.19 us (1%)
    all_to_all x6, blocking collectives, exchange(): return lax.all_to_all(value, axes, split_axis=0, concat_axis=0, tiled=True)  129 us
    pallas_call x1, Pallas kernels, per_device(): call(mlp_kernel, shape((nrows, own_count, width), bf16), [VMEM, HBM], [pl...  3.58 us
    pallas_call x1, Pallas kernels, per_device(): call(gate_kernel, shape((ntp, own_count, width), bf16), [VMEM] * 6 + [HBM...  3.38 us
  transfers between devices with their start and end apart: 2, of which 1 were waited for; matrix products, arithmetic and copies ran while one was open for 0% of the time, Pallas kernels for 5%

profile of v2, /device:TPU:1, one launch (start us, length us, event | category | flops | bytes accessed | tf_op | source)
XLA Modules:
  0.0 158.5 jit_solution(9180529941211480649)
XLA Ops:
  6.5 0.0 all-gather.2.cloned.1.call-start
  6.5 0.9 shard_map.163
  7.5 9.7 %all_to_all.30 = bf16[4,32,512]{2,1,0:T(8,128)(2,1)} all-to-all(bf16[4,32,512]{2,1,0:T(8,128)(2,1)S(1)} %get-tuple-element.15), channel_id=1, replica_groups=mesh['z'=16,'y'=4,'x'=4,'c'=2] {'y'}, dimensions={0} | all-to-all | bytes 262144 | tf_op jit(solution)/shard_map/all_to_all | solution.py:50
  17.2 0.0 all-gather.2.cloned.1.call-update
  17.2 2.2 %collective-permute-start = (bf16[8,768]{1,0:T(8,128)(2,1)S(1)}, bf16[8,768]{1,0:T(8,128)(2,1)S(1)}, u32[]{:S(2)}, u32[]{:S(2)}) collective-permute-start(bf16[8,768]{1,0:T(8,128)(2,1)S(1)} %get-tuple-element.14), channel_id=1, source_target_pairs={{0,8},{8,16},{16,24},{24,32},{32,40},{40,48},{48,56},{56,64},{64,7... | collective-permute-start | bytes 36872 | tf_op jit(solution)/shard_map/ppermute | solution.py:259
  19.4 0.8 collective-permute-done.rim_ref
  20.2 2.9 %shard_map.164 = (f32[128,512]{1,0:T(8,128)S(1)}, bf16[128,128]{1,0:T(8,128)(2,1)S(1)}, f32[8,128]{1,0:T(8,128)S(1)}, bf16[64,16,128]{2,1,0:T(8,128)(2,1)S(1)}) custom-call(bf16[128,512]{1,0:T(8,128)(2,1)} %x_ref.3, bf16[128,128]{1,0:T(8,128)(2,1)} %b_ref.3, bf16[128,128]{1,0:T(8,128)(2,1)} %c_ref.3, bf16[8,768]{1,0:T(8,128)(2,1)S(1)} %collective-permute-done.rim_ref, ...), custom_call_target="tpu_custom_call" | custom-call | tf_op jit(solution)/shard_map/pallas_call | solution.py:264
  23.1 40.5 %all_to_all.31.got_ref = bf16[64,16,128]{2,1,0:T(8,128)(2,1)S(1)} all-to-all(bf16[64,16,128]{2,1,0:T(8,128)(2,1)S(1)} %get-tuple-element.20), channel_id=1, replica_groups=mesh['z'=16,'y'=4,'x'=4,'c'=2] {'z','y'}, dimensions={0} | all-to-all | bytes 524288 | tf_op jit(solution)/shard_map/all_to_all | solution.py:50
  63.6 0.1 shard_map.165
  63.8 24.1 %all_to_all.32.inc_ref = bf16[64,8,128]{2,1,0:T(8,128)(2,1)S(1)} all-to-all(bf16[64,8,128]{2,1,0:T(8,128)(2,1)S(1)} %shard_map.165), channel_id=1, replica_groups=mesh['z'=16,'y'=4,'x'=4,'c'=2] {'z','y'}, dimensions={0} | all-to-all | bytes 262144 | tf_op jit(solution)/shard_map/all_to_all | solution.py:50
  87.9 3.4 %shard_map.166 = bf16[8,16,2048]{2,1,0:T(8,128)(2,1)S(1)} custom-call(f32[128,512]{1,0:T(8,128)S(1)} %get-tuple-element.17.pre_ref, bf16[128,128]{1,0:T(8,128)(2,1)S(1)} %get-tuple-element.18.query_ref, f32[8,128]{1,0:T(8,128)S(1)} %get-tuple-element.19.cum_ref, bf16[64,8,128]{2,1,0:T(8,128)(2,1)S(1)} %all_to_all.32.inc_ref, bf16[128,512]{1,0:T(8,128)(2,1)} %gate_ref.1, ...), custom_call_target="tpu_custom_call" | custom-call | tf_op jit(solution)/shard_map/pallas_call | solution.py:290
  91.3 17.5 %all_to_all.33.got_ref = bf16[8,16,2048]{2,1,0:T(8,128)(2,1)S(1)} all-to-all(bf16[8,16,2048]{2,1,0:T(8,128)(2,1)S(1)} %shard_map.166), channel_id=1, replica_groups=mesh['z'=16,'y'=4,'x'=4,'c'=2] {'x','c'}, dimensions={0} | all-to-all | bytes 1048576 | tf_op jit(solution)/shard_map/all_to_all | solution.py:50
  108.8 1.1 shard_map.167
  109.9 19.1 %all_to_all.34.rows_ref = bf16[16,16,2048]{2,1,0:T(8,128)(2,1)S(1)} all-to-all(bf16[16,16,2048]{2,1,0:T(8,128)(2,1)S(1)} %get-tuple-element.21), channel_id=1, replica_groups=mesh['z'=16,'y'=4,'x'=4,'c'=2] {'y','x'}, dimensions={0} | all-to-all | bytes 2097152 | tf_op jit(solution)/shard_map/all_to_all | solution.py:50
  129.0 0.0 all-gather.2.cloned.1.call-done
  129.0 3.6 %shard_map.168 = bf16[16,16,2048]{2,1,0:T(8,128)(2,1)S(1)} custom-call(bf16[16,16,2048]{2,1,0:T(8,128)(2,1)S(1)} %all_to_all.34.rows_ref, bf16[2,2048,512]{2,1,0:T(8,128)(2,1)} %bitcast.5), custom_call_target="tpu_custom_call" | custom-call | tf_op jit(solution)/shard_map/pallas_call | solution.py:311
  132.5 18.3 %all_to_all.35.got_ref = bf16[16,16,2048]{2,1,0:T(8,128)(2,1)S(1)} all-to-all(bf16[16,16,2048]{2,1,0:T(8,128)(2,1)S(1)} %shard_map.168), channel_id=1, replica_groups=mesh['z'=16,'y'=4,'x'=4,'c'=2] {'y','x'}, dimensions={0} | all-to-all | bytes 2097152 | tf_op jit(solution)/shard_map/all_to_all | solution.py:50
  150.9 0.8 shard_map.169
Async XLA Ops:
  6.5 122.4 %all-gather.2.cloned.1.call-start = ((), (), s32[]{:S(2)}) async-start(), calls=%async_computation.6 | async-start | bytes 4325376 | tf_op jit(solution)/shard_map/all_gather | solution.py:261
  17.2 3.0 %collective-permute-start = (bf16[8,768]{1,0:T(8,128)(2,1)S(1)}, bf16[8,768]{1,0:T(8,128)(2,1)S(1)}, u32[]{:S(2)}, u32[]{:S(2)}) collective-permute-start(bf16[8,768]{1,0:T(8,128)(2,1)S(1)} %get-tuple-element.14), channel_id=1, source_target_pairs={{0,8},{8,16},{16,24},{24,32},{32,40},{40,48},{48,56},{56,64},{64,7... | collective-permute-start | bytes 36872 | tf_op jit(solution)/shard_map/ppermute | solution.py:259
Sparse Core Ops, SparseCore 0:
  17.4 86.6 all-gather.1

commit v3 on v2

--- a/solution.py
+++ b/solution.py
@@ -12,7 +12,9 @@
 BLOCK = 128
 WIDTH = HEADS * HEAD_DIM
 RIM = 8
-SP = ("z", "y")
+PAIR = 2 * HEAD_DIM
+TAIL = 16
+SP = ("zh", "zl", "y")
 TP = ("x", "c")
 ROWS = ("y", "x")
 EPSILON = 1e-05
@@ -78,18 +80,36 @@
     return silu(total)
 
 
-def first_kernel(x_ref, b_ref, c_ref, up_ref, down_ref, rim_ref, mine_ref):
+def put_state(ref, place, start, state, logs):
+    ref[place, start : start + PAIR, :] = state.astype(bf16)
+    row = lax.broadcasted_iota(jnp.int32, (TAIL, STATE), 0)
+    tail = jnp.zeros((TAIL, STATE), f32)
+    for h in range(2):
+        whole = jnp.broadcast_to(logs[h : h + 1, :], (TAIL, STATE))
+        high = whole.astype(bf16).astype(f32)
+        tail = jnp.where(row == 2 * h, high, jnp.where(row == 2 * h + 1, whole - high, tail))
+    ref[place, start + PAIR : start + PAIR + TAIL, :] = tail.astype(bf16)
+
+
+def take_state(ref, place, start):
+    state = ref[place, start : start + PAIR, :].astype(f32)
+    tail = ref[place, start + PAIR : start + PAIR + TAIL, :].astype(f32)
+    return state, jnp.concatenate([tail[2 * h : 2 * h + 1, :] + tail[2 * h + 1 : 2 * h + 2, :] for h in range(2)], axis=0)
+
+
+def factor(logs):
+    grown = jnp.exp(logs)
+    return jnp.concatenate([jnp.broadcast_to(grown[h : h + 1, :], (HEAD_DIM, STATE)) for h in range(2)], axis=0)
+
+
+def first_kernel(x_ref, b_ref, c_ref, rim_ref):
     rim_ref[:, 0:WIDTH] = x_ref[...]
     rim_ref[:, WIDTH : WIDTH + STATE] = b_ref[...]
     rim_ref[:, WIDTH + STATE : WIDTH + 2 * STATE] = c_ref[...]
-    slim = mine_ref.shape[2] // 2
-    for k in range(mine_ref.shape[0]):
-        mine_ref[k, :, 0:slim] = up_ref[:, k * slim : (k + 1) * slim]
-        mine_ref[k, :, slim : 2 * slim] = down_ref[:, k * slim : (k + 1) * slim]
 
 
 def local_kernel(
-    x_ref, b_ref, c_ref, rim_ref, xt_ref, bt_ref, ct_ref, dt_ref, shrink_ref, speed_ref, skip_ref,
+    x_ref, b_ref, c_ref, rim_ref, xt_ref, bt_ref, ct_ref, dt_ref, shrink_ref, up_ref, down_ref, speed_ref, skip_ref,
     pre_ref, query_ref, cum_ref, send_ref, x_room, b_room, c_room,
 ):
     values = convolve(x_ref, rim_ref[:, 0:WIDTH], xt_ref, x_room)
@@ -113,14 +133,15 @@
     weight = steps * jnp.exp(last - cum)
     weighted = (values * spread(weight, HEAD_DIM)).astype(bf16)
     state = dot(weighted, keys, ((0,), (0,)))
-    send_ref[:, 0:8, :] = state.reshape(WIDTH // 8, 8, STATE).astype(bf16)
-    row = lax.broadcasted_iota(jnp.int32, (8, STATE), 0)
-    for h in range(HEADS):
-        whole = jnp.broadcast_to(last[h : h + 1, :], (8, STATE))
-        high = whole.astype(bf16).astype(f32)
-        both = jnp.where(row == 0, high, jnp.where(row == 1, whole - high, 0.0)).astype(bf16)
-        for k in range(HEAD_DIM // 8):
-            send_ref[h * (HEAD_DIM // 8) + k, 8:16, :] = both
+    pieces = send_ref.shape[0]
+    depth, units = up_ref.shape
+    slabs = units // pieces // STATE
+    for k in range(pieces):
+        for j in range(slabs):
+            lanes = slice((k * slabs + j) * STATE, (k * slabs + j + 1) * STATE)
+            send_ref[k, j * depth : (j + 1) * depth, :] = up_ref[:, lanes]
+            send_ref[k, (slabs + j) * depth : (slabs + j + 1) * depth, :] = down_ref[:, lanes]
+        put_state(send_ref, k, 2 * slabs * depth, state[k * PAIR : (k + 1) * PAIR, :], last[2 * k : 2 * k + 2, :])
     scores = dot(query, keys, ((1,), (1,)))
     columns = spread(cum, BLOCK)
     later = lax.broadcasted_iota(jnp.int32, (BLOCK, BLOCK), 0)
@@ -141,13 +162,45 @@
         pre_ref[:, lanes] = within + skip * two
 
 
-def scan_kernel(got_ref, out_ref):
-    carried = jnp.zeros((8, STATE), f32)
+def row_kernel(got_ref, shard_ref, send_ref):
+    start = shard_ref.shape[1]
+    state = logs = None
     for k in range(got_ref.shape[0]):
-        out_ref[k] = carried.astype(bf16)
-        tile = got_ref[k].astype(f32)
-        factor = jnp.exp(tile[8:9, :] + tile[9:10, :])
-        carried = carried * factor + tile[0:8, :]
+        shard_ref[k] = got_ref[k, 0:start, :]
+        more, step = take_state(got_ref, k, start)
+        state, logs = (more, step) if state is None else (state * factor(step) + more, logs + step)
+    for k in range(send_ref.shape[0]):
+        put_state(send_ref, k, 0, state, logs)
+
+
+def near_kernel(got_ref, send_ref, state_ref, logs_ref):
+    here = lax.axis_index("zl")
+    state = before = jnp.zeros((PAIR, STATE), f32)
+    logs = passed = jnp.zeros((2, STATE), f32)
+    for k in range(got_ref.shape[0]):
+        more, step = take_state(got_ref, k, 0)
+        state, logs = state * factor(step) + more, logs + step
+        before, passed = jnp.where(k < here, state, before), jnp.where(k < here, logs, passed)
+    state_ref[...] = before
+    logs_ref[...] = passed
+    for k in range(send_ref.shape[0]):
+        put_state(send_ref, k, 0, state, logs)
+
+
+def far_kernel(got_ref, state_ref, logs_ref, rows_ref, out_ref):
+    here = lax.axis_index("zh")
+    state = before = jnp.zeros((PAIR, STATE), f32)
+    for k in range(got_ref.shape[0] - 1):
+        more, step = take_state(got_ref, k, 0)
+        state = state * factor(step) + more
+        before = jnp.where(k < here, state, before)
+    state = before * factor(logs_ref[...]) + state_ref[...]
+    start = rows_ref.shape[1] - PAIR - TAIL
+    for k in range(rows_ref.shape[0]):
+        out_ref[k] = state.astype(bf16)
+        if k + 1 < rows_ref.shape[0]:
+            more, step = take_state(rows_ref, k, start)
+            state = state * factor(step) + more
 
 
 def gate_kernel(pre_ref, query_ref, cum_ref, inc_ref, gate_ref, gain_ref, w_ref, out_ref, w_room, sem):
@@ -176,26 +229,30 @@
         copies_ref[k] = normed
 
 
-def mlp_kernel(rows_ref, w_ref, out_ref, w_vmem, sems):
-    halves, depth, both = w_ref.shape
-    units = both // 2
+def mlp_kernel(rows_ref, w_ref, out_ref, w_room, sems):
+    halves, shards, inner, slabs, each_depth, lanes = w_ref.shape
     pieces = sems.shape[1]
-    size = depth // pieces
+    take = shards // pieces
+    size = take * inner * each_depth
     copies = []
     for j in range(pieces):
         for k in range(halves):
-            copy = pltpu.make_async_copy(
-                w_ref.at[k, pl.ds(j * size, size)], w_vmem.at[k, pl.ds(j * size, size)], sems.at[k, j]
-            )
+            part = pl.ds(j * take, take)
+            copy = pltpu.make_async_copy(w_ref.at[k, part], w_room.at[k, part], sems.at[k, j])
             copy.start()
             copies.append(copy)
-    count, each, _ = rows_ref.shape
+
+    def piece(k, j, first):
+        parts = [w_room[k, j * take : (j + 1) * take, :, n, :, :] for n in (first, first + 1)]
+        return jnp.concatenate([p.reshape(size, lanes) for p in parts], axis=1)
+
+    count, each, depth = rows_ref.shape
     rows = rows_ref[...].reshape(count * each, depth)
     lifted = [None] * halves
     for j in range(pieces):
         for k in range(halves):
             copies[j * halves + k].wait()
-            part = dot(rows[:, j * size : (j + 1) * size], w_vmem[k, j * size : (j + 1) * size, 0:units], ((1,), (0,)))
+            part = dot(rows[:, j * size : (j + 1) * size], piece(k, j, 0), ((1,), (0,)))
             lifted[k] = part if lifted[k] is None else lifted[k] + part
     hidden = []
     for k in range(halves):
@@ -204,7 +261,7 @@
     for j in range(pieces):
         total = None
         for k in range(halves):
-            part = dot(hidden[k], w_vmem[k, j * size : (j + 1) * size, units:both], ((1,), (1,)))
+            part = dot(hidden[k], piece(k, j, slabs // 2), ((1,), (1,)))
             total = part if total is None else total + part
         out_ref[:, :, j * size : (j + 1) * size] = total.astype(bf16).reshape(count, each, size)
 
@@ -235,41 +292,32 @@
     widening_matrix,
     narrowing_matrix,
 ):
-    ny = lax.axis_size("y")
-    nsp = lax.axis_size("z") * ny
+    ny, nzl, nzh = (lax.axis_size(name) for name in ("y", "zl", "zh"))
+    nsp = nzh * nzl * ny
     ntp = lax.axis_size("x") * lax.axis_size("c")
     nrows = ny * lax.axis_size("x")
-    width = skip_stream_entering.shape[1]
-    own_count = skip_stream_entering.shape[0]
-
+    own_count, width = skip_stream_entering.shape
     depth, units = widening_matrix.shape
-    slim = units // ny
-    rim, mine = pl.pallas_call(
+    shard = 2 * depth * units // ny // STATE
+
+    rim = pl.pallas_call(
         first_kernel,
         grid=(1,),
-        out_shape=[shape((RIM, WIDTH + 2 * STATE), bf16), shape((ny, depth, 2 * slim), bf16)],
-        in_specs=[pl.BlockSpec((RIM, n), lambda i: (BLOCK // RIM - 1, 0)) for n in (WIDTH, STATE, STATE)]
-        + [pl.BlockSpec((depth, units), lambda i: (0, 0))] * 2,
-        out_specs=[
-            pl.BlockSpec((RIM, WIDTH + 2 * STATE), lambda i: (0, 0)),
-            pl.BlockSpec((ny, depth, 2 * slim), lambda i: (0, 0, 0)),
-        ],
+        out_shape=shape((RIM, WIDTH + 2 * STATE), bf16),
+        in_specs=[pl.BlockSpec((RIM, n), lambda i: (BLOCK // RIM - 1, 0)) for n in (WIDTH, STATE, STATE)],
+        out_specs=pl.BlockSpec((RIM, WIDTH + 2 * STATE), lambda i: (0, 0)),
         interpret=INTERPRET,
-    )(content_signal_matrix, writer_signal_matrix, reader_signal_matrix, widening_matrix, narrowing_matrix.T)
+    )(content_signal_matrix, writer_signal_matrix, reader_signal_matrix)
     rim = lax.ppermute(rim, SP, [(k, k + 1) for k in range(nsp - 1)])
-    parts = exchange(mine, "y").reshape(ny * depth, 2 * slim)
-    weights = lax.all_gather(parts, ("c", "z"), axis=0, tiled=True).reshape(-1, width, 2 * slim)
-
-    rim, parts = lax.optimization_barrier((rim, parts))
     pre, query, cum, send = call(
         local_kernel,
         [
             shape((BLOCK, WIDTH), f32),
             shape((BLOCK, STATE), bf16),
             shape((HEADS, BLOCK), f32),
-            shape((nsp, 16, STATE), bf16),
+            shape((ny, shard + PAIR + TAIL, STATE), bf16),
         ],
-        [VMEM] * 9 + [SMEM] * 2,
+        [VMEM] * 11 + [SMEM] * 2,
         [pltpu.VMEM((RIM + BLOCK, n), f32) for n in (WIDTH, STATE, STATE)],
     )(
         content_signal_matrix,
@@ -281,12 +329,28 @@
         reader_filter_coefs,
         interval_before_softplus,
         extra_log_shrink,
+        widening_matrix,
+        narrowing_matrix.T,
         log_forget_speed,
         skip_path_factor,
     )
-    got = exchange(send, SP)
-    before = call(scan_kernel, shape((nsp, 8, STATE), bf16), [VMEM])(near(got))
-    incoming = exchange(before, SP)
+    rows = near(exchange(send, "y"))
+    parts, send = call(
+        row_kernel,
+        [jax.ShapeDtypeStruct((ny, shard, STATE), bf16), shape((nzl, PAIR + TAIL, STATE), bf16)],
+        [VMEM],
+    )(rows)
+    weights = lax.all_gather(parts.reshape(ny * shard, STATE), ("c", "zh", "zl"), axis=0, tiled=True)
+    weights = weights.reshape(-1, nzh * nzl, ny, shard // depth, depth, STATE)
+    got = near(exchange(send, "zl"))
+    send, state, logs = call(
+        near_kernel,
+        [shape((nzh, PAIR + TAIL, STATE), bf16), shape((PAIR, STATE), f32), shape((2, STATE), f32)],
+        [VMEM],
+    )(got)
+    got = near(exchange(send, "zh"))
+    before = call(far_kernel, shape((ny, PAIR, STATE), bf16), [VMEM] * 4)(got, near(state), near(logs), rows)
+    incoming = exchange(before, "y")
     mixed = call(
         gate_kernel,
         shape((ntp, own_count, width), bf16),
@@ -319,7 +383,7 @@
 
 
 def solution(mesh):
-    torus = Mesh(mesh.devices.reshape(16, 4, 4, 2), ("z", "y", "x", "c"))
+    torus = Mesh(mesh.devices.reshape(4, 4, 4, 4, 2), SP + TP)
     placed = (
         P(SP + TP, None),
         P(SP, TP),

time: 160 us -> 147 us (0.919)
  blocking collectives: 129 us -> 113 us
  starting transfers between devices: 2.19 us -> 4.01 us
    all_to_all x6 -> x7, blocking collectives: 129 us -> 113 us  [exchange(): return lax.all_to_all(value, axes, split_axis=0, concat_axis=0, tiled=True)]
    ppermute x1, starting transfers between devices: 2.19 us -> 4.01 us  [per_device(): rim = lax.ppermute(rim, SP, [(k, k + 1) for k in range(nsp - 1)])]
  transfers between devices with their start and end apart: 2 -> 2, of which waited for: 1 -> 1; matrix products, arithmetic and copies ran while one was open for 0% -> 0% of each run, Pallas kernels for 5% -> 3%
where the time goes in v3:
time: 147 us; the launch traced here: 145 us
  blocking collectives  113 us (77%)
  between operations  13.4 us (9%)
  Pallas kernels  13.3 us (9%)
  starting transfers between devices  4.01 us (3%)
    all_to_all x7, blocking collectives, exchange(): return lax.all_to_all(value, axes, split_axis=0, concat_axis=0, tiled=True)  113 us
    ppermute x1, starting transfers between devices, per_device(): rim = lax.ppermute(rim, SP, [(k, k + 1) for k in range(nsp - 1)])  4.01 us
    pallas_call x1, Pallas kernels, per_device(): call(mlp_kernel, shape((nrows, own_count, width), bf16), [VMEM, HBM], [pl...  3.58 us
    pallas_call x1, Pallas kernels, per_device(): call(gate_kernel, shape((ntp, own_count, width), bf16), [VMEM] * 6 + [HBM...  3.38 us
    pallas_call x1, Pallas kernels, per_device(): call(local_kernel, [shape((BLOCK, WIDTH), f32), shape((BLOCK, STATE), bf1...  2.99 us
  transfers between devices with their start and end apart: 2, of which 1 were waited for; matrix products, arithmetic and copies ran while one was open for 0% of the time, Pallas kernels for 3%

profile of v3, /device:TPU:1, one launch (start us, length us, event | category | flops | bytes accessed | tf_op | source)
XLA Modules:
  0.0 145.0 jit_solution(11297830343675554365)
XLA Ops:
  6.5 0.0 all-gather.2.cloned.1.call-start
  6.5 0.7 shard_map.163
  7.3 4.0 %collective-permute-start = (bf16[8,768]{1,0:T(8,128)(2,1)S(1)}, bf16[8,768]{1,0:T(8,128)(2,1)S(1)}, u32[]{:S(2)}, u32[]{:S(2)}) collective-permute-start(bf16[8,768]{1,0:T(8,128)(2,1)S(1)} %shard_map.163), channel_id=1, source_target_pairs={{0,8},{8,16},{16,24},{24,32},{32,40},{40,48},{48,56},{56,64},{64,7... | collective-permute-start | bytes 36872 | tf_op jit(solution)/shard_map/ppermute | solution.py:311
  11.3 0.8 collective-permute-done.rim_ref
  12.1 3.0 %shard_map.164 = (f32[128,512]{1,0:T(8,128)S(1)}, bf16[128,128]{1,0:T(8,128)(2,1)S(1)}, f32[8,128]{1,0:T(8,128)S(1)}, bf16[4,272,128]{2,1,0:T(8,128)(2,1)S(1)}) custom-call(bf16[128,512]{1,0:T(8,128)(2,1)} %x_ref.3, bf16[128,128]{1,0:T(8,128)(2,1)} %b_ref.3, bf16[128,128]{1,0:T(8,128)(2,1)} %c_ref.3, bf16[8,768]{1,0:T(8,128)(2,1)S(1)} %collective-permute-done.rim_ref, ...), custom_call_target="tpu_custom_call" | custom-call | tf_op jit(solution)/shard_map/pallas_call | solution.py:312
  15.1 10.0 %all_to_all.35.got_ref.rows_ref = bf16[4,272,128]{2,1,0:T(8,128)(2,1)S(1)} all-to-all(bf16[4,272,128]{2,1,0:T(8,128)(2,1)S(1)} %get-tuple-element.19), channel_id=1, replica_groups=mesh['zh'=4,'zl'=4,'y'=4,'x'=4,'c'=2] {'y'}, dimensions={0} | all-to-all | bytes 557056 | tf_op jit(solution)/shard_map/all_to_all | solution.py:52
  25.1 0.7 shard_map.165
  25.7 0.0 all-gather.2.cloned.1.call-update
  25.8 11.5 %all_to_all.36.got_ref = bf16[4,144,128]{2,1,0:T(8,128)(2,1)S(1)} all-to-all(bf16[4,144,128]{2,1,0:T(8,128)(2,1)S(1)} %get-tuple-element.20), channel_id=1, replica_groups=mesh['zh'=4,'zl'=4,'y'=4,'x'=4,'c'=2] {'zl'}, dimensions={0} | all-to-all | bytes 294912 | tf_op jit(solution)/shard_map/all_to_all | solution.py:52
  37.3 0.1 shard_map.166
  37.4 27.4 %all_to_all.37.got_ref = bf16[4,144,128]{2,1,0:T(8,128)(2,1)S(1)} all-to-all(bf16[4,144,128]{2,1,0:T(8,128)(2,1)S(1)} %get-tuple-element.21), channel_id=1, replica_groups=mesh['zh'=4,'zl'=4,'y'=4,'x'=4,'c'=2] {'zh'}, dimensions={0} | all-to-all | bytes 294912 | tf_op jit(solution)/shard_map/all_to_all | solution.py:52
  64.8 0.1 shard_map.167
  64.9 7.2 %all_to_all.38.inc_ref = bf16[4,128,128]{2,1,0:T(8,128)(2,1)S(1)} all-to-all(bf16[4,128,128]{2,1,0:T(8,128)(2,1)S(1)} %shard_map.167), channel_id=1, replica_groups=mesh['zh'=4,'zl'=4,'y'=4,'x'=4,'c'=2] {'y'}, dimensions={0} | all-to-all | bytes 262144 | tf_op jit(solution)/shard_map/all_to_all | solution.py:52
  72.1 3.4 %shard_map.168 = bf16[8,16,2048]{2,1,0:T(8,128)(2,1)S(1)} custom-call(f32[128,512]{1,0:T(8,128)S(1)} %get-tuple-element.16.pre_ref, bf16[128,128]{1,0:T(8,128)(2,1)S(1)} %get-tuple-element.17.query_ref, f32[8,128]{1,0:T(8,128)S(1)} %get-tuple-element.18.cum_ref, bf16[4,128,128]{2,1,0:T(8,128)(2,1)S(1)} %all_to_all.38.inc_ref, bf16[128,512]{1,0:T(8,128)(2,1)} %gate_ref.1, ...), custom_call_target="tpu_custom_call" | custom-call | tf_op jit(solution)/shard_map/pallas_call | solution.py:354
  75.5 20.2 %all_to_all.39.got_ref = bf16[8,16,2048]{2,1,0:T(8,128)(2,1)S(1)} all-to-all(bf16[8,16,2048]{2,1,0:T(8,128)(2,1)S(1)} %shard_map.168), channel_id=1, replica_groups=mesh['zh'=4,'zl'=4,'y'=4,'x'=4,'c'=2] {'x','c'}, dimensions={0} | all-to-all | bytes 1048576 | tf_op jit(solution)/shard_map/all_to_all | solution.py:52
  95.7 1.1 shard_map.169
  96.8 18.7 %all_to_all.40.rows_ref = bf16[16,16,2048]{2,1,0:T(8,128)(2,1)S(1)} all-to-all(bf16[16,16,2048]{2,1,0:T(8,128)(2,1)S(1)} %get-tuple-element.24), channel_id=1, replica_groups=mesh['zh'=4,'zl'=4,'y'=4,'x'=4,'c'=2] {'y','x'}, dimensions={0} | all-to-all | bytes 2097152 | tf_op jit(solution)/shard_map/all_to_all | solution.py:52
  115.5 0.0 all-gather.2.cloned.1.call-done
  115.5 3.6 %shard_map.170 = bf16[16,16,2048]{2,1,0:T(8,128)(2,1)S(1)} custom-call(bf16[16,16,2048]{2,1,0:T(8,128)(2,1)S(1)} %all_to_all.40.rows_ref, bf16[2,16,4,4,32,128]{5,4,3,2,1,0:T(8,128)(2,1)} %bitcast.5), custom_call_target="tpu_custom_call" | custom-call | tf_op jit(solution)/shard_map/pallas_call | solution.py:375
  119.1 18.3 %all_to_all.41.got_ref = bf16[16,16,2048]{2,1,0:T(8,128)(2,1)S(1)} all-to-all(bf16[16,16,2048]{2,1,0:T(8,128)(2,1)S(1)} %shard_map.170), channel_id=1, replica_groups=mesh['zh'=4,'zl'=4,'y'=4,'x'=4,'c'=2] {'y','x'}, dimensions={0} | all-to-all | bytes 2097152 | tf_op jit(solution)/shard_map/all_to_all | solution.py:52
  137.4 0.8 shard_map.171
Async XLA Ops:
  6.5 108.9 %all-gather.2.cloned.1.call-start = ((), (), s32[]{:S(2)}) async-start(), calls=%async_computation.7 | async-start | bytes 4325376 | tf_op jit(solution)/shard_map/all_gather | solution.py:343
  7.3 4.8 %collective-permute-start = (bf16[8,768]{1,0:T(8,128)(2,1)S(1)}, bf16[8,768]{1,0:T(8,128)(2,1)S(1)}, u32[]{:S(2)}, u32[]{:S(2)}) collective-permute-start(bf16[8,768]{1,0:T(8,128)(2,1)S(1)} %shard_map.163), channel_id=1, source_target_pairs={{0,8},{8,16},{16,24},{24,32},{32,40},{40,48},{48,56},{56,64},{64,7... | collective-permute-start | bytes 36872 | tf_op jit(solution)/shard_map/ppermute | solution.py:311
Sparse Core Ops, SparseCore 0:
  25.9 82.6 all-gather.1

commit v4 on v3

--- a/solution.py
+++ b/solution.py
@@ -1,3 +1,5 @@
+import functools
+
 import jax
 import jax.numpy as jnp
 from jax import lax
@@ -12,13 +14,14 @@
 BLOCK = 128
 WIDTH = HEADS * HEAD_DIM
 RIM = 8
-PAIR = 2 * HEAD_DIM
 TAIL = 16
+NEAR = ("zl", "y")
 SP = ("zh", "zl", "y")
 TP = ("x", "c")
 ROWS = ("y", "x")
 EPSILON = 1e-05
 INTERPRET = False
+ROOM = pltpu.CompilerParams(vmem_limit_bytes=16 << 20)
 
 f32 = jnp.float32
 bf16 = jnp.bfloat16
@@ -80,26 +83,20 @@
     return silu(total)
 
 
-def put_state(ref, place, start, state, logs):
-    ref[place, start : start + PAIR, :] = state.astype(bf16)
+def put_state(ref, place, start, state, log):
+    count = state.shape[0]
+    ref[place, start : start + count, :] = state.astype(bf16)
     row = lax.broadcasted_iota(jnp.int32, (TAIL, STATE), 0)
-    tail = jnp.zeros((TAIL, STATE), f32)
-    for h in range(2):
-        whole = jnp.broadcast_to(logs[h : h + 1, :], (TAIL, STATE))
-        high = whole.astype(bf16).astype(f32)
-        tail = jnp.where(row == 2 * h, high, jnp.where(row == 2 * h + 1, whole - high, tail))
-    ref[place, start + PAIR : start + PAIR + TAIL, :] = tail.astype(bf16)
+    whole = jnp.broadcast_to(log, (TAIL, STATE))
+    high = whole.astype(bf16).astype(f32)
+    tail = jnp.where(row == 0, high, jnp.where(row == 1, whole - high, 0.0))
+    ref[place, start + count : start + count + TAIL, :] = tail.astype(bf16)
 
 
 def take_state(ref, place, start):
-    state = ref[place, start : start + PAIR, :].astype(f32)
-    tail = ref[place, start + PAIR : start + PAIR + TAIL, :].astype(f32)
-    return state, jnp.concatenate([tail[2 * h : 2 * h + 1, :] + tail[2 * h + 1 : 2 * h + 2, :] for h in range(2)], axis=0)
-
-
-def factor(logs):
-    grown = jnp.exp(logs)
-    return jnp.concatenate([jnp.broadcast_to(grown[h : h + 1, :], (HEAD_DIM, STATE)) for h in range(2)], axis=0)
+    end = ref.shape[1] - TAIL
+    tail = ref[place, end : end + TAIL, :].astype(f32)
+    return ref[place, start:end, :].astype(f32), tail[0:1, :] + tail[1:2, :]
 
 
 def first_kernel(x_ref, b_ref, c_ref, rim_ref):
@@ -109,9 +106,11 @@
 
 
 def local_kernel(
-    x_ref, b_ref, c_ref, rim_ref, xt_ref, bt_ref, ct_ref, dt_ref, shrink_ref, up_ref, down_ref, speed_ref, skip_ref,
-    pre_ref, query_ref, cum_ref, send_ref, x_room, b_room, c_room,
+    slices, x_ref, b_ref, c_ref, rim_ref, xt_ref, bt_ref, ct_ref, dt_ref, shrink_ref, up_ref, down_ref, speed_ref, skip_ref, w_ref,
+    pre_ref, query_ref, cum_ref, send_ref, w_out, x_room, b_room, c_room, sem,
 ):
+    copy = pltpu.make_async_copy(w_ref, w_out, sem)
+    copy.start()
     values = convolve(x_ref, rim_ref[:, 0:WIDTH], xt_ref, x_room)
     keys = convolve(b_ref, rim_ref[:, WIDTH : WIDTH + STATE], bt_ref, b_room).astype(bf16)
     query = convolve(c_ref, rim_ref[:, WIDTH + STATE : WIDTH + 2 * STATE], ct_ref, c_room).astype(bf16)
@@ -135,13 +134,15 @@
     state = dot(weighted, keys, ((0,), (0,)))
     pieces = send_ref.shape[0]
     depth, units = up_ref.shape
-    slabs = units // pieces // STATE
-    for k in range(pieces):
-        for j in range(slabs):
-            lanes = slice((k * slabs + j) * STATE, (k * slabs + j + 1) * STATE)
-            send_ref[k, j * depth : (j + 1) * depth, :] = up_ref[:, lanes]
-            send_ref[k, (slabs + j) * depth : (slabs + j + 1) * depth, :] = down_ref[:, lanes]
-        put_state(send_ref, k, 2 * slabs * depth, state[k * PAIR : (k + 1) * PAIR, :], last[2 * k : 2 * k + 2, :])
+    count = WIDTH // pieces
+    slabs = units // slices // STATE
+    for place in range(pieces):
+        slab, k = divmod(place, slices)
+        source = up_ref if slab < slabs else down_ref
+        first_lane = (k * slabs + slab % slabs) * STATE
+        send_ref[place, 0:depth, :] = source[:, first_lane : first_lane + STATE]
+        h = place * count // HEAD_DIM
+        put_state(send_ref, place, depth, state[place * count : (place + 1) * count, :], last[h : h + 1, :])
     scores = dot(query, keys, ((1,), (1,)))
     columns = spread(cum, BLOCK)
     later = lax.broadcasted_iota(jnp.int32, (BLOCK, BLOCK), 0)
@@ -160,59 +161,44 @@
         within = jnp.where(first, parts[0], parts[1])
         skip = jnp.where(first, skip_ref[2 * pair], skip_ref[2 * pair + 1])
         pre_ref[:, lanes] = within + skip * two
-
-
-def row_kernel(got_ref, shard_ref, send_ref):
+    copy.wait()
+
+
+def near_kernel(got_ref, shard_ref, send_ref):
     start = shard_ref.shape[1]
-    state = logs = None
+    state = log = None
     for k in range(got_ref.shape[0]):
         shard_ref[k] = got_ref[k, 0:start, :]
         more, step = take_state(got_ref, k, start)
-        state, logs = (more, step) if state is None else (state * factor(step) + more, logs + step)
+        state, log = (more, step) if state is None else (state * jnp.exp(step) + more, log + step)
     for k in range(send_ref.shape[0]):
-        put_state(send_ref, k, 0, state, logs)
-
-
-def near_kernel(got_ref, send_ref, state_ref, logs_ref):
-    here = lax.axis_index("zl")
-    state = before = jnp.zeros((PAIR, STATE), f32)
-    logs = passed = jnp.zeros((2, STATE), f32)
-    for k in range(got_ref.shape[0]):
-        more, step = take_state(got_ref, k, 0)
-        state, logs = state * factor(step) + more, logs + step
-        before, passed = jnp.where(k < here, state, before), jnp.where(k < here, logs, passed)
-    state_ref[...] = before
-    logs_ref[...] = passed
-    for k in range(send_ref.shape[0]):
-        put_state(send_ref, k, 0, state, logs)
-
-
-def far_kernel(got_ref, state_ref, logs_ref, rows_ref, out_ref):
+        put_state(send_ref, k, 0, state, log)
+
+
+def far_kernel(got_ref, near_ref, out_ref):
     here = lax.axis_index("zh")
-    state = before = jnp.zeros((PAIR, STATE), f32)
+    count = out_ref.shape[1]
+    state = before = jnp.zeros((count, STATE), f32)
     for k in range(got_ref.shape[0] - 1):
         more, step = take_state(got_ref, k, 0)
-        state = state * factor(step) + more
+        state = state * jnp.exp(step) + more
         before = jnp.where(k < here, state, before)
-    state = before * factor(logs_ref[...]) + state_ref[...]
-    start = rows_ref.shape[1] - PAIR - TAIL
-    for k in range(rows_ref.shape[0]):
+    state = before
+    start = near_ref.shape[1] - count - TAIL
+    for k in range(near_ref.shape[0]):
         out_ref[k] = state.astype(bf16)
-        if k + 1 < rows_ref.shape[0]:
-            more, step = take_state(rows_ref, k, start)
-            state = state * factor(step) + more
-
-
-def gate_kernel(pre_ref, query_ref, cum_ref, inc_ref, gate_ref, gain_ref, w_ref, out_ref, w_room, sem):
-    copy = pltpu.make_async_copy(w_ref, w_room, sem)
-    copy.start()
+        if k + 1 < near_ref.shape[0]:
+            more, step = take_state(near_ref, k, start)
+            state = state * jnp.exp(step) + more
+
+
+def gate_kernel(pre_ref, query_ref, cum_ref, inc_ref, gate_ref, gain_ref, w_ref, out_ref):
     inc = inc_ref[...].reshape(WIDTH, STATE)
     arriving = dot(query_ref[...], inc, ((1,), (1,))) * spread(jnp.exp(cum_ref[...]), HEAD_DIM)
     gated = (pre_ref[...] + arriving) * silu(gate_ref[...].astype(f32))
     scale = lax.rsqrt(jnp.mean(gated * gated, axis=-1, keepdims=True) + EPSILON)
     heads_out = (gated * scale * gain_ref[...]).astype(bf16)
-    copy.wait()
-    out = dot(heads_out, w_room[...], ((1,), (0,))).astype(bf16)
+    out = dot(heads_out, w_ref[...], ((1,), (0,))).astype(bf16)
     out_ref[...] = out.reshape(out_ref.shape)
 
 
@@ -230,21 +216,16 @@
 
 
 def mlp_kernel(rows_ref, w_ref, out_ref, w_room, sems):
-    halves, shards, inner, slabs, each_depth, lanes = w_ref.shape
-    pieces = sems.shape[1]
-    take = shards // pieces
-    size = take * inner * each_depth
+    halves, pieces, slabs, size, lanes = w_ref.shape
     copies = []
     for j in range(pieces):
         for k in range(halves):
-            part = pl.ds(j * take, take)
-            copy = pltpu.make_async_copy(w_ref.at[k, part], w_room.at[k, part], sems.at[k, j])
+            copy = pltpu.make_async_copy(w_ref.at[k, j], w_room.at[k, j], sems.at[k, j])
             copy.start()
             copies.append(copy)
 
     def piece(k, j, first):
-        parts = [w_room[k, j * take : (j + 1) * take, :, n, :, :] for n in (first, first + 1)]
-        return jnp.concatenate([p.reshape(size, lanes) for p in parts], axis=1)
+        return jnp.concatenate([w_room[k, j, n] for n in range(first, first + slabs // 2)], axis=1)
 
     count, each, depth = rows_ref.shape
     rows = rows_ref[...].reshape(count * each, depth)
@@ -298,7 +279,8 @@
     nrows = ny * lax.axis_size("x")
     own_count, width = skip_stream_entering.shape
     depth, units = widening_matrix.shape
-    shard = 2 * depth * units // ny // STATE
+    pieces = nzl * ny
+    count = WIDTH // pieces
 
     rim = pl.pallas_call(
         first_kernel,
@@ -309,16 +291,17 @@
         interpret=INTERPRET,
     )(content_signal_matrix, writer_signal_matrix, reader_signal_matrix)
     rim = lax.ppermute(rim, SP, [(k, k + 1) for k in range(nsp - 1)])
-    pre, query, cum, send = call(
-        local_kernel,
+    pre, query, cum, send, projection = call(
+        functools.partial(local_kernel, ny),
         [
             shape((BLOCK, WIDTH), f32),
             shape((BLOCK, STATE), bf16),
             shape((HEADS, BLOCK), f32),
-            shape((ny, shard + PAIR + TAIL, STATE), bf16),
+            shape((pieces, depth + count + TAIL, STATE), bf16),
+            shape(blend_result_matrix.shape, bf16),
         ],
-        [VMEM] * 11 + [SMEM] * 2,
-        [pltpu.VMEM((RIM + BLOCK, n), f32) for n in (WIDTH, STATE, STATE)],
+        [VMEM] * 11 + [SMEM] * 2 + [HBM],
+        [pltpu.VMEM((RIM + BLOCK, n), f32) for n in (WIDTH, STATE, STATE)] + [pltpu.SemaphoreType.DMA(())],
     )(
         content_signal_matrix,
         writer_signal_matrix,
@@ -333,29 +316,25 @@
         narrowing_matrix.T,
         log_forget_speed,
         skip_path_factor,
-    )
-    rows = near(exchange(send, "y"))
+        blend_result_matrix,
+    )
+    got = near(exchange(send, NEAR))
     parts, send = call(
-        row_kernel,
-        [jax.ShapeDtypeStruct((ny, shard, STATE), bf16), shape((nzl, PAIR + TAIL, STATE), bf16)],
+        near_kernel,
+        [jax.ShapeDtypeStruct((pieces, depth, STATE), bf16), shape((nzh, count + TAIL, STATE), bf16)],
         [VMEM],
-    )(rows)
-    weights = lax.all_gather(parts.reshape(ny * shard, STATE), ("c", "zh", "zl"), axis=0, tiled=True)
-    weights = weights.reshape(-1, nzh * nzl, ny, shard // depth, depth, STATE)
-    got = near(exchange(send, "zl"))
-    send, state, logs = call(
-        near_kernel,
-        [shape((nzh, PAIR + TAIL, STATE), bf16), shape((PAIR, STATE), f32), shape((2, STATE), f32)],
-        [VMEM],
+        compiler_params=ROOM,
     )(got)
-    got = near(exchange(send, "zh"))
-    before = call(far_kernel, shape((ny, PAIR, STATE), bf16), [VMEM] * 4)(got, near(state), near(logs), rows)
-    incoming = exchange(before, "y")
+    weights = lax.all_gather(parts.reshape(pieces * depth, STATE), ("c", "zh", "zl"), axis=0, tiled=True)
+    weights = weights.reshape(-1, nzh, nzl, pieces * depth, STATE)
+    far = near(exchange(send, "zh"))
+    before = call(far_kernel, shape((pieces, count, STATE), bf16), [VMEM] * 2, compiler_params=ROOM)(far, got)
+    incoming = exchange(before, NEAR)
     mixed = call(
         gate_kernel,
         shape((ntp, own_count, width), bf16),
-        [VMEM] * 6 + [HBM],
-        [pltpu.VMEM(blend_result_matrix.shape, bf16), pltpu.SemaphoreType.DMA(())],
+        [VMEM] * 7,
+        compiler_params=ROOM,
     )(
         near(pre),
         near(query),
@@ -363,7 +342,7 @@
         near(incoming),
         multiplier_signal,
         cluster_scaling_vector.reshape(1, -1),
-        blend_result_matrix,
+        near(projection),
     )
     mixed = exchange(mixed, TP)
     own, copies = call(
@@ -376,7 +355,7 @@
         mlp_kernel,
         shape((nrows, own_count, width), bf16),
         [VMEM, HBM],
-        [pltpu.VMEM(weights.shape, bf16), pltpu.SemaphoreType.DMA((weights.shape[0], 4))],
+        [pltpu.VMEM(weights.shape, bf16), pltpu.SemaphoreType.DMA(weights.shape[:2])],
     )(near(rows), weights)
     out = exchange(out, ROWS)
     return call(final_kernel, jax.ShapeDtypeStruct((own_count, width), bf16), [VMEM] * 2)(near(out), near(own))

time: 147 us -> 146 us (level)
  Pallas kernels: 13.3 us -> 10.8 us
  blocking collectives: 113 us -> 115 us
  waiting for transfers between devices: 0.83 us -> 2.47 us
    pallas_call x5 -> x4, Pallas kernels: 7.14 us -> 4.63 us  [the longest x1 3.01 us: per_device(): call(functools.partial(local_kernel, ny), [shape((BLOCK, WIDTH), f32), sh...]
    all_gather x1, waiting for transfers between devices: 0.01 us -> 1.64 us  [per_device(): lax.all_gather(parts.reshape(pieces * depth, STATE), ('c', 'zh', 'zl'), a...]
    all_to_all x7 -> x6, blocking collectives: 113 us -> 115 us  [exchange(): return lax.all_to_all(value, axes, split_axis=0, concat_axis=0, tiled=True)]
  transfers between devices with their start and end apart: 2 -> 2, of which waited for: 1 -> 2; matrix products, arithmetic and copies ran while one was open for 0% -> 0% of each run, Pallas kernels for 3% -> 1%
where the time goes in v4:
time: 146 us; the launch traced here: 145 us
  blocking collectives  115 us (79%)
  between operations  13.4 us (9%)
  Pallas kernels  10.8 us (7%)
  starting transfers between devices  4.01 us (3%)
  waiting for transfers between devices  2.47 us (2%)
    all_to_all x6, blocking collectives, exchange(): return lax.all_to_all(value, axes, split_axis=0, concat_axis=0, tiled=True)  115 us
    ppermute x1, starting transfers between devices, per_device(): rim = lax.ppermute(rim, SP, [(k, k + 1) for k in range(nsp - 1)])  4.01 us
    pallas_call x1, Pallas kernels, per_device(): call(mlp_kernel, shape((nrows, own_count, width), bf16), [VMEM, HBM], [pl...  3.58 us
    pallas_call x1, Pallas kernels, per_device(): call(functools.partial(local_kernel, ny), [shape((BLOCK, WIDTH), f32), sh...  3.01 us
  transfers between devices with their start and end apart: 2, of which 2 were waited for; matrix products, arithmetic and copies ran while one was open for 0% of the time, Pallas kernels for 1%

profile of v4, /device:TPU:1, one launch (start us, length us, event | category | flops | bytes accessed | tf_op | source)
XLA Modules:
  0.0 145.5 jit_solution(6021387036499769048)
XLA Ops:
  6.5 0.0 all-gather.2.cloned.1.call-start
  6.5 0.7 shard_map.163
  7.3 4.0 %collective-permute-start = (bf16[8,768]{1,0:T(8,128)(2,1)S(1)}, bf16[8,768]{1,0:T(8,128)(2,1)S(1)}, u32[]{:S(2)}, u32[]{:S(2)}) collective-permute-start(bf16[8,768]{1,0:T(8,128)(2,1)S(1)} %shard_map.163), channel_id=1, source_target_pairs={{0,8},{8,16},{16,24},{24,32},{32,40},{40,48},{48,56},{56,64},{64,7... | collective-permute-start | bytes 36872 | tf_op jit(solution)/shard_map/ppermute | solution.py:293
  11.3 0.8 collective-permute-done.rim_ref
  12.1 0.0 copy-start
  12.1 0.0 copy-start.1
  12.1 3.0 %shard_map.164 = (f32[128,512]{1,0:T(8,128)S(1)}, bf16[128,128]{1,0:T(8,128)(2,1)S(1)}, f32[8,128]{1,0:T(8,128)S(1)}, bf16[16,80,128]{2,1,0:T(8,128)(2,1)S(1)}, bf16[512,2048]{1,0:T(8,128)(2,1)S(1)}) custom-call(bf16[128,512]{1,0:T(8,128)(2,1)} %x_ref.3, bf16[128,128]{1,0:T(8,128)(2,1)} %b_ref.3, bf16[128,128]{1,0:T(8,128)(2,1)} %c_ref.3, ...), custom_call_target="tpu_custom_call" | custom-call | tf_op jit(solution)/shard_map/pallas_call | solution.py:294
  15.1 18.9 %all_to_all.30.got_ref.near_ref = bf16[16,80,128]{2,1,0:T(8,128)(2,1)S(1)} all-to-all(bf16[16,80,128]{2,1,0:T(8,128)(2,1)S(1)} %get-tuple-element.17), channel_id=1, replica_groups=mesh['zh'=4,'zl'=4,'y'=4,'x'=4,'c'=2] {'zl','y'}, dimensions={0} | all-to-all | bytes 655360 | tf_op jit(solution)/shard_map/all_to_all | solution.py:55
  34.0 0.7 shard_map.165
  34.7 0.0 all-gather.2.cloned.1.call-update
  34.7 23.5 %all_to_all.31.got_ref = bf16[4,48,128]{2,1,0:T(8,128)(2,1)S(1)} all-to-all(bf16[4,48,128]{2,1,0:T(8,128)(2,1)S(1)} %get-tuple-element.18), channel_id=1, replica_groups=mesh['zh'=4,'zl'=4,'y'=4,'x'=4,'c'=2] {'zh'}, dimensions={0} | all-to-all | bytes 98304 | tf_op jit(solution)/shard_map/all_to_all | solution.py:55
  58.2 0.1 shard_map.166
  58.2 13.3 %all_to_all.32.inc_ref = bf16[16,32,128]{2,1,0:T(8,128)(2,1)S(1)} all-to-all(bf16[16,32,128]{2,1,0:T(8,128)(2,1)S(1)} %shard_map.166), channel_id=1, replica_groups=mesh['zh'=4,'zl'=4,'y'=4,'x'=4,'c'=2] {'zl','y'}, dimensions={0} | all-to-all | bytes 262144 | tf_op jit(solution)/shard_map/all_to_all | solution.py:55
  71.5 0.0 copy-done
  71.5 0.0 copy-done.1
  71.5 0.9 shard_map.167
  72.4 17.5 %all_to_all.33.got_ref = bf16[8,16,2048]{2,1,0:T(8,128)(2,1)S(1)} all-to-all(bf16[8,16,2048]{2,1,0:T(8,128)(2,1)S(1)} %shard_map.167), channel_id=1, replica_groups=mesh['zh'=4,'zl'=4,'y'=4,'x'=4,'c'=2] {'x','c'}, dimensions={0} | all-to-all | bytes 1048576 | tf_op jit(solution)/shard_map/all_to_all | solution.py:55
  89.9 1.1 shard_map.168
  91.0 18.8 %all_to_all.34.rows_ref = bf16[16,16,2048]{2,1,0:T(8,128)(2,1)S(1)} all-to-all(bf16[16,16,2048]{2,1,0:T(8,128)(2,1)S(1)} %get-tuple-element.20), channel_id=1, replica_groups=mesh['zh'=4,'zl'=4,'y'=4,'x'=4,'c'=2] {'y','x'}, dimensions={0} | all-to-all | bytes 2097152 | tf_op jit(solution)/shard_map/all_to_all | solution.py:55
  109.8 1.6 %all-gather.2.cloned.1.call-done = bf16[16384,128]{1,0:T(8,128)(2,1)} async-done(((bf16[512,128]{1,0:T(8,128)(2,1)}), bf16[16384,128]{1,0:T(8,128)(2,1)}) %all-gather.2.cloned.1.call-update) | async-done | bytes 4194320 | tf_op jit(solution)/shard_map/all_gather | solution.py:328
  111.4 3.6 %shard_map.169 = bf16[16,16,2048]{2,1,0:T(8,128)(2,1)S(1)} custom-call(bf16[16,16,2048]{2,1,0:T(8,128)(2,1)S(1)} %all_to_all.34.rows_ref, bf16[2,4,4,512,128]{4,3,2,1,0:T(8,128)(2,1)} %bitcast.6), custom_call_target="tpu_custom_call" | custom-call | tf_op jit(solution)/shard_map/pallas_call | solution.py:354
  115.0 22.8 %all_to_all.35.got_ref = bf16[16,16,2048]{2,1,0:T(8,128)(2,1)S(1)} all-to-all(bf16[16,16,2048]{2,1,0:T(8,128)(2,1)S(1)} %shard_map.169), channel_id=1, replica_groups=mesh['zh'=4,'zl'=4,'y'=4,'x'=4,'c'=2] {'y','x'}, dimensions={0} | all-to-all | bytes 2097152 | tf_op jit(solution)/shard_map/all_to_all | solution.py:55
  137.8 0.8 shard_map.170
Async XLA Ops:
  6.5 104.9 %all-gather.2.cloned.1.call-start = ((), (), s32[]{:S(2)}) async-start(), calls=%async_computation.6 | async-start | bytes 4325376 | tf_op jit(solution)/shard_map/all_gather | solution.py:328
  7.3 4.8 %collective-permute-start = (bf16[8,768]{1,0:T(8,128)(2,1)S(1)}, bf16[8,768]{1,0:T(8,128)(2,1)S(1)}, u32[]{:S(2)}, u32[]{:S(2)}) collective-permute-start(bf16[8,768]{1,0:T(8,128)(2,1)S(1)} %shard_map.163), channel_id=1, source_target_pairs={{0,8},{8,16},{16,24},{24,32},{32,40},{40,48},{48,56},{56,64},{64,7... | collective-permute-start | bytes 36872 | tf_op jit(solution)/shard_map/ppermute | solution.py:293
  12.1 59.4 %copy-start = (bf16[128,512]{1,0:T(8,128)(2,1)S(1)}, bf16[128,512]{1,0:T(8,128)(2,1)}, u32[]{:S(2)}) copy-start(bf16[128,512]{1,0:T(8,128)(2,1)} %gate_ref.1) | copy-start | bytes 393220
  12.1 59.4 %copy-start.1 = (f32[512]{0:T(512)S(1)}, f32[512]{0:T(512)}, u32[]{:S(2)}) copy-start(f32[512]{0:T(512)} %param.29) | copy-start | bytes 6148
Sparse Core Ops, SparseCore 0:
  34.8 76.5 all-gather.1

commit v5 on v4

--- a/solution.py
+++ b/solution.py
@@ -1,5 +1,3 @@
-import functools
-
 import jax
 import jax.numpy as jnp
 from jax import lax
@@ -99,14 +97,25 @@
     return ref[place, start:end, :].astype(f32), tail[0:1, :] + tail[1:2, :]
 
 
-def first_kernel(x_ref, b_ref, c_ref, rim_ref):
+def rim_kernel(x_ref, b_ref, c_ref, rim_ref):
     rim_ref[:, 0:WIDTH] = x_ref[...]
     rim_ref[:, WIDTH : WIDTH + STATE] = b_ref[...]
     rim_ref[:, WIDTH + STATE : WIDTH + 2 * STATE] = c_ref[...]
 
 
+def pack_kernel(up_ref, down_ref, mine_ref):
+    depth, units = up_ref.shape
+    slices = mine_ref.shape[0]
+    slabs = units // slices // STATE
+    for k in range(slices):
+        for j in range(slabs):
+            lanes = slice((k * slabs + j) * STATE, (k * slabs + j + 1) * STATE)
+            mine_ref[k, j * depth : (j + 1) * depth, :] = up_ref[:, lanes]
+            mine_ref[k, (slabs + j) * depth : (slabs + j + 1) * depth, :] = down_ref[:, lanes]
+
+
 def local_kernel(
-    slices, x_ref, b_ref, c_ref, rim_ref, xt_ref, bt_ref, ct_ref, dt_ref, shrink_ref, up_ref, down_ref, speed_ref, skip_ref, w_ref,
+    x_ref, b_ref, c_ref, rim_ref, xt_ref, bt_ref, ct_ref, dt_ref, shrink_ref, speed_ref, skip_ref, w_ref,
     pre_ref, query_ref, cum_ref, send_ref, w_out, x_room, b_room, c_room, sem,
 ):
     copy = pltpu.make_async_copy(w_ref, w_out, sem)
@@ -133,16 +142,10 @@
     weighted = (values * spread(weight, HEAD_DIM)).astype(bf16)
     state = dot(weighted, keys, ((0,), (0,)))
     pieces = send_ref.shape[0]
-    depth, units = up_ref.shape
     count = WIDTH // pieces
-    slabs = units // slices // STATE
     for place in range(pieces):
-        slab, k = divmod(place, slices)
-        source = up_ref if slab < slabs else down_ref
-        first_lane = (k * slabs + slab % slabs) * STATE
-        send_ref[place, 0:depth, :] = source[:, first_lane : first_lane + STATE]
         h = place * count // HEAD_DIM
-        put_state(send_ref, place, depth, state[place * count : (place + 1) * count, :], last[h : h + 1, :])
+        put_state(send_ref, place, 0, state[place * count : (place + 1) * count, :], last[h : h + 1, :])
     scores = dot(query, keys, ((1,), (1,)))
     columns = spread(cum, BLOCK)
     later = lax.broadcasted_iota(jnp.int32, (BLOCK, BLOCK), 0)
@@ -164,12 +167,10 @@
     copy.wait()
 
 
-def near_kernel(got_ref, shard_ref, send_ref):
-    start = shard_ref.shape[1]
+def near_kernel(got_ref, send_ref):
     state = log = None
     for k in range(got_ref.shape[0]):
-        shard_ref[k] = got_ref[k, 0:start, :]
-        more, step = take_state(got_ref, k, start)
+        more, step = take_state(got_ref, k, 0)
         state, log = (more, step) if state is None else (state * jnp.exp(step) + more, log + step)
     for k in range(send_ref.shape[0]):
         put_state(send_ref, k, 0, state, log)
@@ -184,11 +185,10 @@
         state = state * jnp.exp(step) + more
         before = jnp.where(k < here, state, before)
     state = before
-    start = near_ref.shape[1] - count - TAIL
     for k in range(near_ref.shape[0]):
         out_ref[k] = state.astype(bf16)
         if k + 1 < near_ref.shape[0]:
-            more, step = take_state(near_ref, k, start)
+            more, step = take_state(near_ref, k, 0)
             state = state * jnp.exp(step) + more
 
 
@@ -216,16 +216,21 @@
 
 
 def mlp_kernel(rows_ref, w_ref, out_ref, w_room, sems):
-    halves, pieces, slabs, size, lanes = w_ref.shape
+    halves, shards, inner, slabs, each_depth, lanes = w_ref.shape
+    pieces = sems.shape[1]
+    take = shards // pieces
+    size = take * inner * each_depth
     copies = []
     for j in range(pieces):
         for k in range(halves):
-            copy = pltpu.make_async_copy(w_ref.at[k, j], w_room.at[k, j], sems.at[k, j])
+            part = pl.ds(j * take, take)
+            copy = pltpu.make_async_copy(w_ref.at[k, part], w_room.at[k, part], sems.at[k, j])
             copy.start()
             copies.append(copy)
 
     def piece(k, j, first):
-        return jnp.concatenate([w_room[k, j, n] for n in range(first, first + slabs // 2)], axis=1)
+        parts = [w_room[k, j * take : (j + 1) * take, :, n, :, :] for n in (first, first + 1)]
+        return jnp.concatenate([p.reshape(size, lanes) for p in parts], axis=1)
 
     count, each, depth = rows_ref.shape
     rows = rows_ref[...].reshape(count * each, depth)
@@ -254,7 +259,7 @@
     out_ref[...] = (own_ref[...].astype(f32) + total.astype(bf16).astype(f32)).astype(bf16)
 
 
-def per_device(
+def layer(
     skip_stream_entering,
     content_signal_matrix,
     writer_signal_matrix,
@@ -281,9 +286,10 @@
     depth, units = widening_matrix.shape
     pieces = nzl * ny
     count = WIDTH // pieces
+    shard = 2 * depth * units // ny // STATE
 
     rim = pl.pallas_call(
-        first_kernel,
+        rim_kernel,
         grid=(1,),
         out_shape=shape((RIM, WIDTH + 2 * STATE), bf16),
         in_specs=[pl.BlockSpec((RIM, n), lambda i: (BLOCK // RIM - 1, 0)) for n in (WIDTH, STATE, STATE)],
@@ -291,16 +297,23 @@
         interpret=INTERPRET,
     )(content_signal_matrix, writer_signal_matrix, reader_signal_matrix)
     rim = lax.ppermute(rim, SP, [(k, k + 1) for k in range(nsp - 1)])
+    mine = call(pack_kernel, shape((ny, shard, STATE), bf16), [VMEM] * 2)(
+        widening_matrix, narrowing_matrix.T
+    )
+    parts = exchange(mine, "y")
+    weights = lax.all_gather(parts.reshape(ny * shard, STATE), ("c", "zh", "zl"), axis=0, tiled=True)
+    weights = weights.reshape(-1, nzh * nzl, ny, shard // depth, depth, STATE)
+    rim, parts = lax.optimization_barrier((rim, parts))
     pre, query, cum, send, projection = call(
-        functools.partial(local_kernel, ny),
+        local_kernel,
         [
             shape((BLOCK, WIDTH), f32),
             shape((BLOCK, STATE), bf16),
             shape((HEADS, BLOCK), f32),
-            shape((pieces, depth + count + TAIL, STATE), bf16),
+            shape((pieces, count + TAIL, STATE), bf16),
             shape(blend_result_matrix.shape, bf16),
         ],
-        [VMEM] * 11 + [SMEM] * 2 + [HBM],
+        [VMEM] * 9 + [SMEM] * 2 + [HBM],
         [pltpu.VMEM((RIM + BLOCK, n), f32) for n in (WIDTH, STATE, STATE)] + [pltpu.SemaphoreType.DMA(())],
     )(
         content_signal_matrix,
@@ -312,21 +325,12 @@
         reader_filter_coefs,
         interval_before_softplus,
         extra_log_shrink,
-        widening_matrix,
-        narrowing_matrix.T,
         log_forget_speed,
         skip_path_factor,
         blend_result_matrix,
     )
     got = near(exchange(send, NEAR))
-    parts, send = call(
-        near_kernel,
-        [jax.ShapeDtypeStruct((pieces, depth, STATE), bf16), shape((nzh, count + TAIL, STATE), bf16)],
-        [VMEM],
-        compiler_params=ROOM,
-    )(got)
-    weights = lax.all_gather(parts.reshape(pieces * depth, STATE), ("c", "zh", "zl"), axis=0, tiled=True)
-    weights = weights.reshape(-1, nzh, nzl, pieces * depth, STATE)
+    send = call(near_kernel, shape((nzh, count + TAIL, STATE), bf16), [VMEM], compiler_params=ROOM)(got)
     far = near(exchange(send, "zh"))
     before = call(far_kernel, shape((pieces, count, STATE), bf16), [VMEM] * 2, compiler_params=ROOM)(far, got)
     incoming = exchange(before, NEAR)
@@ -355,7 +359,7 @@
         mlp_kernel,
         shape((nrows, own_count, width), bf16),
         [VMEM, HBM],
-        [pltpu.VMEM(weights.shape, bf16), pltpu.SemaphoreType.DMA(weights.shape[:2])],
+        [pltpu.VMEM(weights.shape, bf16), pltpu.SemaphoreType.DMA((weights.shape[0], 4))],
     )(near(rows), weights)
     out = exchange(out, ROWS)
     return call(final_kernel, jax.ShapeDtypeStruct((own_count, width), bf16), [VMEM] * 2)(near(out), near(own))
@@ -382,6 +386,4 @@
         P(SP, TP),
         P(TP, SP),
     )
-    return jax.shard_map(
-        per_device, mesh=torus, in_specs=placed, out_specs=P(SP + TP, None), check_vma=False
-    )
+    return jax.shard_map(layer, mesh=torus, in_specs=placed, out_specs=P(SP + TP, None), check_vma=False)

time: 146 us -> 152 us (1.041)
  blocking collectives: 115 us -> 123 us
  starting transfers between devices: 4.01 us -> 2.18 us
  waiting for transfers between devices: 2.47 us -> 0.83 us
    all_to_all x6 -> x7, blocking collectives: 115 us -> 123 us  [exchange(): return lax.all_to_all(value, axes, split_axis=0, concat_axis=0, tiled=True)]
    ppermute x1, starting transfers between devices: 4.01 us -> 2.18 us  [layer(): rim = lax.ppermute(rim, SP, [(k, k + 1) for k in range(nsp - 1)])]
    all_gather x1, waiting for transfers between devices: 1.64 us -> 0.01 us  [layer(): lax.all_gather(parts.reshape(ny * shard, STATE), ('c', 'zh', 'zl'), axis=...]
    pallas_call x8 -> x9, Pallas kernels: 10.8 us -> 12.1 us  [the longest x1 3.98 us: layer(): call(local_kernel, [shape((BLOCK, WIDTH), f32), shape((BLOCK, STATE), bf1...]
  transfers between devices with their start and end apart: 2 -> 2, of which waited for: 2 -> 1; matrix products, arithmetic and copies ran while one was open for 0% -> 0% of each run, Pallas kernels for 1% -> 5%
where the time goes in v5:
time: 152 us; the launch traced here: 151 us
  blocking collectives  123 us (81%)
  between operations  13.5 us (9%)
  Pallas kernels  12.1 us (8%)
  starting transfers between devices  2.18 us (1%)
    all_to_all x7, blocking collectives, exchange(): return lax.all_to_all(value, axes, split_axis=0, concat_axis=0, tiled=True)  123 us
    pallas_call x1, Pallas kernels, layer(): call(local_kernel, [shape((BLOCK, WIDTH), f32), shape((BLOCK, STATE), bf1...  3.98 us
    pallas_call x1, Pallas kernels, layer(): call(mlp_kernel, shape((nrows, own_count, width), bf16), [VMEM, HBM], [pl...  3.58 us
  transfers between devices with their start and end apart: 2, of which 1 were waited for; matrix products, arithmetic and copies ran while one was open for 0% of the time, Pallas kernels for 5%

profile of v5, /device:TPU:1, one launch (start us, length us, event | category | flops | bytes accessed | tf_op | source)
XLA Modules:
  0.0 151.3 jit_solution(1157652036053001385)
XLA Ops:
  6.5 0.0 all-gather.2.cloned.1.call-start
  6.5 0.9 shard_map.164
  7.4 0.0 copy-start
  7.4 0.0 copy-start.1
  7.5 9.9 %all_to_all.35 = bf16[4,128,128]{2,1,0:T(8,128)(2,1)} all-to-all(bf16[4,128,128]{2,1,0:T(8,128)(2,1)S(1)} %shard_map.164), channel_id=1, replica_groups=mesh['zh'=4,'zl'=4,'y'=4,'x'=4,'c'=2] {'y'}, dimensions={0} | all-to-all | bytes 262144 | tf_op jit(solution)/shard_map/all_to_all | solution.py:53
  17.3 0.0 all-gather.2.cloned.1.call-update
  17.4 0.7 shard_map.163
  18.1 2.2 %collective-permute-start = (bf16[8,768]{1,0:T(8,128)(2,1)S(1)}, bf16[8,768]{1,0:T(8,128)(2,1)S(1)}, u32[]{:S(2)}, u32[]{:S(2)}) collective-permute-start(bf16[8,768]{1,0:T(8,128)(2,1)S(1)} %shard_map.163), channel_id=1, source_target_pairs={{0,8},{8,16},{16,24},{24,32},{32,40},{40,48},{48,56},{56,64},{64,7... | collective-permute-start | bytes 36872 | tf_op jit(solution)/shard_map/ppermute | solution.py:299
  20.3 0.8 collective-permute-done.rim_ref
  21.1 4.0 %shard_map.165 = (f32[128,512]{1,0:T(8,128)S(1)}, bf16[128,128]{1,0:T(8,128)(2,1)S(1)}, f32[8,128]{1,0:T(8,128)S(1)}, bf16[16,48,128]{2,1,0:T(8,128)(2,1)S(1)}, bf16[512,2048]{1,0:T(8,128)(2,1)S(1)}) custom-call(bf16[128,512]{1,0:T(8,128)(2,1)} %x_ref.3, bf16[128,128]{1,0:T(8,128)(2,1)} %b_ref.3, bf16[128,128]{1,0:T(8,128)(2,1)} %c_ref.3, ...), custom_call_target="tpu_custom_call" | custom-call | tf_op jit(solution)/shard_map/pallas_call | solution.py:307
  25.1 18.6 %all_to_all.36.got_ref.near_ref = bf16[16,48,128]{2,1,0:T(8,128)(2,1)S(1)} all-to-all(bf16[16,48,128]{2,1,0:T(8,128)(2,1)S(1)} %get-tuple-element.17), channel_id=1, replica_groups=mesh['zh'=4,'zl'=4,'y'=4,'x'=4,'c'=2] {'zl','y'}, dimensions={0} | all-to-all | bytes 393216 | tf_op jit(solution)/shard_map/all_to_all | solution.py:53
  43.7 0.1 shard_map.166
  43.7 24.5 %all_to_all.37.got_ref = bf16[4,48,128]{2,1,0:T(8,128)(2,1)S(1)} all-to-all(bf16[4,48,128]{2,1,0:T(8,128)(2,1)S(1)} %shard_map.166), channel_id=1, replica_groups=mesh['zh'=4,'zl'=4,'y'=4,'x'=4,'c'=2] {'zh'}, dimensions={0} | all-to-all | bytes 98304 | tf_op jit(solution)/shard_map/all_to_all | solution.py:53
  68.2 0.1 shard_map.167
  68.3 11.0 %all_to_all.38.inc_ref = bf16[16,32,128]{2,1,0:T(8,128)(2,1)S(1)} all-to-all(bf16[16,32,128]{2,1,0:T(8,128)(2,1)S(1)} %shard_map.167), channel_id=1, replica_groups=mesh['zh'=4,'zl'=4,'y'=4,'x'=4,'c'=2] {'zl','y'}, dimensions={0} | all-to-all | bytes 262144 | tf_op jit(solution)/shard_map/all_to_all | solution.py:53
  79.3 0.0 copy-done
  79.3 0.0 copy-done.1
  79.3 0.9 shard_map.168
  80.3 21.4 %all_to_all.39.got_ref = bf16[8,16,2048]{2,1,0:T(8,128)(2,1)S(1)} all-to-all(bf16[8,16,2048]{2,1,0:T(8,128)(2,1)S(1)} %shard_map.168), channel_id=1, replica_groups=mesh['zh'=4,'zl'=4,'y'=4,'x'=4,'c'=2] {'x','c'}, dimensions={0} | all-to-all | bytes 1048576 | tf_op jit(solution)/shard_map/all_to_all | solution.py:53
  101.6 1.1 shard_map.169
  102.7 18.8 %all_to_all.40.rows_ref = bf16[16,16,2048]{2,1,0:T(8,128)(2,1)S(1)} all-to-all(bf16[16,16,2048]{2,1,0:T(8,128)(2,1)S(1)} %get-tuple-element.19), channel_id=1, replica_groups=mesh['zh'=4,'zl'=4,'y'=4,'x'=4,'c'=2] {'y','x'}, dimensions={0} | all-to-all | bytes 2097152 | tf_op jit(solution)/shard_map/all_to_all | solution.py:53
  121.5 0.0 all-gather.2.cloned.1.call-done
  121.5 3.6 %shard_map.170 = bf16[16,16,2048]{2,1,0:T(8,128)(2,1)S(1)} custom-call(bf16[16,16,2048]{2,1,0:T(8,128)(2,1)S(1)} %all_to_all.40.rows_ref, bf16[2,16,4,4,32,128]{5,4,3,2,1,0:T(8,128)(2,1)} %bitcast.6), custom_call_target="tpu_custom_call" | custom-call | tf_op jit(solution)/shard_map/pallas_call | solution.py:358
  125.1 18.6 %all_to_all.41.got_ref = bf16[16,16,2048]{2,1,0:T(8,128)(2,1)S(1)} all-to-all(bf16[16,16,2048]{2,1,0:T(8,128)(2,1)S(1)} %shard_map.170), channel_id=1, replica_groups=mesh['zh'=4,'zl'=4,'y'=4,'x'=4,'c'=2] {'y','x'}, dimensions={0} | all-to-all | bytes 2097152 | tf_op jit(solution)/shard_map/all_to_all | solution.py:53
  143.7 0.8 shard_map.171
Async XLA Ops:
  6.5 115.0 %all-gather.2.cloned.1.call-start = ((), (), s32[]{:S(2)}) async-start(), calls=%async_computation.7 | async-start | bytes 4325376 | tf_op jit(solution)/shard_map/all_gather | solution.py:304
  7.4 71.9 %copy-start = (bf16[128,512]{1,0:T(8,128)(2,1)S(1)}, bf16[128,512]{1,0:T(8,128)(2,1)}, u32[]{:S(2)}) copy-start(bf16[128,512]{1,0:T(8,128)(2,1)} %gate_ref.1) | copy-start | bytes 393220
  7.4 71.9 %copy-start.1 = (f32[512]{0:T(512)S(1)}, f32[512]{0:T(512)}, u32[]{:S(2)}) copy-start(f32[512]{0:T(512)} %param.29) | copy-start | bytes 6148
  18.1 3.0 %collective-permute-start = (bf16[8,768]{1,0:T(8,128)(2,1)S(1)}, bf16[8,768]{1,0:T(8,128)(2,1)S(1)}, u32[]{:S(2)}, u32[]{:S(2)}) collective-permute-start(bf16[8,768]{1,0:T(8,128)(2,1)S(1)} %shard_map.163), channel_id=1, source_target_pairs={{0,8},{8,16},{16,24},{24,32},{32,40},{40,48},{48,56},{56,64},{64,7... | collective-permute-start | bytes 36872 | tf_op jit(solution)/shard_map/ppermute | solution.py:299
Sparse Core Ops, SparseCore 0:
  17.5 79.6 all-gather.1

commit v6 on v3

--- a/solution.py
+++ b/solution.py
@@ -19,6 +19,7 @@
 ROWS = ("y", "x")
 EPSILON = 1e-05
 INTERPRET = False
+ROOM = pltpu.CompilerParams(vmem_limit_bytes=16 << 20)
 
 f32 = jnp.float32
 bf16 = jnp.bfloat16
@@ -67,17 +68,15 @@
     return value / (1.0 + jnp.exp(-value))
 
 
-def convolve(src_ref, rim, taps_ref, room):
-    room[0:RIM, :] = rim.astype(f32)
-    room[RIM : RIM + BLOCK, :] = src_ref[...].astype(f32)
+def convolve(room, taps_ref, count):
     taps = taps_ref[...].astype(f32)
     width = taps.shape[0]
     total = None
     for k in range(width):
         start = RIM - width + 1 + k
-        term = room[start : start + BLOCK, :] * taps[k : k + 1, :]
+        term = room[start : start + count, :] * taps[k : k + 1, :]
         total = term if total is None else total + term
-    return silu(total)
+    return total
 
 
 def put_state(ref, place, start, state, logs):
@@ -108,14 +107,16 @@
     rim_ref[:, WIDTH + STATE : WIDTH + 2 * STATE] = c_ref[...]
 
 
-def local_kernel(
-    x_ref, b_ref, c_ref, rim_ref, xt_ref, bt_ref, ct_ref, dt_ref, shrink_ref, up_ref, down_ref, speed_ref, skip_ref,
-    pre_ref, query_ref, cum_ref, send_ref, x_room, b_room, c_room,
+def early_kernel(
+    x_ref, b_ref, c_ref, xt_ref, bt_ref, ct_ref, dt_ref, shrink_ref, speed_ref,
+    x_out, b_out, c_out, cum_ref, weight_ref, mask_ref, x_room, b_room, c_room,
 ):
-    values = convolve(x_ref, rim_ref[:, 0:WIDTH], xt_ref, x_room)
-    keys = convolve(b_ref, rim_ref[:, WIDTH : WIDTH + STATE], bt_ref, b_room).astype(bf16)
-    query = convolve(c_ref, rim_ref[:, WIDTH + STATE : WIDTH + 2 * STATE], ct_ref, c_room).astype(bf16)
-    query_ref[...] = query
+    for src_ref, taps_ref, out_ref, room in (
+        (x_ref, xt_ref, x_out, x_room), (b_ref, bt_ref, b_out, b_room), (c_ref, ct_ref, c_out, c_room)
+    ):
+        room[0:RIM, :] = jnp.zeros((RIM, room.shape[1]), f32)
+        room[RIM : RIM + BLOCK, :] = src_ref[...].astype(f32)
+        out_ref[...] = convolve(room, taps_ref, BLOCK)
     before = dt_ref[...]
     steps = jnp.maximum(before, 0.0) + jnp.log1p(jnp.exp(-jnp.abs(before)))
     head = lax.broadcasted_iota(jnp.int32, (HEADS, BLOCK), 0)
@@ -129,10 +130,37 @@
         cum = cum + jnp.where(token >= reach, pltpu.roll(cum, reach, 1), 0.0)
         reach *= 2
     cum_ref[...] = cum
-    last = cum[:, BLOCK - 1 : BLOCK]
-    weight = steps * jnp.exp(last - cum)
-    weighted = (values * spread(weight, HEAD_DIM)).astype(bf16)
-    state = dot(weighted, keys, ((0,), (0,)))
+    weight_ref[...] = spread(steps * jnp.exp(cum[:, BLOCK - 1 : BLOCK] - cum), HEAD_DIM)
+    columns = spread(cum, BLOCK)
+    later = lax.broadcasted_iota(jnp.int32, (BLOCK, BLOCK), 0)
+    earlier = lax.broadcasted_iota(jnp.int32, (BLOCK, BLOCK), 1)
+    causal = later >= earlier
+    for h in range(HEADS):
+        away = columns[:, h * BLOCK : (h + 1) * BLOCK] - cum[h : h + 1, :]
+        mask_ref[h] = jnp.exp(jnp.where(causal, away, -jnp.inf)) * steps[h : h + 1, :]
+
+
+def local_kernel(
+    x_ref, b_ref, c_ref, rim_ref, xt_ref, bt_ref, ct_ref, x_sum, b_sum, c_sum, cum_ref, weight_ref, mask_ref,
+    up_ref, down_ref, skip_ref, w_ref,
+    pre_ref, query_ref, send_ref, w_out, x_room, b_room, c_room, sem,
+):
+    copy = pltpu.make_async_copy(w_ref, w_out, sem)
+    copy.start()
+    rows = []
+    lane = 0
+    for src_ref, taps_ref, sum_ref, room in (
+        (x_ref, xt_ref, x_sum, x_room), (b_ref, bt_ref, b_sum, b_room), (c_ref, ct_ref, c_sum, c_room)
+    ):
+        room[0:RIM, :] = rim_ref[:, lane : lane + room.shape[1]].astype(f32)
+        room[RIM : 2 * RIM, :] = src_ref[...].astype(f32)
+        lane += room.shape[1]
+        head = convolve(room, taps_ref, RIM)
+        rows.append(silu(jnp.concatenate([head, sum_ref[RIM:BLOCK, :]], axis=0)))
+    values, keys, query = rows[0], rows[1].astype(bf16), rows[2].astype(bf16)
+    query_ref[...] = query
+    last = cum_ref[:, BLOCK - 1 : BLOCK]
+    state = dot((values * weight_ref[...]).astype(bf16), keys, ((0,), (0,)))
     pieces = send_ref.shape[0]
     depth, units = up_ref.shape
     slabs = units // pieces // STATE
@@ -143,10 +171,6 @@
             send_ref[k, (slabs + j) * depth : (slabs + j + 1) * depth, :] = down_ref[:, lanes]
         put_state(send_ref, k, 2 * slabs * depth, state[k * PAIR : (k + 1) * PAIR, :], last[2 * k : 2 * k + 2, :])
     scores = dot(query, keys, ((1,), (1,)))
-    columns = spread(cum, BLOCK)
-    later = lax.broadcasted_iota(jnp.int32, (BLOCK, BLOCK), 0)
-    earlier = lax.broadcasted_iota(jnp.int32, (BLOCK, BLOCK), 1)
-    causal = later >= earlier
     first = lax.broadcasted_iota(jnp.int32, (BLOCK, 2 * HEAD_DIM), 1) < HEAD_DIM
     for pair in range(HEADS // 2):
         lanes = slice(pair * 2 * HEAD_DIM, (pair + 1) * 2 * HEAD_DIM)
@@ -154,12 +178,12 @@
         two_low = two.astype(bf16)
         parts = []
         for h in (2 * pair, 2 * pair + 1):
-            away = columns[:, h * BLOCK : (h + 1) * BLOCK] - cum[h : h + 1, :]
-            mixing = scores * jnp.exp(jnp.where(causal, away, -jnp.inf)) * steps[h : h + 1, :]
+            mixing = scores * mask_ref[h]
             parts.append(dot(mixing.astype(bf16), two_low, ((1,), (0,))))
         within = jnp.where(first, parts[0], parts[1])
         skip = jnp.where(first, skip_ref[2 * pair], skip_ref[2 * pair + 1])
         pre_ref[:, lanes] = within + skip * two
+    copy.wait()
 
 
 def row_kernel(got_ref, shard_ref, send_ref):
@@ -203,16 +227,13 @@
             state = state * factor(step) + more
 
 
-def gate_kernel(pre_ref, query_ref, cum_ref, inc_ref, gate_ref, gain_ref, w_ref, out_ref, w_room, sem):
-    copy = pltpu.make_async_copy(w_ref, w_room, sem)
-    copy.start()
+def gate_kernel(pre_ref, query_ref, cum_ref, inc_ref, gate_ref, gain_ref, w_ref, out_ref):
     inc = inc_ref[...].reshape(WIDTH, STATE)
     arriving = dot(query_ref[...], inc, ((1,), (1,))) * spread(jnp.exp(cum_ref[...]), HEAD_DIM)
     gated = (pre_ref[...] + arriving) * silu(gate_ref[...].astype(f32))
     scale = lax.rsqrt(jnp.mean(gated * gated, axis=-1, keepdims=True) + EPSILON)
     heads_out = (gated * scale * gain_ref[...]).astype(bf16)
-    copy.wait()
-    out = dot(heads_out, w_room[...], ((1,), (0,))).astype(bf16)
+    out = dot(heads_out, w_ref[...], ((1,), (0,))).astype(bf16)
     out_ref[...] = out.reshape(out_ref.shape)
 
 
@@ -273,7 +294,7 @@
     out_ref[...] = (own_ref[...].astype(f32) + total.astype(bf16).astype(f32)).astype(bf16)
 
 
-def per_device(
+def layer(
     skip_stream_entering,
     content_signal_matrix,
     writer_signal_matrix,
@@ -309,36 +330,65 @@
         interpret=INTERPRET,
     )(content_signal_matrix, writer_signal_matrix, reader_signal_matrix)
     rim = lax.ppermute(rim, SP, [(k, k + 1) for k in range(nsp - 1)])
-    pre, query, cum, send = call(
-        local_kernel,
+    *sums, cum, weight, mask = call(
+        early_kernel,
         [
             shape((BLOCK, WIDTH), f32),
-            shape((BLOCK, STATE), bf16),
+            shape((BLOCK, STATE), f32),
+            shape((BLOCK, STATE), f32),
             shape((HEADS, BLOCK), f32),
-            shape((ny, shard + PAIR + TAIL, STATE), bf16),
+            shape((BLOCK, WIDTH), f32),
+            shape((HEADS, BLOCK, BLOCK), f32),
         ],
-        [VMEM] * 11 + [SMEM] * 2,
+        [VMEM] * 8 + [SMEM],
         [pltpu.VMEM((RIM + BLOCK, n), f32) for n in (WIDTH, STATE, STATE)],
     )(
         content_signal_matrix,
         writer_signal_matrix,
         reader_signal_matrix,
-        near(rim),
         content_filter_coefs,
         writer_filter_coefs,
         reader_filter_coefs,
         interval_before_softplus,
         extra_log_shrink,
-        widening_matrix,
-        narrowing_matrix.T,
         log_forget_speed,
-        skip_path_factor,
     )
+
+    def whole(value):
+        zeros = (0,) * value.ndim
+        return pl.BlockSpec(value.shape, lambda i: zeros)
+
+    head_rows = (content_signal_matrix, writer_signal_matrix, reader_signal_matrix)
+    taps = (content_filter_coefs, writer_filter_coefs, reader_filter_coefs)
+    kept = [near(value) for value in (*sums, cum, weight, mask)]
+    outs = [
+        shape((BLOCK, WIDTH), f32),
+        jax.ShapeDtypeStruct((BLOCK, STATE), bf16),
+        shape((ny, shard + PAIR + TAIL, STATE), bf16),
+        shape(blend_result_matrix.shape, bf16),
+    ]
+    narrowing = narrowing_matrix.T
+    pre, query, send, projection = pl.pallas_call(
+        local_kernel,
+        grid=(1,),
+        out_shape=outs,
+        in_specs=[pl.BlockSpec((RIM, value.shape[1]), lambda i: (0, 0)) for value in head_rows]
+        + [VMEM]
+        + [whole(value) for value in taps]
+        + [VMEM] * len(kept)
+        + [whole(widening_matrix), whole(narrowing), SMEM, HBM],
+        out_specs=[VMEM] * 4,
+        scratch_shapes=[pltpu.VMEM((2 * RIM, n), f32) for n in (WIDTH, STATE, STATE)]
+        + [pltpu.SemaphoreType.DMA(())],
+        interpret=INTERPRET,
+        compiler_params=pltpu.CompilerParams(vmem_limit_bytes=56 << 20),
+    )(*head_rows, near(rim), *taps, *kept, widening_matrix, narrowing, skip_path_factor, blend_result_matrix)
     rows = near(exchange(send, "y"))
     parts, send = call(
         row_kernel,
         [jax.ShapeDtypeStruct((ny, shard, STATE), bf16), shape((nzl, PAIR + TAIL, STATE), bf16)],
         [VMEM],
+        compiler_params=ROOM,
     )(rows)
     weights = lax.all_gather(parts.reshape(ny * shard, STATE), ("c", "zh", "zl"), axis=0, tiled=True)
     weights = weights.reshape(-1, nzh * nzl, ny, shard // depth, depth, STATE)
@@ -347,23 +397,26 @@
         near_kernel,
         [shape((nzh, PAIR + TAIL, STATE), bf16), shape((PAIR, STATE), f32), shape((2, STATE), f32)],
         [VMEM],
+        compiler_params=ROOM,
     )(got)
     got = near(exchange(send, "zh"))
-    before = call(far_kernel, shape((ny, PAIR, STATE), bf16), [VMEM] * 4)(got, near(state), near(logs), rows)
+    before = call(far_kernel, shape((ny, PAIR, STATE), bf16), [VMEM] * 4, compiler_params=ROOM)(
+        got, near(state), near(logs), rows
+    )
     incoming = exchange(before, "y")
     mixed = call(
         gate_kernel,
         shape((ntp, own_count, width), bf16),
-        [VMEM] * 6 + [HBM],
-        [pltpu.VMEM(blend_result_matrix.shape, bf16), pltpu.SemaphoreType.DMA(())],
+        [VMEM] * 7,
+        compiler_params=ROOM,
     )(
         near(pre),
-        near(query),
-        near(cum),
+        query,
+        cum,
         near(incoming),
         multiplier_signal,
         cluster_scaling_vector.reshape(1, -1),
-        blend_result_matrix,
+        near(projection),
     )
     mixed = exchange(mixed, TP)
     own, copies = call(
@@ -403,6 +456,4 @@
         P(SP, TP),
         P(TP, SP),
     )
-    return jax.shard_map(
-        per_device, mesh=torus, in_specs=placed, out_specs=P(SP + TP, None), check_vma=False
-    )
+    return jax.shard_map(layer, mesh=torus, in_specs=placed, out_specs=P(SP + TP, None), check_vma=False)

time: 147 us -> 145 us (0.986)
    all_to_all x7, blocking collectives: 113 us -> 112 us  [exchange(): return lax.all_to_all(value, axes, split_axis=0, concat_axis=0, tiled=True)]
    pallas_call x9 -> x10, Pallas kernels: 13.3 us -> 13.7 us  [the longest x1 3.58 us: layer(): call(mlp_kernel, shape((nrows, own_count, width), bf16), [VMEM, HBM], [pl...]
  transfers between devices with their start and end apart: 2 -> 2, of which waited for: 1 -> 0; matrix products, arithmetic and copies ran while one was open for 0% -> 0% of each run, Pallas kernels for 3% -> 3%
where the time goes in v6:
time: 145 us; the launch traced here: 143 us
  blocking collectives  112 us (77%)
  Pallas kernels  13.7 us (9%)
  between operations  13.5 us (9%)
  starting transfers between devices  4.01 us (3%)
    all_to_all x7, blocking collectives, exchange(): return lax.all_to_all(value, axes, split_axis=0, concat_axis=0, tiled=True)  112 us
    ppermute x1, starting transfers between devices, layer(): rim = lax.ppermute(rim, SP, [(k, k + 1) for k in range(nsp - 1)])  4.01 us
    pallas_call x1, Pallas kernels, layer(): call(mlp_kernel, shape((nrows, own_count, width), bf16), [VMEM, HBM], [pl...  3.58 us
    pallas_call x1, Pallas kernels, layer(): pl.pallas_call(local_kernel, grid=(1,), out_shape=outs, in_specs=[pl.Bloc...  3.22 us
  transfers between devices with their start and end apart: 2, of which 0 were waited for; matrix products, arithmetic and copies ran while one was open for 0% of the time, Pallas kernels for 3%

profile of v6, /device:TPU:1, one launch (start us, length us, event | category | flops | bytes accessed | tf_op | source)
XLA Modules:
  0.0 142.9 jit_solution(11733705012442786768)
XLA Ops:
  6.5 0.0 all-gather.2.cloned.1.call-start
  6.5 0.7 shard_map.163
  7.3 4.0 %collective-permute-start = (bf16[8,768]{1,0:T(8,128)(2,1)S(1)}, bf16[8,768]{1,0:T(8,128)(2,1)S(1)}, u32[]{:S(2)}, u32[]{:S(2)}) collective-permute-start(bf16[8,768]{1,0:T(8,128)(2,1)S(1)} %shard_map.163), channel_id=1, source_target_pairs={{0,8},{8,16},{16,24},{24,32},{32,40},{40,48},{48,56},{56,64},{64,7... | collective-permute-start | bytes 36872 | tf_op jit(solution)/shard_map/ppermute | solution.py:332
  11.3 2.6 %shard_map.164 = (f32[128,512]{1,0:T(8,128)S(1)}, f32[128,128]{1,0:T(8,128)S(1)}, f32[128,128]{1,0:T(8,128)S(1)}, f32[8,128]{1,0:T(8,128)S(1)}, f32[128,512]{1,0:T(8,128)S(1)}, /*index=5*/f32[8,128,128]{2,1,0:T(8,128)S(1)}) custom-call(bf16[128,512]{1,0:T(8,128)(2,1)} %x_ref.5, bf16[128,128]{1,0:T(8,128)(2,1)} %b_ref.5, bf16[128,128]{1,0:T(8,128)(2,1)} %c_ref.5, ...), custom_call_target="tpu_custom_call" | custom-call | tf_op jit(solution)/shard_map/pallas_call | solution.py:333
  13.9 0.0 copy-start.2
  13.9 0.0 collective-permute-done.rim_ref
  13.9 3.2 %shard_map.165 = (f32[128,512]{1,0:T(8,128)S(1)}, bf16[128,128]{1,0:T(8,128)(2,1)}, bf16[4,272,128]{2,1,0:T(8,128)(2,1)S(1)}, bf16[512,2048]{1,0:T(8,128)(2,1)S(1)}) custom-call(bf16[128,512]{1,0:T(8,128)(2,1)} %x_ref.5, bf16[128,128]{1,0:T(8,128)(2,1)} %b_ref.5, bf16[128,128]{1,0:T(8,128)(2,1)} %c_ref.5, bf16[8,768]{1,0:T(8,128)(2,1)S(1)} %collective-permute-done.rim_ref, ...), custom_call_target="tpu_custom_call" | custom-call | tf_op jit(solution)/shard_map/pallas_call | solution.py:371
  17.1 0.0 copy-done.2
  17.1 0.0 copy-start
  17.1 0.0 copy-start.1
  17.2 0.0 copy-start.4
  17.2 0.0 copy-start.3
  17.2 9.6 %all_to_all.35.got_ref.rows_ref = bf16[4,272,128]{2,1,0:T(8,128)(2,1)S(1)} all-to-all(bf16[4,272,128]{2,1,0:T(8,128)(2,1)S(1)} %get-tuple-element.30), channel_id=1, replica_groups=mesh['zh'=4,'zl'=4,'y'=4,'x'=4,'c'=2] {'y'}, dimensions={0} | all-to-all | bytes 557056 | tf_op jit(solution)/shard_map/all_to_all | solution.py:53
  26.7 0.7 shard_map.166
  27.4 0.0 all-gather.2.cloned.1.call-update
  27.4 12.1 %all_to_all.36.got_ref = bf16[4,144,128]{2,1,0:T(8,128)(2,1)S(1)} all-to-all(bf16[4,144,128]{2,1,0:T(8,128)(2,1)S(1)} %get-tuple-element.31), channel_id=1, replica_groups=mesh['zh'=4,'zl'=4,'y'=4,'x'=4,'c'=2] {'zl'}, dimensions={0} | all-to-all | bytes 294912 | tf_op jit(solution)/shard_map/all_to_all | solution.py:53
  39.6 0.1 shard_map.167
  39.6 25.6 %all_to_all.37.got_ref = bf16[4,144,128]{2,1,0:T(8,128)(2,1)S(1)} all-to-all(bf16[4,144,128]{2,1,0:T(8,128)(2,1)S(1)} %get-tuple-element.32), channel_id=1, replica_groups=mesh['zh'=4,'zl'=4,'y'=4,'x'=4,'c'=2] {'zh'}, dimensions={0} | all-to-all | bytes 294912 | tf_op jit(solution)/shard_map/all_to_all | solution.py:53
  65.2 0.1 shard_map.168
  65.3 7.2 %all_to_all.38.inc_ref = bf16[4,128,128]{2,1,0:T(8,128)(2,1)S(1)} all-to-all(bf16[4,128,128]{2,1,0:T(8,128)(2,1)S(1)} %shard_map.168), channel_id=1, replica_groups=mesh['zh'=4,'zl'=4,'y'=4,'x'=4,'c'=2] {'y'}, dimensions={0} | all-to-all | bytes 262144 | tf_op jit(solution)/shard_map/all_to_all | solution.py:53
  72.5 0.0 copy-done
  72.5 0.0 copy-done.1
  72.5 0.0 copy-done.4
  72.5 0.0 copy-done.3
  72.5 0.9 shard_map.169
  73.4 20.2 %all_to_all.39.got_ref = bf16[8,16,2048]{2,1,0:T(8,128)(2,1)S(1)} all-to-all(bf16[8,16,2048]{2,1,0:T(8,128)(2,1)S(1)} %shard_map.169), channel_id=1, replica_groups=mesh['zh'=4,'zl'=4,'y'=4,'x'=4,'c'=2] {'x','c'}, dimensions={0} | all-to-all | bytes 1048576 | tf_op jit(solution)/shard_map/all_to_all | solution.py:53
  93.6 1.1 shard_map.170
  94.7 18.6 %all_to_all.40.rows_ref = bf16[16,16,2048]{2,1,0:T(8,128)(2,1)S(1)} all-to-all(bf16[16,16,2048]{2,1,0:T(8,128)(2,1)S(1)} %get-tuple-element.36), channel_id=1, replica_groups=mesh['zh'=4,'zl'=4,'y'=4,'x'=4,'c'=2] {'y','x'}, dimensions={0} | all-to-all | bytes 2097152 | tf_op jit(solution)/shard_map/all_to_all | solution.py:53
  113.4 0.0 all-gather.2.cloned.1.call-done
  113.4 3.6 %shard_map.171 = bf16[16,16,2048]{2,1,0:T(8,128)(2,1)S(1)} custom-call(bf16[16,16,2048]{2,1,0:T(8,128)(2,1)S(1)} %all_to_all.40.rows_ref, bf16[2,16,4,4,32,128]{5,4,3,2,1,0:T(8,128)(2,1)} %bitcast.6), custom_call_target="tpu_custom_call" | custom-call | tf_op jit(solution)/shard_map/pallas_call | solution.py:428
  116.9 18.3 %all_to_all.41.got_ref = bf16[16,16,2048]{2,1,0:T(8,128)(2,1)S(1)} all-to-all(bf16[16,16,2048]{2,1,0:T(8,128)(2,1)S(1)} %shard_map.171), channel_id=1, replica_groups=mesh['zh'=4,'zl'=4,'y'=4,'x'=4,'c'=2] {'y','x'}, dimensions={0} | all-to-all | bytes 2097152 | tf_op jit(solution)/shard_map/all_to_all | solution.py:53
  135.2 0.8 shard_map.172
Async XLA Ops:
  6.5 106.8 %all-gather.2.cloned.1.call-start = ((), (), s32[]{:S(2)}) async-start(), calls=%async_computation.7 | async-start | bytes 4325376 | tf_op jit(solution)/shard_map/all_gather | solution.py:393
  7.3 6.6 %collective-permute-start = (bf16[8,768]{1,0:T(8,128)(2,1)S(1)}, bf16[8,768]{1,0:T(8,128)(2,1)S(1)}, u32[]{:S(2)}, u32[]{:S(2)}) collective-permute-start(bf16[8,768]{1,0:T(8,128)(2,1)S(1)} %shard_map.163), channel_id=1, source_target_pairs={{0,8},{8,16},{16,24},{24,32},{32,40},{40,48},{48,56},{56,64},{64,7... | collective-permute-start | bytes 36872 | tf_op jit(solution)/shard_map/ppermute | solution.py:332
  13.9 3.2 %copy-start.2 = (f32[8,128]{1,0:T(8,128)}, f32[8,128]{1,0:T(8,128)S(1)}, u32[]{:S(2)}) copy-start(f32[8,128]{1,0:T(8,128)S(1)} %get-tuple-element.25.cum_ref) | copy-start | bytes 12292
  17.1 55.4 %copy-start = (bf16[128,512]{1,0:T(8,128)(2,1)S(1)}, bf16[128,512]{1,0:T(8,128)(2,1)}, u32[]{:S(2)}) copy-start(bf16[128,512]{1,0:T(8,128)(2,1)} %gate_ref.1) | copy-start | bytes 393220
  17.1 55.4 %copy-start.1 = (bf16[128,128]{1,0:T(8,128)(2,1)S(1)}, bf16[128,128]{1,0:T(8,128)(2,1)}, u32[]{:S(2)}) copy-start(bf16[128,128]{1,0:T(8,128)(2,1)} %get-tuple-element.29.query_ref) | copy-start | bytes 98308
  17.2 55.4 %copy-start.4 = (f32[512]{0:T(512)S(1)}, f32[512]{0:T(512)}, u32[]{:S(2)}) copy-start(f32[512]{0:T(512)} %param.29) | copy-start | bytes 6148
  17.2 55.3 %copy-start.3 = (f32[8,128]{1,0:T(8,128)S(1)}, f32[8,128]{1,0:T(8,128)}, u32[]{:S(2)}) copy-start(f32[8,128]{1,0:T(8,128)} %copy-done.2) | copy-start | bytes 12292
Sparse Core Ops, SparseCore 0:
  27.5 81.2 all-gather.1

commit v7 on v6

--- a/solution.py
+++ b/solution.py
@@ -108,9 +108,11 @@
 
 
 def early_kernel(
-    x_ref, b_ref, c_ref, xt_ref, bt_ref, ct_ref, dt_ref, shrink_ref, speed_ref,
-    x_out, b_out, c_out, cum_ref, weight_ref, mask_ref, x_room, b_room, c_room,
+    x_ref, b_ref, c_ref, xt_ref, bt_ref, ct_ref, dt_ref, shrink_ref, speed_ref, w_ref,
+    x_out, b_out, c_out, cum_ref, weight_ref, mask_ref, w_out, x_room, b_room, c_room, sem,
 ):
+    copy = pltpu.make_async_copy(w_ref.at[0 : w_out.shape[0]], w_out, sem)
+    copy.start()
     for src_ref, taps_ref, out_ref, room in (
         (x_ref, xt_ref, x_out, x_room), (b_ref, bt_ref, b_out, b_room), (c_ref, ct_ref, c_out, c_room)
     ):
@@ -138,6 +140,7 @@
     for h in range(HEADS):
         away = columns[:, h * BLOCK : (h + 1) * BLOCK] - cum[h : h + 1, :]
         mask_ref[h] = jnp.exp(jnp.where(causal, away, -jnp.inf)) * steps[h : h + 1, :]
+    copy.wait()
 
 
 def local_kernel(
@@ -145,7 +148,8 @@
     up_ref, down_ref, skip_ref, w_ref,
     pre_ref, query_ref, send_ref, w_out, x_room, b_room, c_room, sem,
 ):
-    copy = pltpu.make_async_copy(w_ref, w_out, sem)
+    half = w_out.shape[0]
+    copy = pltpu.make_async_copy(w_ref.at[half : 2 * half], w_out, sem)
     copy.start()
     rows = []
     lane = 0
@@ -227,48 +231,53 @@
             state = state * factor(step) + more
 
 
-def gate_kernel(pre_ref, query_ref, cum_ref, inc_ref, gate_ref, gain_ref, w_ref, out_ref):
+def gate_kernel(pre_ref, query_ref, cum_ref, inc_ref, gate_ref, gain_ref, upper_ref, lower_ref, out_ref):
     inc = inc_ref[...].reshape(WIDTH, STATE)
     arriving = dot(query_ref[...], inc, ((1,), (1,))) * spread(jnp.exp(cum_ref[...]), HEAD_DIM)
     gated = (pre_ref[...] + arriving) * silu(gate_ref[...].astype(f32))
     scale = lax.rsqrt(jnp.mean(gated * gated, axis=-1, keepdims=True) + EPSILON)
     heads_out = (gated * scale * gain_ref[...]).astype(bf16)
-    out = dot(heads_out, w_ref[...], ((1,), (0,))).astype(bf16)
-    out_ref[...] = out.reshape(out_ref.shape)
+    half = upper_ref.shape[0]
+    out = dot(heads_out[:, 0:half], upper_ref[...], ((1,), (0,)))
+    out = out + dot(heads_out[:, half : 2 * half], lower_ref[...], ((1,), (0,)))
+    out_ref[...] = out.astype(bf16).reshape(out_ref.shape)
 
 
 def norm_kernel(got_ref, skip_ref, gain_ref, own_ref, copies_ref):
     total = got_ref[0].astype(f32)
     for k in range(1, got_ref.shape[0]):
         total = total + got_ref[k].astype(f32)
+    total = total.reshape(own_ref.shape)
     own = (skip_ref[...].astype(f32) + total.astype(bf16).astype(f32)).astype(bf16)
     own_ref[...] = own
     wide = own.astype(f32)
     scale = lax.rsqrt(jnp.mean(wide * wide, axis=-1, keepdims=True) + EPSILON)
     normed = (wide * scale * gain_ref[...]).astype(bf16)
     for k in range(copies_ref.shape[0]):
-        copies_ref[k] = normed
+        copies_ref[k] = normed.reshape(copies_ref.shape[1:])
 
 
 def mlp_kernel(rows_ref, w_ref, out_ref, w_room, sems):
     halves, shards, inner, slabs, each_depth, lanes = w_ref.shape
-    pieces = sems.shape[1]
+    pieces = sems.shape[2]
     take = shards // pieces
     size = take * inner * each_depth
     copies = []
-    for j in range(pieces):
-        for k in range(halves):
-            part = pl.ds(j * take, take)
-            copy = pltpu.make_async_copy(w_ref.at[k, part], w_room.at[k, part], sems.at[k, j])
-            copy.start()
-            copies.append(copy)
+    for part in range(2):
+        some = pl.ds(part * (slabs // 2), slabs // 2)
+        for j in range(pieces):
+            for k in range(halves):
+                place = (k, pl.ds(j * take, take), slice(None), some)
+                copy = pltpu.make_async_copy(w_ref.at[place], w_room.at[place], sems.at[part, k, j])
+                copy.start()
+                copies.append(copy)
 
     def piece(k, j, first):
         parts = [w_room[k, j * take : (j + 1) * take, :, n, :, :] for n in (first, first + 1)]
         return jnp.concatenate([p.reshape(size, lanes) for p in parts], axis=1)
 
-    count, each, depth = rows_ref.shape
-    rows = rows_ref[...].reshape(count * each, depth)
+    depth = rows_ref.shape[-1]
+    rows = rows_ref[...].reshape(-1, depth)
     lifted = [None] * halves
     for j in range(pieces):
         for k in range(halves):
@@ -282,15 +291,17 @@
     for j in range(pieces):
         total = None
         for k in range(halves):
+            copies[(pieces + j) * halves + k].wait()
             part = dot(hidden[k], piece(k, j, slabs // 2), ((1,), (1,)))
             total = part if total is None else total + part
-        out_ref[:, :, j * size : (j + 1) * size] = total.astype(bf16).reshape(count, each, size)
+        out_ref[:, :, :, j * size : (j + 1) * size] = total.astype(bf16).reshape(*out_ref.shape[:3], size)
 
 
 def final_kernel(got_ref, own_ref, out_ref):
     total = got_ref[0].astype(f32)
     for k in range(1, got_ref.shape[0]):
         total = total + got_ref[k].astype(f32)
+    total = total.reshape(own_ref.shape)
     out_ref[...] = (own_ref[...].astype(f32) + total.astype(bf16).astype(f32)).astype(bf16)
 
 
@@ -318,6 +329,7 @@
     ntp = lax.axis_size("x") * lax.axis_size("c")
     nrows = ny * lax.axis_size("x")
     own_count, width = skip_stream_entering.shape
+    own_tiles = (own_count // 8, 8, width)
     depth, units = widening_matrix.shape
     shard = 2 * depth * units // ny // STATE
 
@@ -330,7 +342,8 @@
         interpret=INTERPRET,
     )(content_signal_matrix, writer_signal_matrix, reader_signal_matrix)
     rim = lax.ppermute(rim, SP, [(k, k + 1) for k in range(nsp - 1)])
-    *sums, cum, weight, mask = call(
+    half = (blend_result_matrix.shape[0] // 2, width)
+    *sums, cum, weight, mask, upper = call(
         early_kernel,
         [
             shape((BLOCK, WIDTH), f32),
@@ -339,9 +352,11 @@
             shape((HEADS, BLOCK), f32),
             shape((BLOCK, WIDTH), f32),
             shape((HEADS, BLOCK, BLOCK), f32),
+            shape(half, bf16),
         ],
-        [VMEM] * 8 + [SMEM],
-        [pltpu.VMEM((RIM + BLOCK, n), f32) for n in (WIDTH, STATE, STATE)],
+        [VMEM] * 8 + [SMEM, HBM],
+        [pltpu.VMEM((RIM + BLOCK, n), f32) for n in (WIDTH, STATE, STATE)] + [pltpu.SemaphoreType.DMA(())],
+        compiler_params=pltpu.CompilerParams(vmem_limit_bytes=56 << 20),
     )(
         content_signal_matrix,
         writer_signal_matrix,
@@ -352,6 +367,7 @@
         interval_before_softplus,
         extra_log_shrink,
         log_forget_speed,
+        blend_result_matrix,
     )
 
     def whole(value):
@@ -363,12 +379,12 @@
     kept = [near(value) for value in (*sums, cum, weight, mask)]
     outs = [
         shape((BLOCK, WIDTH), f32),
-        jax.ShapeDtypeStruct((BLOCK, STATE), bf16),
+        shape((BLOCK, STATE), bf16),
         shape((ny, shard + PAIR + TAIL, STATE), bf16),
-        shape(blend_result_matrix.shape, bf16),
+        shape(half, bf16),
     ]
     narrowing = narrowing_matrix.T
-    pre, query, send, projection = pl.pallas_call(
+    pre, query, send, lower = pl.pallas_call(
         local_kernel,
         grid=(1,),
         out_shape=outs,
@@ -406,30 +422,31 @@
     incoming = exchange(before, "y")
     mixed = call(
         gate_kernel,
-        shape((ntp, own_count, width), bf16),
-        [VMEM] * 7,
+        shape((ntp, *own_tiles), bf16),
+        [VMEM] * 8,
         compiler_params=ROOM,
     )(
         near(pre),
-        query,
-        cum,
+        near(query),
+        near(cum),
         near(incoming),
         multiplier_signal,
         cluster_scaling_vector.reshape(1, -1),
-        near(projection),
+        near(upper),
+        near(lower),
     )
     mixed = exchange(mixed, TP)
     own, copies = call(
         norm_kernel,
-        [shape((own_count, width), bf16), shape((nrows, own_count, width), bf16)],
+        [shape((own_count, width), bf16), shape((nrows, *own_tiles), bf16)],
         [VMEM] * 3,
     )(near(mixed), skip_stream_entering, feature_blend_scaling.reshape(1, -1))
     rows = exchange(copies, ROWS)
     out = call(
         mlp_kernel,
-        shape((nrows, own_count, width), bf16),
+        shape((nrows, *own_tiles), bf16),
         [VMEM, HBM],
-        [pltpu.VMEM(weights.shape, bf16), pltpu.SemaphoreType.DMA((weights.shape[0], 4))],
+        [pltpu.VMEM(weights.shape, bf16), pltpu.SemaphoreType.DMA((2, weights.shape[0], 4))],
     )(near(rows), weights)
     out = exchange(out, ROWS)
     return call(final_kernel, jax.ShapeDtypeStruct((own_count, width), bf16), [VMEM] * 2)(near(out), near(own))

time: 145 us -> 144 us (level)
  no operation moved by 1% of the time
where the time goes in v7:
time: 144 us; the launch traced here: 142 us
  blocking collectives  111 us (77%)
  between operations  13.5 us (9%)
  Pallas kernels  13.3 us (9%)
  starting transfers between devices  4.14 us (3%)
    all_to_all x7, blocking collectives, exchange(): return lax.all_to_all(value, axes, split_axis=0, concat_axis=0, tiled=True)  111 us
    pallas_call x1, Pallas kernels, layer(): call(mlp_kernel, shape((nrows, *own_tiles), bf16), [VMEM, HBM], [pltpu.VM...  4.18 us
    ppermute x1, starting transfers between devices, layer(): rim = lax.ppermute(rim, SP, [(k, k + 1) for k in range(nsp - 1)])  4.14 us
  transfers between devices with their start and end apart: 2, of which 0 were waited for; matrix products, arithmetic and copies ran while one was open for 0% of the time, Pallas kernels for 3%

profile of v7, /device:TPU:1, one launch (start us, length us, event | category | flops | bytes accessed | tf_op | source)
XLA Modules:
  0.0 142.4 jit_solution(5532744820736391732)
XLA Ops:
  6.5 0.0 all-gather.2.cloned.1.call-start
  6.5 0.7 shard_map.163
  7.3 0.0 copy-start
  7.3 0.0 copy-start.1
  7.3 4.1 %collective-permute-start = (bf16[8,768]{1,0:T(8,128)(2,1)S(1)}, bf16[8,768]{1,0:T(8,128)(2,1)S(1)}, u32[]{:S(2)}, u32[]{:S(2)}) collective-permute-start(bf16[8,768]{1,0:T(8,128)(2,1)S(1)} %shard_map.163), channel_id=1, source_target_pairs={{0,8},{8,16},{16,24},{24,32},{32,40},{40,48},{48,56},{56,64},{64,7... | collective-permute-start | bytes 36872 | tf_op jit(solution)/shard_map/ppermute | solution.py:344
  11.4 2.7 %shard_map.164 = (f32[128,512]{1,0:T(8,128)S(1)}, f32[128,128]{1,0:T(8,128)S(1)}, f32[128,128]{1,0:T(8,128)S(1)}, f32[8,128]{1,0:T(8,128)S(1)}, f32[128,512]{1,0...) custom-call(bf16[128,512]{1,0:T(8,128)(2,1)} %x_ref.5, bf16[128,128]{1,0:T(8,128)(2,1)} %b_ref.5, ...), custom_call_target="tpu_custom_call" | custom-call | tf_op jit(solution)/shard_map/pallas_call | solution.py:346
  14.1 0.0 collective-permute-done.rim_ref
  14.1 2.2 %shard_map.165 = (f32[128,512]{1,0:T(8,128)S(1)}, bf16[128,128]{1,0:T(8,128)(2,1)S(1)}, bf16[4,272,128]{2,1,0:T(8,128)(2,1)S(1)}, bf16[256,2048]{1,0:T(8,128)(2,1)S(1)}) custom-call(bf16[128,512]{1,0:T(8,128)(2,1)} %x_ref.5, bf16[128,128]{1,0:T(8,128)(2,1)} %b_ref.5, bf16[128,128]{1,0:T(8,128)(2,1)} %c_ref.5, ...), custom_call_target="tpu_custom_call" | custom-call | tf_op jit(solution)/shard_map/pallas_call | solution.py:387
  16.3 9.4 %all_to_all.35.got_ref.rows_ref = bf16[4,272,128]{2,1,0:T(8,128)(2,1)S(1)} all-to-all(bf16[4,272,128]{2,1,0:T(8,128)(2,1)S(1)} %get-tuple-element.31), channel_id=1, replica_groups=mesh['zh'=4,'zl'=4,'y'=4,'x'=4,'c'=2] {'y'}, dimensions={0} | all-to-all | bytes 557056 | tf_op jit(solution)/shard_map/all_to_all | solution.py:53
  25.8 0.7 shard_map.166
  26.4 0.0 all-gather.2.cloned.1.call-update
  26.4 12.1 %all_to_all.36.got_ref = bf16[4,144,128]{2,1,0:T(8,128)(2,1)S(1)} all-to-all(bf16[4,144,128]{2,1,0:T(8,128)(2,1)S(1)} %get-tuple-element.32), channel_id=1, replica_groups=mesh['zh'=4,'zl'=4,'y'=4,'x'=4,'c'=2] {'zl'}, dimensions={0} | all-to-all | bytes 294912 | tf_op jit(solution)/shard_map/all_to_all | solution.py:53
  38.6 0.1 shard_map.167
  38.6 25.6 %all_to_all.37.got_ref = bf16[4,144,128]{2,1,0:T(8,128)(2,1)S(1)} all-to-all(bf16[4,144,128]{2,1,0:T(8,128)(2,1)S(1)} %get-tuple-element.33), channel_id=1, replica_groups=mesh['zh'=4,'zl'=4,'y'=4,'x'=4,'c'=2] {'zh'}, dimensions={0} | all-to-all | bytes 294912 | tf_op jit(solution)/shard_map/all_to_all | solution.py:53
  64.2 0.1 shard_map.168
  64.3 7.2 %all_to_all.38.inc_ref = bf16[4,128,128]{2,1,0:T(8,128)(2,1)S(1)} all-to-all(bf16[4,128,128]{2,1,0:T(8,128)(2,1)S(1)} %shard_map.168), channel_id=1, replica_groups=mesh['zh'=4,'zl'=4,'y'=4,'x'=4,'c'=2] {'y'}, dimensions={0} | all-to-all | bytes 262144 | tf_op jit(solution)/shard_map/all_to_all | solution.py:53
  71.5 0.0 copy-done
  71.5 0.0 copy-done.1
  71.5 0.9 shard_map.169
  72.4 20.2 %all_to_all.39.got_ref = bf16[8,2,8,2048]{3,2,1,0:T(8,128)(2,1)S(1)} all-to-all(bf16[8,2,8,2048]{3,2,1,0:T(8,128)(2,1)S(1)} %shard_map.169), channel_id=1, replica_groups=mesh['zh'=4,'zl'=4,'y'=4,'x'=4,'c'=2] {'x','c'}, dimensions={0} | all-to-all | bytes 1048576 | tf_op jit(solution)/shard_map/all_to_all | solution.py:53
  92.6 1.1 shard_map.170
  93.7 18.6 %all_to_all.40.rows_ref = bf16[16,2,8,2048]{3,2,1,0:T(8,128)(2,1)S(1)} all-to-all(bf16[16,2,8,2048]{3,2,1,0:T(8,128)(2,1)S(1)} %get-tuple-element.38), channel_id=1, replica_groups=mesh['zh'=4,'zl'=4,'y'=4,'x'=4,'c'=2] {'y','x'}, dimensions={0} | all-to-all | bytes 2097152 | tf_op jit(solution)/shard_map/all_to_all | solution.py:53
  112.3 0.0 all-gather.2.cloned.1.call-done
  112.3 4.2 %shard_map.171 = bf16[16,2,8,2048]{3,2,1,0:T(8,128)(2,1)S(1)} custom-call(bf16[16,2,8,2048]{3,2,1,0:T(8,128)(2,1)S(1)} %all_to_all.40.rows_ref, bf16[2,16,4,4,32,128]{5,4,3,2,1,0:T(8,128)(2,1)} %bitcast.6), custom_call_target="tpu_custom_call" | custom-call | tf_op jit(solution)/shard_map/pallas_call | solution.py:445
  116.5 18.3 %all_to_all.41.got_ref = bf16[16,2,8,2048]{3,2,1,0:T(8,128)(2,1)S(1)} all-to-all(bf16[16,2,8,2048]{3,2,1,0:T(8,128)(2,1)S(1)} %shard_map.171), channel_id=1, replica_groups=mesh['zh'=4,'zl'=4,'y'=4,'x'=4,'c'=2] {'y','x'}, dimensions={0} | all-to-all | bytes 2097152 | tf_op jit(solution)/shard_map/all_to_all | solution.py:53
  134.8 0.8 shard_map.172
Async XLA Ops:
  6.5 105.8 %all-gather.2.cloned.1.call-start = ((), (), s32[]{:S(2)}) async-start(), calls=%async_computation.7 | async-start | bytes 4325376 | tf_op jit(solution)/shard_map/all_gather | solution.py:409
  7.3 64.2 %copy-start = (bf16[128,512]{1,0:T(8,128)(2,1)S(1)}, bf16[128,512]{1,0:T(8,128)(2,1)}, u32[]{:S(2)}) copy-start(bf16[128,512]{1,0:T(8,128)(2,1)} %gate_ref.1) | copy-start | bytes 393220
  7.3 64.2 %copy-start.1 = (f32[512]{0:T(512)S(1)}, f32[512]{0:T(512)}, u32[]{:S(2)}) copy-start(f32[512]{0:T(512)} %param.29) | copy-start | bytes 6148
  7.3 6.8 %collective-permute-start = (bf16[8,768]{1,0:T(8,128)(2,1)S(1)}, bf16[8,768]{1,0:T(8,128)(2,1)S(1)}, u32[]{:S(2)}, u32[]{:S(2)}) collective-permute-start(bf16[8,768]{1,0:T(8,128)(2,1)S(1)} %shard_map.163), channel_id=1, source_target_pairs={{0,8},{8,16},{16,24},{24,32},{32,40},{40,48},{48,56},{56,64},{64,7... | collective-permute-start | bytes 36872 | tf_op jit(solution)/shard_map/ppermute | solution.py:344
Sparse Core Ops, SparseCore 0:
  26.6 81.1 all-gather.1

commit v8 on v4

--- a/solution.py
+++ b/solution.py
@@ -70,17 +70,15 @@
     return value / (1.0 + jnp.exp(-value))
 
 
-def convolve(src_ref, rim, taps_ref, room):
-    room[0:RIM, :] = rim.astype(f32)
-    room[RIM : RIM + BLOCK, :] = src_ref[...].astype(f32)
+def convolve(room, taps_ref, count):
     taps = taps_ref[...].astype(f32)
     width = taps.shape[0]
     total = None
     for k in range(width):
         start = RIM - width + 1 + k
-        term = room[start : start + BLOCK, :] * taps[k : k + 1, :]
+        term = room[start : start + count, :] * taps[k : k + 1, :]
         total = term if total is None else total + term
-    return silu(total)
+    return total
 
 
 def put_state(ref, place, start, state, log):
@@ -105,16 +103,16 @@
     rim_ref[:, WIDTH + STATE : WIDTH + 2 * STATE] = c_ref[...]
 
 
-def local_kernel(
-    slices, x_ref, b_ref, c_ref, rim_ref, xt_ref, bt_ref, ct_ref, dt_ref, shrink_ref, up_ref, down_ref, speed_ref, skip_ref, w_ref,
-    pre_ref, query_ref, cum_ref, send_ref, w_out, x_room, b_room, c_room, sem,
+def early_kernel(
+    x_ref, b_ref, c_ref, xt_ref, bt_ref, ct_ref, dt_ref, shrink_ref, speed_ref,
+    x_out, b_out, c_out, cum_ref, weight_ref, mask_ref, x_room, b_room, c_room,
 ):
-    copy = pltpu.make_async_copy(w_ref, w_out, sem)
-    copy.start()
-    values = convolve(x_ref, rim_ref[:, 0:WIDTH], xt_ref, x_room)
-    keys = convolve(b_ref, rim_ref[:, WIDTH : WIDTH + STATE], bt_ref, b_room).astype(bf16)
-    query = convolve(c_ref, rim_ref[:, WIDTH + STATE : WIDTH + 2 * STATE], ct_ref, c_room).astype(bf16)
-    query_ref[...] = query
+    for src_ref, taps_ref, out_ref, room in (
+        (x_ref, xt_ref, x_out, x_room), (b_ref, bt_ref, b_out, b_room), (c_ref, ct_ref, c_out, c_room)
+    ):
+        room[0:RIM, :] = jnp.zeros((RIM, room.shape[1]), f32)
+        room[RIM : RIM + BLOCK, :] = src_ref[...].astype(f32)
+        out_ref[...] = convolve(room, taps_ref, BLOCK)
     before = dt_ref[...]
     steps = jnp.maximum(before, 0.0) + jnp.log1p(jnp.exp(-jnp.abs(before)))
     head = lax.broadcasted_iota(jnp.int32, (HEADS, BLOCK), 0)
@@ -128,10 +126,35 @@
         cum = cum + jnp.where(token >= reach, pltpu.roll(cum, reach, 1), 0.0)
         reach *= 2
     cum_ref[...] = cum
-    last = cum[:, BLOCK - 1 : BLOCK]
-    weight = steps * jnp.exp(last - cum)
-    weighted = (values * spread(weight, HEAD_DIM)).astype(bf16)
-    state = dot(weighted, keys, ((0,), (0,)))
+    weight_ref[...] = spread(steps * jnp.exp(cum[:, BLOCK - 1 : BLOCK] - cum), HEAD_DIM)
+    columns = spread(cum, BLOCK)
+    later = lax.broadcasted_iota(jnp.int32, (BLOCK, BLOCK), 0)
+    earlier = lax.broadcasted_iota(jnp.int32, (BLOCK, BLOCK), 1)
+    causal = later >= earlier
+    for h in range(HEADS):
+        away = columns[:, h * BLOCK : (h + 1) * BLOCK] - cum[h : h + 1, :]
+        mask_ref[h] = jnp.exp(jnp.where(causal, away, -jnp.inf)) * steps[h : h + 1, :]
+
+
+def local_kernel(
+    slices, x_ref, b_ref, c_ref, rim_ref, xt_ref, bt_ref, ct_ref, x_sum, b_sum, c_sum, cum_ref, weight_ref, mask_ref,
+    up_ref, down_ref, skip_ref,
+    pre_ref, query_ref, send_ref, x_room, b_room, c_room,
+):
+    rows = []
+    lane = 0
+    for src_ref, taps_ref, sum_ref, room in (
+        (x_ref, xt_ref, x_sum, x_room), (b_ref, bt_ref, b_sum, b_room), (c_ref, ct_ref, c_sum, c_room)
+    ):
+        room[0:RIM, :] = rim_ref[:, lane : lane + room.shape[1]].astype(f32)
+        room[RIM : 2 * RIM, :] = src_ref[...].astype(f32)
+        lane += room.shape[1]
+        head = convolve(room, taps_ref, RIM)
+        rows.append(silu(jnp.concatenate([head, sum_ref[RIM:BLOCK, :]], axis=0)))
+    values, keys, query = rows[0], rows[1].astype(bf16), rows[2].astype(bf16)
+    query_ref[...] = query
+    last = cum_ref[:, BLOCK - 1 : BLOCK]
+    state = dot((values * weight_ref[...]).astype(bf16), keys, ((0,), (0,)))
     pieces = send_ref.shape[0]
     depth, units = up_ref.shape
     count = WIDTH // pieces
@@ -144,10 +167,6 @@
         h = place * count // HEAD_DIM
         put_state(send_ref, place, depth, state[place * count : (place + 1) * count, :], last[h : h + 1, :])
     scores = dot(query, keys, ((1,), (1,)))
-    columns = spread(cum, BLOCK)
-    later = lax.broadcasted_iota(jnp.int32, (BLOCK, BLOCK), 0)
-    earlier = lax.broadcasted_iota(jnp.int32, (BLOCK, BLOCK), 1)
-    causal = later >= earlier
     first = lax.broadcasted_iota(jnp.int32, (BLOCK, 2 * HEAD_DIM), 1) < HEAD_DIM
     for pair in range(HEADS // 2):
         lanes = slice(pair * 2 * HEAD_DIM, (pair + 1) * 2 * HEAD_DIM)
@@ -155,20 +174,18 @@
         two_low = two.astype(bf16)
         parts = []
         for h in (2 * pair, 2 * pair + 1):
-            away = columns[:, h * BLOCK : (h + 1) * BLOCK] - cum[h : h + 1, :]
-            mixing = scores * jnp.exp(jnp.where(causal, away, -jnp.inf)) * steps[h : h + 1, :]
+            mixing = scores * mask_ref[h]
             parts.append(dot(mixing.astype(bf16), two_low, ((1,), (0,))))
         within = jnp.where(first, parts[0], parts[1])
         skip = jnp.where(first, skip_ref[2 * pair], skip_ref[2 * pair + 1])
         pre_ref[:, lanes] = within + skip * two
-    copy.wait()
 
 
 def near_kernel(got_ref, shard_ref, send_ref):
     start = shard_ref.shape[1]
+    shard_ref[...] = got_ref[:, 0:start, :]
     state = log = None
     for k in range(got_ref.shape[0]):
-        shard_ref[k] = got_ref[k, 0:start, :]
         more, step = take_state(got_ref, k, start)
         state, log = (more, step) if state is None else (state * jnp.exp(step) + more, log + step)
     for k in range(send_ref.shape[0]):
@@ -198,37 +215,40 @@
     gated = (pre_ref[...] + arriving) * silu(gate_ref[...].astype(f32))
     scale = lax.rsqrt(jnp.mean(gated * gated, axis=-1, keepdims=True) + EPSILON)
     heads_out = (gated * scale * gain_ref[...]).astype(bf16)
-    out = dot(heads_out, w_ref[...], ((1,), (0,))).astype(bf16)
-    out_ref[...] = out.reshape(out_ref.shape)
+    out = dot(heads_out, w_ref[...], ((1,), (0,)))
+    out_ref[...] = out.astype(bf16).reshape(out_ref.shape)
 
 
 def norm_kernel(got_ref, skip_ref, gain_ref, own_ref, copies_ref):
     total = got_ref[0].astype(f32)
     for k in range(1, got_ref.shape[0]):
         total = total + got_ref[k].astype(f32)
+    total = total.reshape(own_ref.shape)
     own = (skip_ref[...].astype(f32) + total.astype(bf16).astype(f32)).astype(bf16)
     own_ref[...] = own
     wide = own.astype(f32)
     scale = lax.rsqrt(jnp.mean(wide * wide, axis=-1, keepdims=True) + EPSILON)
     normed = (wide * scale * gain_ref[...]).astype(bf16)
     for k in range(copies_ref.shape[0]):
-        copies_ref[k] = normed
+        copies_ref[k] = normed.reshape(copies_ref.shape[1:])
 
 
 def mlp_kernel(rows_ref, w_ref, out_ref, w_room, sems):
-    halves, pieces, slabs, size, lanes = w_ref.shape
+    halves, pieces, slabs, size, _ = w_ref.shape
     copies = []
-    for j in range(pieces):
-        for k in range(halves):
-            copy = pltpu.make_async_copy(w_ref.at[k, j], w_room.at[k, j], sems.at[k, j])
-            copy.start()
-            copies.append(copy)
+    for part in range(2):
+        some = pl.ds(part * (slabs // 2), slabs // 2)
+        for j in range(pieces):
+            for k in range(halves):
+                copy = pltpu.make_async_copy(w_ref.at[k, j, some], w_room.at[k, j, some], sems.at[part, k, j])
+                copy.start()
+                copies.append(copy)
 
     def piece(k, j, first):
         return jnp.concatenate([w_room[k, j, n] for n in range(first, first + slabs // 2)], axis=1)
 
-    count, each, depth = rows_ref.shape
-    rows = rows_ref[...].reshape(count * each, depth)
+    depth = rows_ref.shape[-1]
+    rows = rows_ref[...].reshape(-1, depth)
     lifted = [None] * halves
     for j in range(pieces):
         for k in range(halves):
@@ -242,19 +262,21 @@
     for j in range(pieces):
         total = None
         for k in range(halves):
+            copies[(pieces + j) * halves + k].wait()
             part = dot(hidden[k], piece(k, j, slabs // 2), ((1,), (1,)))
             total = part if total is None else total + part
-        out_ref[:, :, j * size : (j + 1) * size] = total.astype(bf16).reshape(count, each, size)
+        out_ref[:, :, :, j * size : (j + 1) * size] = total.astype(bf16).reshape(*out_ref.shape[:3], size)
 
 
 def final_kernel(got_ref, own_ref, out_ref):
     total = got_ref[0].astype(f32)
     for k in range(1, got_ref.shape[0]):
         total = total + got_ref[k].astype(f32)
+    total = total.reshape(own_ref.shape)
     out_ref[...] = (own_ref[...].astype(f32) + total.astype(bf16).astype(f32)).astype(bf16)
 
 
-def per_device(
+def layer(
     skip_stream_entering,
     content_signal_matrix,
     writer_signal_matrix,
@@ -278,7 +300,8 @@
     ntp = lax.axis_size("x") * lax.axis_size("c")
     nrows = ny * lax.axis_size("x")
     own_count, width = skip_stream_entering.shape
-    depth, units = widening_matrix.shape
+    own_tiles = (own_count // 8, 8, width)
+    depth, _ = widening_matrix.shape
     pieces = nzl * ny
     count = WIDTH // pieces
 
@@ -289,35 +312,61 @@
         in_specs=[pl.BlockSpec((RIM, n), lambda i: (BLOCK // RIM - 1, 0)) for n in (WIDTH, STATE, STATE)],
         out_specs=pl.BlockSpec((RIM, WIDTH + 2 * STATE), lambda i: (0, 0)),
         interpret=INTERPRET,
+        compiler_params=pltpu.CompilerParams(vmem_limit_bytes=54 << 20),
     )(content_signal_matrix, writer_signal_matrix, reader_signal_matrix)
     rim = lax.ppermute(rim, SP, [(k, k + 1) for k in range(nsp - 1)])
-    pre, query, cum, send, projection = call(
-        functools.partial(local_kernel, ny),
+    *sums, cum, weight, mask = call(
+        early_kernel,
         [
             shape((BLOCK, WIDTH), f32),
-            shape((BLOCK, STATE), bf16),
+            shape((BLOCK, STATE), f32),
+            shape((BLOCK, STATE), f32),
             shape((HEADS, BLOCK), f32),
-            shape((pieces, depth + count + TAIL, STATE), bf16),
-            shape(blend_result_matrix.shape, bf16),
+            shape((BLOCK, WIDTH), f32),
+            shape((HEADS, BLOCK, BLOCK), f32),
         ],
-        [VMEM] * 11 + [SMEM] * 2 + [HBM],
-        [pltpu.VMEM((RIM + BLOCK, n), f32) for n in (WIDTH, STATE, STATE)] + [pltpu.SemaphoreType.DMA(())],
+        [VMEM] * 8 + [SMEM],
+        [pltpu.VMEM((RIM + BLOCK, n), f32) for n in (WIDTH, STATE, STATE)],
+        compiler_params=pltpu.CompilerParams(vmem_limit_bytes=54 << 20),
     )(
         content_signal_matrix,
         writer_signal_matrix,
         reader_signal_matrix,
-        near(rim),
         content_filter_coefs,
         writer_filter_coefs,
         reader_filter_coefs,
         interval_before_softplus,
         extra_log_shrink,
-        widening_matrix,
-        narrowing_matrix.T,
         log_forget_speed,
-        skip_path_factor,
-        blend_result_matrix,
     )
+
+    def whole(value):
+        zeros = (0,) * value.ndim
+        return pl.BlockSpec(value.shape, lambda i: zeros)
+
+    head_rows = (content_signal_matrix, writer_signal_matrix, reader_signal_matrix)
+    taps = (content_filter_coefs, writer_filter_coefs, reader_filter_coefs)
+    kept = [near(value) for value in (*sums, cum, weight, mask)]
+    outs = [
+        shape((BLOCK, WIDTH), f32),
+        shape((BLOCK, STATE), bf16),
+        shape((pieces, depth + count + TAIL, STATE), bf16),
+    ]
+    narrowing = narrowing_matrix.T
+    pre, query, send = pl.pallas_call(
+        functools.partial(local_kernel, ny),
+        grid=(1,),
+        out_shape=outs,
+        in_specs=[pl.BlockSpec((RIM, value.shape[1]), lambda i: (0, 0)) for value in head_rows]
+        + [VMEM]
+        + [whole(value) for value in taps]
+        + [VMEM] * len(kept)
+        + [whole(widening_matrix), whole(narrowing), SMEM],
+        out_specs=[VMEM] * 3,
+        scratch_shapes=[pltpu.VMEM((2 * RIM, n), f32) for n in (WIDTH, STATE, STATE)],
+        interpret=INTERPRET,
+        compiler_params=pltpu.CompilerParams(vmem_limit_bytes=54 << 20),
+    )(*head_rows, near(rim), *taps, *kept, widening_matrix, narrowing, skip_path_factor)
     got = near(exchange(send, NEAR))
     parts, send = call(
         near_kernel,
@@ -332,7 +381,7 @@
     incoming = exchange(before, NEAR)
     mixed = call(
         gate_kernel,
-        shape((ntp, own_count, width), bf16),
+        shape((ntp, *own_tiles), bf16),
         [VMEM] * 7,
         compiler_params=ROOM,
     )(
@@ -340,22 +389,22 @@
         near(query),
         near(cum),
         near(incoming),
-        multiplier_signal,
-        cluster_scaling_vector.reshape(1, -1),
-        near(projection),
+        near(multiplier_signal),
+        near(cluster_scaling_vector.reshape(1, -1)),
+        near(blend_result_matrix),
     )
     mixed = exchange(mixed, TP)
     own, copies = call(
         norm_kernel,
-        [shape((own_count, width), bf16), shape((nrows, own_count, width), bf16)],
+        [shape((own_count, width), bf16), shape((nrows, *own_tiles), bf16)],
         [VMEM] * 3,
     )(near(mixed), skip_stream_entering, feature_blend_scaling.reshape(1, -1))
     rows = exchange(copies, ROWS)
     out = call(
         mlp_kernel,
-        shape((nrows, own_count, width), bf16),
+        shape((nrows, *own_tiles), bf16),
         [VMEM, HBM],
-        [pltpu.VMEM(weights.shape, bf16), pltpu.SemaphoreType.DMA(weights.shape[:2])],
+        [pltpu.VMEM(weights.shape, bf16), pltpu.SemaphoreType.DMA((2, *weights.shape[:2]))],
     )(near(rows), weights)
     out = exchange(out, ROWS)
     return call(final_kernel, jax.ShapeDtypeStruct((own_count, width), bf16), [VMEM] * 2)(near(out), near(own))
@@ -382,6 +431,4 @@
         P(SP, TP),
         P(TP, SP),
     )
-    return jax.shard_map(
-        per_device, mesh=torus, in_specs=placed, out_specs=P(SP + TP, None), check_vma=False
-    )
+    return jax.shard_map(layer, mesh=torus, in_specs=placed, out_specs=P(SP + TP, None), check_vma=False)

time: 146 us -> 146 us (level)
  waiting for transfers between devices: 2.47 us -> 0.15 us
  blocking collectives: 115 us -> 113 us
  Pallas kernels: 10.8 us -> 12.5 us
  local copies, waits for them, and re-layouts: 0.01 us -> 1.6 us
    pallas_call x8 -> x9, Pallas kernels: 10.8 us -> 12.5 us  [the longest x1 4.18 us: layer(): call(mlp_kernel, shape((nrows, *own_tiles), bf16), [VMEM, HBM], [pltpu.VM...]
    unnamed x4 -> x6, local copies, waits for them, and re-layouts: 0.01 us -> 1.6 us
    all_gather x1, waiting for transfers between devices: 1.64 us -> 0.13 us  [layer(): lax.all_gather(parts.reshape(pieces * depth, STATE), ('c', 'zh', 'zl'), a...]
  transfers between devices with their start and end apart: 2 -> 2, of which waited for: 2 -> 1; matrix products, arithmetic and copies ran while one was open for 0% -> 0% of each run, Pallas kernels for 1% -> 3%
where the time goes in v8:
time: 146 us; the launch traced here: 145 us
  blocking collectives  113 us (77%)
  between operations  13.5 us (9%)
  Pallas kernels  12.5 us (9%)
  starting transfers between devices  4.01 us (3%)
  local copies, waits for them, and re-layouts  1.6 us (1%)
    all_to_all x6, blocking collectives, exchange(): return lax.all_to_all(value, axes, split_axis=0, concat_axis=0, tiled=True)  113 us
    pallas_call x1, Pallas kernels, layer(): call(mlp_kernel, shape((nrows, *own_tiles), bf16), [VMEM, HBM], [pltpu.VM...  4.18 us
    ppermute x1, starting transfers between devices, layer(): rim = lax.ppermute(rim, SP, [(k, k + 1) for k in range(nsp - 1)])  4.01 us
  transfers between devices with their start and end apart: 2, of which 1 were waited for; matrix products, arithmetic and copies ran while one was open for 0% of the time, Pallas kernels for 3%

profile of v8, /device:TPU:1, one launch (start us, length us, event | category | flops | bytes accessed | tf_op | source)
XLA Modules:
  0.0 145.0 jit_solution(13909078934913024226)
XLA Ops:
  6.5 0.0 copy-start
  6.5 0.0 all-gather.2.cloned.1.call-start
  6.5 0.9 shard_map.163
  7.4 4.0 %collective-permute-start = (bf16[8,768]{1,0:T(8,128)(2,1)S(1)}, bf16[8,768]{1,0:T(8,128)(2,1)S(1)}, u32[]{:S(2)}, u32[]{:S(2)}) collective-permute-start(bf16[8,768]{1,0:T(8,128)(2,1)S(1)} %shard_map.163), channel_id=1, source_target_pairs={{0,8},{8,16},{16,24},{24,32},{32,40},{40,48},{48,56},{56,64},{64,7... | collective-permute-start | bytes 36872 | tf_op jit(solution)/shard_map/ppermute | solution.py:317
  11.4 2.6 %shard_map.164 = (f32[128,512]{1,0:T(8,128)S(1)}, f32[128,128]{1,0:T(8,128)S(1)}, f32[128,128]{1,0:T(8,128)S(1)}, f32[8,128]{1,0:T(8,128)S(1)}, f32[128,512]{1,0:T(8,128)S(1)}, /*index=5*/f32[8,128,128]{2,1,0:T(8,128)S(1)}) custom-call(bf16[128,512]{1,0:T(8,128)(2,1)} %x_ref.5, bf16[128,128]{1,0:T(8,128)(2,1)} %b_ref.5, bf16[128,128]{1,0:T(8,128)(2,1)} %c_ref.5, ...), custom_call_target="tpu_custom_call" | custom-call | tf_op jit(solution)/shard_map/pallas_call | solution.py:318
  14.0 0.0 collective-permute-done.rim_ref
  14.0 1.4 shard_map.165
  15.5 19.6 %all_to_all.30.got_ref.near_ref = bf16[16,80,128]{2,1,0:T(8,128)(2,1)S(1)} all-to-all(bf16[16,80,128]{2,1,0:T(8,128)(2,1)S(1)} %get-tuple-element.26), channel_id=1, replica_groups=mesh['zh'=4,'zl'=4,'y'=4,'x'=4,'c'=2] {'zl','y'}, dimensions={0} | all-to-all | bytes 655360 | tf_op jit(solution)/shard_map/all_to_all | solution.py:55
  35.0 0.7 shard_map.166
  35.7 0.0 all-gather.2.cloned.1.call-update
  35.7 22.7 %all_to_all.31.got_ref = bf16[4,48,128]{2,1,0:T(8,128)(2,1)S(1)} all-to-all(bf16[4,48,128]{2,1,0:T(8,128)(2,1)S(1)} %get-tuple-element.27), channel_id=1, replica_groups=mesh['zh'=4,'zl'=4,'y'=4,'x'=4,'c'=2] {'zh'}, dimensions={0} | all-to-all | bytes 98304 | tf_op jit(solution)/shard_map/all_to_all | solution.py:55
  58.4 0.1 shard_map.167
  58.5 12.3 %all_to_all.32.inc_ref = bf16[16,32,128]{2,1,0:T(8,128)(2,1)S(1)} all-to-all(bf16[16,32,128]{2,1,0:T(8,128)(2,1)S(1)} %shard_map.167), channel_id=1, replica_groups=mesh['zh'=4,'zl'=4,'y'=4,'x'=4,'c'=2] {'zl','y'}, dimensions={0} | all-to-all | bytes 262144 | tf_op jit(solution)/shard_map/all_to_all | solution.py:55
  70.8 0.0 copy-done
  70.8 0.0 copy-start.1
  70.8 0.9 copy-done.1
  71.7 0.0 copy-start.2
  71.7 0.7 copy-done.2
  72.4 0.9 shard_map.168
  73.3 17.5 %all_to_all.33.got_ref = bf16[8,2,8,2048]{3,2,1,0:T(8,128)(2,1)S(1)} all-to-all(bf16[8,2,8,2048]{3,2,1,0:T(8,128)(2,1)S(1)} %shard_map.168), channel_id=1, replica_groups=mesh['zh'=4,'zl'=4,'y'=4,'x'=4,'c'=2] {'x','c'}, dimensions={0} | all-to-all | bytes 1048576 | tf_op jit(solution)/shard_map/all_to_all | solution.py:55
  90.7 1.1 shard_map.169
  91.8 18.8 %all_to_all.34.rows_ref = bf16[16,2,8,2048]{3,2,1,0:T(8,128)(2,1)S(1)} all-to-all(bf16[16,2,8,2048]{3,2,1,0:T(8,128)(2,1)S(1)} %get-tuple-element.28), channel_id=1, replica_groups=mesh['zh'=4,'zl'=4,'y'=4,'x'=4,'c'=2] {'y','x'}, dimensions={0} | all-to-all | bytes 2097152 | tf_op jit(solution)/shard_map/all_to_all | solution.py:55
  110.6 0.1 all-gather.2.cloned.1.call-done
  110.7 4.2 %shard_map.170 = bf16[16,2,8,2048]{3,2,1,0:T(8,128)(2,1)S(1)} custom-call(bf16[16,2,8,2048]{3,2,1,0:T(8,128)(2,1)S(1)} %all_to_all.34.rows_ref, bf16[2,4,4,512,128]{4,3,2,1,0:T(8,128)(2,1)} %bitcast.6), custom_call_target="tpu_custom_call" | custom-call | tf_op jit(solution)/shard_map/pallas_call | solution.py:403
  114.9 22.5 %all_to_all.35.got_ref = bf16[16,2,8,2048]{3,2,1,0:T(8,128)(2,1)S(1)} all-to-all(bf16[16,2,8,2048]{3,2,1,0:T(8,128)(2,1)S(1)} %shard_map.170), channel_id=1, replica_groups=mesh['zh'=4,'zl'=4,'y'=4,'x'=4,'c'=2] {'y','x'}, dimensions={0} | all-to-all | bytes 2097152 | tf_op jit(solution)/shard_map/all_to_all | solution.py:55
  137.4 0.8 shard_map.171
Async XLA Ops:
  6.5 64.3 %copy-start = (bf16[512,2048]{1,0:T(8,128)(2,1)S(1)}, bf16[512,2048]{1,0:T(8,128)(2,1)}, u32[]{:S(2)}) copy-start(bf16[512,2048]{1,0:T(8,128)(2,1)} %w_ref.1) | copy-start | bytes 6291460
  6.5 104.2 %all-gather.2.cloned.1.call-start = ((), (), s32[]{:S(2)}) async-start(), calls=%async_computation.6 | async-start | bytes 4325376 | tf_op jit(solution)/shard_map/all_gather | solution.py:377
  7.4 6.6 %collective-permute-start = (bf16[8,768]{1,0:T(8,128)(2,1)S(1)}, bf16[8,768]{1,0:T(8,128)(2,1)S(1)}, u32[]{:S(2)}, u32[]{:S(2)}) collective-permute-start(bf16[8,768]{1,0:T(8,128)(2,1)S(1)} %shard_map.163), channel_id=1, source_target_pairs={{0,8},{8,16},{16,24},{24,32},{32,40},{40,48},{48,56},{56,64},{64,7... | collective-permute-start | bytes 36872 | tf_op jit(solution)/shard_map/ppermute | solution.py:317
  70.8 0.9 copy-start.1
  71.7 0.7 copy-start.2
Sparse Core Ops, SparseCore 0:
  35.8 74.8 all-gather.1

commit v9 on v7

--- a/solution.py
+++ b/solution.py
@@ -16,7 +16,7 @@
 TAIL = 16
 SP = ("zh", "zl", "y")
 TP = ("x", "c")
-ROWS = ("y", "x")
+ROWS = ("x", "y")
 EPSILON = 1e-05
 INTERPRET = False
 ROOM = pltpu.CompilerParams(vmem_limit_bytes=16 << 20)
@@ -108,11 +108,9 @@
 
 
 def early_kernel(
-    x_ref, b_ref, c_ref, xt_ref, bt_ref, ct_ref, dt_ref, shrink_ref, speed_ref, w_ref,
-    x_out, b_out, c_out, cum_ref, weight_ref, mask_ref, w_out, x_room, b_room, c_room, sem,
+    x_ref, b_ref, c_ref, xt_ref, bt_ref, ct_ref, dt_ref, shrink_ref, speed_ref,
+    x_out, b_out, c_out, cum_ref, weight_ref, mask_ref, x_room, b_room, c_room,
 ):
-    copy = pltpu.make_async_copy(w_ref.at[0 : w_out.shape[0]], w_out, sem)
-    copy.start()
     for src_ref, taps_ref, out_ref, room in (
         (x_ref, xt_ref, x_out, x_room), (b_ref, bt_ref, b_out, b_room), (c_ref, ct_ref, c_out, c_room)
     ):
@@ -140,17 +138,13 @@
     for h in range(HEADS):
         away = columns[:, h * BLOCK : (h + 1) * BLOCK] - cum[h : h + 1, :]
         mask_ref[h] = jnp.exp(jnp.where(causal, away, -jnp.inf)) * steps[h : h + 1, :]
-    copy.wait()
 
 
 def local_kernel(
     x_ref, b_ref, c_ref, rim_ref, xt_ref, bt_ref, ct_ref, x_sum, b_sum, c_sum, cum_ref, weight_ref, mask_ref,
-    up_ref, down_ref, skip_ref, w_ref,
-    pre_ref, query_ref, send_ref, w_out, x_room, b_room, c_room, sem,
+    up_ref, down_ref, skip_ref,
+    pre_ref, query_ref, send_ref, x_room, b_room, c_room,
 ):
-    half = w_out.shape[0]
-    copy = pltpu.make_async_copy(w_ref.at[half : 2 * half], w_out, sem)
-    copy.start()
     rows = []
     lane = 0
     for src_ref, taps_ref, sum_ref, room in (
@@ -187,7 +181,6 @@
         within = jnp.where(first, parts[0], parts[1])
         skip = jnp.where(first, skip_ref[2 * pair], skip_ref[2 * pair + 1])
         pre_ref[:, lanes] = within + skip * two
-    copy.wait()
 
 
 def row_kernel(got_ref, shard_ref, send_ref):
@@ -231,15 +224,13 @@
             state = state * factor(step) + more
 
 
-def gate_kernel(pre_ref, query_ref, cum_ref, inc_ref, gate_ref, gain_ref, upper_ref, lower_ref, out_ref):
+def gate_kernel(pre_ref, query_ref, cum_ref, inc_ref, gate_ref, gain_ref, w_ref, out_ref):
     inc = inc_ref[...].reshape(WIDTH, STATE)
     arriving = dot(query_ref[...], inc, ((1,), (1,))) * spread(jnp.exp(cum_ref[...]), HEAD_DIM)
     gated = (pre_ref[...] + arriving) * silu(gate_ref[...].astype(f32))
     scale = lax.rsqrt(jnp.mean(gated * gated, axis=-1, keepdims=True) + EPSILON)
     heads_out = (gated * scale * gain_ref[...]).astype(bf16)
-    half = upper_ref.shape[0]
-    out = dot(heads_out[:, 0:half], upper_ref[...], ((1,), (0,)))
-    out = out + dot(heads_out[:, half : 2 * half], lower_ref[...], ((1,), (0,)))
+    out = dot(heads_out, w_ref[...], ((1,), (0,)))
     out_ref[...] = out.astype(bf16).reshape(out_ref.shape)
 
 
@@ -268,9 +259,10 @@
         for j in range(pieces):
             for k in range(halves):
                 place = (k, pl.ds(j * take, take), slice(None), some)
-                copy = pltpu.make_async_copy(w_ref.at[place], w_room.at[place], sems.at[part, k, j])
-                copy.start()
-                copies.append(copy)
+                copies.append(pltpu.make_async_copy(w_ref.at[place], w_room.at[place], sems.at[part, k, j]))
+    count = pieces * halves
+    for copy in copies[:count]:
+        copy.start()
 
     def piece(k, j, first):
         parts = [w_room[k, j * take : (j + 1) * take, :, n, :, :] for n in (first, first + 1)]
@@ -282,6 +274,7 @@
     for j in range(pieces):
         for k in range(halves):
             copies[j * halves + k].wait()
+            copies[count + j * halves + k].start()
             part = dot(rows[:, j * size : (j + 1) * size], piece(k, j, 0), ((1,), (0,)))
             lifted[k] = part if lifted[k] is None else lifted[k] + part
     hidden = []
@@ -291,7 +284,7 @@
     for j in range(pieces):
         total = None
         for k in range(halves):
-            copies[(pieces + j) * halves + k].wait()
+            copies[count + j * halves + k].wait()
             part = dot(hidden[k], piece(k, j, slabs // 2), ((1,), (1,)))
             total = part if total is None else total + part
         out_ref[:, :, :, j * size : (j + 1) * size] = total.astype(bf16).reshape(*out_ref.shape[:3], size)
@@ -340,10 +333,10 @@
         in_specs=[pl.BlockSpec((RIM, n), lambda i: (BLOCK // RIM - 1, 0)) for n in (WIDTH, STATE, STATE)],
         out_specs=pl.BlockSpec((RIM, WIDTH + 2 * STATE), lambda i: (0, 0)),
         interpret=INTERPRET,
+        compiler_params=pltpu.CompilerParams(vmem_limit_bytes=54 << 20),
     )(content_signal_matrix, writer_signal_matrix, reader_signal_matrix)
     rim = lax.ppermute(rim, SP, [(k, k + 1) for k in range(nsp - 1)])
-    half = (blend_result_matrix.shape[0] // 2, width)
-    *sums, cum, weight, mask, upper = call(
+    *sums, cum, weight, mask = call(
         early_kernel,
         [
             shape((BLOCK, WIDTH), f32),
@@ -352,11 +345,10 @@
             shape((HEADS, BLOCK), f32),
             shape((BLOCK, WIDTH), f32),
             shape((HEADS, BLOCK, BLOCK), f32),
-            shape(half, bf16),
         ],
-        [VMEM] * 8 + [SMEM, HBM],
-        [pltpu.VMEM((RIM + BLOCK, n), f32) for n in (WIDTH, STATE, STATE)] + [pltpu.SemaphoreType.DMA(())],
-        compiler_params=pltpu.CompilerParams(vmem_limit_bytes=56 << 20),
+        [VMEM] * 8 + [SMEM],
+        [pltpu.VMEM((RIM + BLOCK, n), f32) for n in (WIDTH, STATE, STATE)],
+        compiler_params=pltpu.CompilerParams(vmem_limit_bytes=54 << 20),
     )(
         content_signal_matrix,
         writer_signal_matrix,
@@ -367,7 +359,6 @@
         interval_before_softplus,
         extra_log_shrink,
         log_forget_speed,
-        blend_result_matrix,
     )
 
     def whole(value):
@@ -381,10 +372,9 @@
         shape((BLOCK, WIDTH), f32),
         shape((BLOCK, STATE), bf16),
         shape((ny, shard + PAIR + TAIL, STATE), bf16),
-        shape(half, bf16),
     ]
     narrowing = narrowing_matrix.T
-    pre, query, send, lower = pl.pallas_call(
+    pre, query, send = pl.pallas_call(
         local_kernel,
         grid=(1,),
         out_shape=outs,
@@ -392,13 +382,12 @@
         + [VMEM]
         + [whole(value) for value in taps]
         + [VMEM] * len(kept)
-        + [whole(widening_matrix), whole(narrowing), SMEM, HBM],
-        out_specs=[VMEM] * 4,
-        scratch_shapes=[pltpu.VMEM((2 * RIM, n), f32) for n in (WIDTH, STATE, STATE)]
-        + [pltpu.SemaphoreType.DMA(())],
+        + [whole(widening_matrix), whole(narrowing), SMEM],
+        out_specs=[VMEM] * 3,
+        scratch_shapes=[pltpu.VMEM((2 * RIM, n), f32) for n in (WIDTH, STATE, STATE)],
         interpret=INTERPRET,
-        compiler_params=pltpu.CompilerParams(vmem_limit_bytes=56 << 20),
-    )(*head_rows, near(rim), *taps, *kept, widening_matrix, narrowing, skip_path_factor, blend_result_matrix)
+        compiler_params=pltpu.CompilerParams(vmem_limit_bytes=54 << 20),
+    )(*head_rows, near(rim), *taps, *kept, widening_matrix, narrowing, skip_path_factor)
     rows = near(exchange(send, "y"))
     parts, send = call(
         row_kernel,
@@ -423,7 +412,7 @@
     mixed = call(
         gate_kernel,
         shape((ntp, *own_tiles), bf16),
-        [VMEM] * 8,
+        [VMEM] * 7,
         compiler_params=ROOM,
     )(
         near(pre),
@@ -432,8 +421,7 @@
         near(incoming),
         multiplier_signal,
         cluster_scaling_vector.reshape(1, -1),
-        near(upper),
-        near(lower),
+        near(blend_result_matrix),
     )
     mixed = exchange(mixed, TP)
     own, copies = call(

time: 144 us -> 143 us (level)
  no operation moved by 1% of the time
where the time goes in v9:
time: 143 us; the launch traced here: 141 us
  blocking collectives  111 us (78%)
  between operations  13.5 us (9%)
  Pallas kernels  12.6 us (9%)
  starting transfers between devices  4.01 us (3%)
    all_to_all x7, blocking collectives, exchange(): return lax.all_to_all(value, axes, split_axis=0, concat_axis=0, tiled=True)  111 us
    pallas_call x1, Pallas kernels, layer(): call(mlp_kernel, shape((nrows, *own_tiles), bf16), [VMEM, HBM], [pltpu.VM...  4.19 us
    ppermute x1, starting transfers between devices, layer(): rim = lax.ppermute(rim, SP, [(k, k + 1) for k in range(nsp - 1)])  4.01 us
  transfers between devices with their start and end apart: 2, of which 0 were waited for; matrix products, arithmetic and copies ran while one was open for 0% of the time, Pallas kernels for 3%

profile of v9, /device:TPU:1, one launch (start us, length us, event | category | flops | bytes accessed | tf_op | source)
XLA Modules:
  0.0 141.1 jit_solution(14182754454142905967)
XLA Ops:
  6.5 0.0 copy-start.2
  6.5 0.0 copy-start.1
  6.5 0.0 copy-start
  6.5 0.0 all-gather.2.cloned.1.call-start
  6.5 0.9 shard_map.163
  7.4 4.0 %collective-permute-start = (bf16[8,768]{1,0:T(8,128)(2,1)S(1)}, bf16[8,768]{1,0:T(8,128)(2,1)S(1)}, u32[]{:S(2)}, u32[]{:S(2)}) collective-permute-start(bf16[8,768]{1,0:T(8,128)(2,1)S(1)} %shard_map.163), channel_id=1, source_target_pairs={{0,8},{8,16},{16,24},{24,32},{32,40},{40,48},{48,56},{56,64},{64,7... | collective-permute-start | bytes 36872 | tf_op jit(solution)/shard_map/ppermute | solution.py:338
  11.4 2.6 %shard_map.164 = (f32[128,512]{1,0:T(8,128)S(1)}, f32[128,128]{1,0:T(8,128)S(1)}, f32[128,128]{1,0:T(8,128)S(1)}, f32[8,128]{1,0:T(8,128)S(1)}, f32[128,512]{1,0:T(8,128)S(1)}, /*index=5*/f32[8,128,128]{2,1,0:T(8,128)S(1)}) custom-call(bf16[128,512]{1,0:T(8,128)(2,1)} %x_ref.5, bf16[128,128]{1,0:T(8,128)(2,1)} %b_ref.5, bf16[128,128]{1,0:T(8,128)(2,1)} %c_ref.5, ...), custom_call_target="tpu_custom_call" | custom-call | tf_op jit(solution)/shard_map/pallas_call | solution.py:339
  14.0 0.0 collective-permute-done.rim_ref
  14.0 1.4 shard_map.165
  15.5 9.4 %all_to_all.35.got_ref.rows_ref = bf16[4,272,128]{2,1,0:T(8,128)(2,1)S(1)} all-to-all(bf16[4,272,128]{2,1,0:T(8,128)(2,1)S(1)} %get-tuple-element.29), channel_id=1, replica_groups=mesh['zh'=4,'zl'=4,'y'=4,'x'=4,'c'=2] {'y'}, dimensions={0} | all-to-all | bytes 557056 | tf_op jit(solution)/shard_map/all_to_all | solution.py:53
  24.9 0.7 shard_map.166
  25.5 0.0 all-gather.2.cloned.1.call-update
  25.6 12.1 %all_to_all.36.got_ref = bf16[4,144,128]{2,1,0:T(8,128)(2,1)S(1)} all-to-all(bf16[4,144,128]{2,1,0:T(8,128)(2,1)S(1)} %get-tuple-element.30), channel_id=1, replica_groups=mesh['zh'=4,'zl'=4,'y'=4,'x'=4,'c'=2] {'zl'}, dimensions={0} | all-to-all | bytes 294912 | tf_op jit(solution)/shard_map/all_to_all | solution.py:53
  37.7 0.1 shard_map.167
  37.8 25.6 %all_to_all.37.got_ref = bf16[4,144,128]{2,1,0:T(8,128)(2,1)S(1)} all-to-all(bf16[4,144,128]{2,1,0:T(8,128)(2,1)S(1)} %get-tuple-element.31), channel_id=1, replica_groups=mesh['zh'=4,'zl'=4,'y'=4,'x'=4,'c'=2] {'zh'}, dimensions={0} | all-to-all | bytes 294912 | tf_op jit(solution)/shard_map/all_to_all | solution.py:53
  63.4 0.1 shard_map.168
  63.5 7.2 %all_to_all.38.inc_ref = bf16[4,128,128]{2,1,0:T(8,128)(2,1)S(1)} all-to-all(bf16[4,128,128]{2,1,0:T(8,128)(2,1)S(1)} %shard_map.168), channel_id=1, replica_groups=mesh['zh'=4,'zl'=4,'y'=4,'x'=4,'c'=2] {'y'}, dimensions={0} | all-to-all | bytes 262144 | tf_op jit(solution)/shard_map/all_to_all | solution.py:53
  70.7 0.0 copy-done.2
  70.7 0.0 copy-done.1
  70.7 0.0 copy-done
  70.7 0.9 shard_map.169
  71.6 20.2 %all_to_all.39.got_ref = bf16[8,2,8,2048]{3,2,1,0:T(8,128)(2,1)S(1)} all-to-all(bf16[8,2,8,2048]{3,2,1,0:T(8,128)(2,1)S(1)} %shard_map.169), channel_id=1, replica_groups=mesh['zh'=4,'zl'=4,'y'=4,'x'=4,'c'=2] {'x','c'}, dimensions={0} | all-to-all | bytes 1048576 | tf_op jit(solution)/shard_map/all_to_all | solution.py:53
  91.8 1.1 shard_map.170
  92.9 18.1 %all_to_all.40.rows_ref = bf16[16,2,8,2048]{3,2,1,0:T(8,128)(2,1)S(1)} all-to-all(bf16[16,2,8,2048]{3,2,1,0:T(8,128)(2,1)S(1)} %get-tuple-element.34), channel_id=1, replica_groups=mesh['zh'=4,'zl'=4,'y'=4,'x'=4,'c'=2] {'x','y'}, dimensions={0} | all-to-all | bytes 2097152 | tf_op jit(solution)/shard_map/all_to_all | solution.py:53
  111.0 0.0 all-gather.2.cloned.1.call-done
  111.0 4.2 %shard_map.171 = bf16[16,2,8,2048]{3,2,1,0:T(8,128)(2,1)S(1)} custom-call(bf16[16,2,8,2048]{3,2,1,0:T(8,128)(2,1)S(1)} %all_to_all.40.rows_ref, bf16[2,16,4,4,32,128]{5,4,3,2,1,0:T(8,128)(2,1)} %bitcast.6), custom_call_target="tpu_custom_call" | custom-call | tf_op jit(solution)/shard_map/pallas_call | solution.py:433
  115.2 18.3 %all_to_all.41.got_ref = bf16[16,2,8,2048]{3,2,1,0:T(8,128)(2,1)S(1)} all-to-all(bf16[16,2,8,2048]{3,2,1,0:T(8,128)(2,1)S(1)} %shard_map.171), channel_id=1, replica_groups=mesh['zh'=4,'zl'=4,'y'=4,'x'=4,'c'=2] {'x','y'}, dimensions={0} | all-to-all | bytes 2097152 | tf_op jit(solution)/shard_map/all_to_all | solution.py:53
  133.5 0.8 shard_map.172
Async XLA Ops:
  6.5 64.2 %copy-start.2 = (f32[512]{0:T(512)S(1)}, f32[512]{0:T(512)}, u32[]{:S(2)}) copy-start(f32[512]{0:T(512)} %param.29) | copy-start | bytes 6148
  6.5 64.2 %copy-start.1 = (bf16[128,512]{1,0:T(8,128)(2,1)S(1)}, bf16[128,512]{1,0:T(8,128)(2,1)}, u32[]{:S(2)}) copy-start(bf16[128,512]{1,0:T(8,128)(2,1)} %gate_ref.1) | copy-start | bytes 393220
  6.5 64.2 %copy-start = (bf16[512,2048]{1,0:T(8,128)(2,1)S(1)}, bf16[512,2048]{1,0:T(8,128)(2,1)}, u32[]{:S(2)}) copy-start(bf16[512,2048]{1,0:T(8,128)(2,1)} %w_ref.1) | copy-start | bytes 6291460
  6.5 104.5 %all-gather.2.cloned.1.call-start = ((), (), s32[]{:S(2)}) async-start(), calls=%async_computation.7 | async-start | bytes 4325376 | tf_op jit(solution)/shard_map/all_gather | solution.py:398
  7.4 6.6 %collective-permute-start = (bf16[8,768]{1,0:T(8,128)(2,1)S(1)}, bf16[8,768]{1,0:T(8,128)(2,1)S(1)}, u32[]{:S(2)}, u32[]{:S(2)}) collective-permute-start(bf16[8,768]{1,0:T(8,128)(2,1)S(1)} %shard_map.163), channel_id=1, source_target_pairs={{0,8},{8,16},{16,24},{24,32},{32,40},{40,48},{48,56},{56,64},{64,7... | collective-permute-start | bytes 36872 | tf_op jit(solution)/shard_map/ppermute | solution.py:338
Sparse Core Ops, SparseCore 0:
  25.7 80.9 all-gather.1

commit v10 on v9

--- a/solution.py
+++ b/solution.py
@@ -250,19 +250,16 @@
 
 def mlp_kernel(rows_ref, w_ref, out_ref, w_room, sems):
     halves, shards, inner, slabs, each_depth, lanes = w_ref.shape
-    pieces = sems.shape[2]
+    pieces = sems.shape[1]
     take = shards // pieces
     size = take * inner * each_depth
     copies = []
-    for part in range(2):
-        some = pl.ds(part * (slabs // 2), slabs // 2)
-        for j in range(pieces):
-            for k in range(halves):
-                place = (k, pl.ds(j * take, take), slice(None), some)
-                copies.append(pltpu.make_async_copy(w_ref.at[place], w_room.at[place], sems.at[part, k, j]))
-    count = pieces * halves
-    for copy in copies[:count]:
-        copy.start()
+    for j in range(pieces):
+        for k in range(halves):
+            part = pl.ds(j * take, take)
+            copy = pltpu.make_async_copy(w_ref.at[k, part], w_room.at[k, part], sems.at[k, j])
+            copy.start()
+            copies.append(copy)
 
     def piece(k, j, first):
         parts = [w_room[k, j * take : (j + 1) * take, :, n, :, :] for n in (first, first + 1)]
@@ -274,7 +271,6 @@
     for j in range(pieces):
         for k in range(halves):
             copies[j * halves + k].wait()
-            copies[count + j * halves + k].start()
             part = dot(rows[:, j * size : (j + 1) * size], piece(k, j, 0), ((1,), (0,)))
             lifted[k] = part if lifted[k] is None else lifted[k] + part
     hidden = []
@@ -284,7 +280,6 @@
     for j in range(pieces):
         total = None
         for k in range(halves):
-            copies[count + j * halves + k].wait()
             part = dot(hidden[k], piece(k, j, slabs // 2), ((1,), (1,)))
             total = part if total is None else total + part
         out_ref[:, :, :, j * size : (j + 1) * size] = total.astype(bf16).reshape(*out_ref.shape[:3], size)
@@ -428,13 +423,14 @@
         norm_kernel,
         [shape((own_count, width), bf16), shape((nrows, *own_tiles), bf16)],
         [VMEM] * 3,
+        compiler_params=ROOM,
     )(near(mixed), skip_stream_entering, feature_blend_scaling.reshape(1, -1))
     rows = exchange(copies, ROWS)
     out = call(
         mlp_kernel,
         shape((nrows, *own_tiles), bf16),
         [VMEM, HBM],
-        [pltpu.VMEM(weights.shape, bf16), pltpu.SemaphoreType.DMA((2, weights.shape[0], 4))],
+        [pltpu.VMEM(weights.shape, bf16), pltpu.SemaphoreType.DMA((weights.shape[0], 4))],
     )(near(rows), weights)
     out = exchange(out, ROWS)
     return call(final_kernel, jax.ShapeDtypeStruct((own_count, width), bf16), [VMEM] * 2)(near(out), near(own))

time: 143 us -> 142 us (level)
  no operation moved by 1% of the time
where the time goes in v10:
time: 142 us; the launch traced here: 140 us
  blocking collectives  111 us (78%)
  between operations  13.5 us (10%)
  Pallas kernels  11.2 us (8%)
  starting transfers between devices  4.01 us (3%)
    all_to_all x7, blocking collectives, exchange(): return lax.all_to_all(value, axes, split_axis=0, concat_axis=0, tiled=True)  111 us
    ppermute x1, starting transfers between devices, layer(): rim = lax.ppermute(rim, SP, [(k, k + 1) for k in range(nsp - 1)])  4.01 us
    pallas_call x1, Pallas kernels, layer(): call(mlp_kernel, shape((nrows, *own_tiles), bf16), [VMEM, HBM], [pltpu.VM...  3.58 us
  transfers between devices with their start and end apart: 2, of which 0 were waited for; matrix products, arithmetic and copies ran while one was open for 0% of the time, Pallas kernels for 3%

profile of v10, /device:TPU:1, one launch (start us, length us, event | category | flops | bytes accessed | tf_op | source)
XLA Modules:
  0.0 139.6 jit_solution(7642077655631640779)
XLA Ops:
  6.5 0.0 copy-start.4
  6.5 0.0 copy-start.1
  6.5 0.0 copy-start
  6.5 0.0 all-gather.2.cloned.1.call-start
  6.5 0.9 shard_map.163
  7.4 4.0 %collective-permute-start = (bf16[8,768]{1,0:T(8,128)(2,1)S(1)}, bf16[8,768]{1,0:T(8,128)(2,1)S(1)}, u32[]{:S(2)}, u32[]{:S(2)}) collective-permute-start(bf16[8,768]{1,0:T(8,128)(2,1)S(1)} %shard_map.163), channel_id=1, source_target_pairs={{0,8},{8,16},{16,24},{24,32},{32,40},{40,48},{48,56},{56,64},{64,7... | collective-permute-start | bytes 36872 | tf_op jit(solution)/shard_map/ppermute | solution.py:333
  11.4 2.6 %shard_map.164 = (f32[128,512]{1,0:T(8,128)S(1)}, f32[128,128]{1,0:T(8,128)S(1)}, f32[128,128]{1,0:T(8,128)S(1)}, f32[8,128]{1,0:T(8,128)S(1)}, f32[128,512]{1,0:T(8,128)S(1)}, /*index=5*/f32[8,128,128]{2,1,0:T(8,128)S(1)}) custom-call(bf16[128,512]{1,0:T(8,128)(2,1)} %x_ref.5, bf16[128,128]{1,0:T(8,128)(2,1)} %b_ref.5, bf16[128,128]{1,0:T(8,128)(2,1)} %c_ref.5, ...), custom_call_target="tpu_custom_call" | custom-call | tf_op jit(solution)/shard_map/pallas_call | solution.py:334
  14.0 0.0 collective-permute-done.rim_ref
  14.0 0.0 copy-start.2
  14.1 0.0 copy-start.3
  14.1 1.4 %shard_map.165 = (f32[128,512]{1,0:T(8,128)S(1)}, bf16[128,128]{1,0:T(8,128)(2,1)S(1)}, bf16[4,272,128]{2,1,0:T(8,128)(2,1)S(1)}) custom-call(bf16[128,512]{1,0:T(8,128)(2,1)} %x_ref.5, bf16[128,128]{1,0:T(8,128)(2,1)} %b_ref.5, bf16[128,128]{1,0:T(8,128)(2,1)} %c_ref.5, bf16[8,768]{1,0:T(8,128)(2,1)S(1)} %collective-permute-done.rim_ref, ...), custom_call_target="tpu_custom_call" | custom-call | tf_op jit(solution)/shard_map/pallas_call | solution.py:372
  15.5 9.4 %all_to_all.35.got_ref.rows_ref = bf16[4,272,128]{2,1,0:T(8,128)(2,1)S(1)} all-to-all(bf16[4,272,128]{2,1,0:T(8,128)(2,1)S(1)} %get-tuple-element.29), channel_id=1, replica_groups=mesh['zh'=4,'zl'=4,'y'=4,'x'=4,'c'=2] {'y'}, dimensions={0} | all-to-all | bytes 557056 | tf_op jit(solution)/shard_map/all_to_all | solution.py:53
  24.9 0.7 shard_map.166
  25.6 0.0 all-gather.2.cloned.1.call-update
  25.6 12.1 %all_to_all.36.got_ref = bf16[4,144,128]{2,1,0:T(8,128)(2,1)S(1)} all-to-all(bf16[4,144,128]{2,1,0:T(8,128)(2,1)S(1)} %get-tuple-element.30), channel_id=1, replica_groups=mesh['zh'=4,'zl'=4,'y'=4,'x'=4,'c'=2] {'zl'}, dimensions={0} | all-to-all | bytes 294912 | tf_op jit(solution)/shard_map/all_to_all | solution.py:53
  37.7 0.1 shard_map.167
  37.8 25.6 %all_to_all.37.got_ref = bf16[4,144,128]{2,1,0:T(8,128)(2,1)S(1)} all-to-all(bf16[4,144,128]{2,1,0:T(8,128)(2,1)S(1)} %get-tuple-element.31), channel_id=1, replica_groups=mesh['zh'=4,'zl'=4,'y'=4,'x'=4,'c'=2] {'zh'}, dimensions={0} | all-to-all | bytes 294912 | tf_op jit(solution)/shard_map/all_to_all | solution.py:53
  63.4 0.1 shard_map.168
  63.5 7.2 %all_to_all.38.inc_ref = bf16[4,128,128]{2,1,0:T(8,128)(2,1)S(1)} all-to-all(bf16[4,128,128]{2,1,0:T(8,128)(2,1)S(1)} %shard_map.168), channel_id=1, replica_groups=mesh['zh'=4,'zl'=4,'y'=4,'x'=4,'c'=2] {'y'}, dimensions={0} | all-to-all | bytes 262144 | tf_op jit(solution)/shard_map/all_to_all | solution.py:53
  70.7 0.0 copy-done.4
  70.7 0.0 copy-done.1
  70.7 0.0 copy-done
  70.7 0.9 shard_map.169
  71.6 20.1 %all_to_all.39.got_ref = bf16[8,2,8,2048]{3,2,1,0:T(8,128)(2,1)S(1)} all-to-all(bf16[8,2,8,2048]{3,2,1,0:T(8,128)(2,1)S(1)} %shard_map.169), channel_id=1, replica_groups=mesh['zh'=4,'zl'=4,'y'=4,'x'=4,'c'=2] {'x','c'}, dimensions={0} | all-to-all | bytes 1048576 | tf_op jit(solution)/shard_map/all_to_all | solution.py:53
  91.7 0.0 copy-done.2
  91.7 0.0 copy-done.3
  91.7 0.2 shard_map.170
  92.0 18.2 %all_to_all.40.rows_ref = bf16[16,2,8,2048]{3,2,1,0:T(8,128)(2,1)S(1)} all-to-all(bf16[16,2,8,2048]{3,2,1,0:T(8,128)(2,1)S(1)} %get-tuple-element.34), channel_id=1, replica_groups=mesh['zh'=4,'zl'=4,'y'=4,'x'=4,'c'=2] {'x','y'}, dimensions={0} | all-to-all | bytes 2097152 | tf_op jit(solution)/shard_map/all_to_all | solution.py:53
  110.2 0.0 all-gather.2.cloned.1.call-done
  110.2 3.6 %shard_map.171 = bf16[16,2,8,2048]{3,2,1,0:T(8,128)(2,1)S(1)} custom-call(bf16[16,2,8,2048]{3,2,1,0:T(8,128)(2,1)S(1)} %all_to_all.40.rows_ref, bf16[2,16,4,4,32,128]{5,4,3,2,1,0:T(8,128)(2,1)} %bitcast.7), custom_call_target="tpu_custom_call" | custom-call | tf_op jit(solution)/shard_map/pallas_call | solution.py:429
  113.8 18.2 %all_to_all.41.got_ref = bf16[16,2,8,2048]{3,2,1,0:T(8,128)(2,1)S(1)} all-to-all(bf16[16,2,8,2048]{3,2,1,0:T(8,128)(2,1)S(1)} %shard_map.171), channel_id=1, replica_groups=mesh['zh'=4,'zl'=4,'y'=4,'x'=4,'c'=2] {'x','y'}, dimensions={0} | all-to-all | bytes 2097152 | tf_op jit(solution)/shard_map/all_to_all | solution.py:53
  132.0 0.8 shard_map.172
Async XLA Ops:
  6.5 64.2 %copy-start.4 = (f32[512]{0:T(512)S(1)}, f32[512]{0:T(512)}, u32[]{:S(2)}) copy-start(f32[512]{0:T(512)} %param.29) | copy-start | bytes 6148
  6.5 64.2 %copy-start.1 = (bf16[128,512]{1,0:T(8,128)(2,1)S(1)}, bf16[128,512]{1,0:T(8,128)(2,1)}, u32[]{:S(2)}) copy-start(bf16[128,512]{1,0:T(8,128)(2,1)} %gate_ref.1) | copy-start | bytes 393220
  6.5 64.2 %copy-start = (bf16[512,2048]{1,0:T(8,128)(2,1)S(1)}, bf16[512,2048]{1,0:T(8,128)(2,1)}, u32[]{:S(2)}) copy-start(bf16[512,2048]{1,0:T(8,128)(2,1)} %w_ref.1) | copy-start | bytes 6291460
  6.5 103.7 %all-gather.2.cloned.1.call-start = ((), (), s32[]{:S(2)}) async-start(), calls=%async_computation.7 | async-start | bytes 4325376 | tf_op jit(solution)/shard_map/all_gather | solution.py:393
  7.4 6.6 %collective-permute-start = (bf16[8,768]{1,0:T(8,128)(2,1)S(1)}, bf16[8,768]{1,0:T(8,128)(2,1)S(1)}, u32[]{:S(2)}, u32[]{:S(2)}) collective-permute-start(bf16[8,768]{1,0:T(8,128)(2,1)S(1)} %shard_map.163), channel_id=1, source_target_pairs={{0,8},{8,16},{16,24},{24,32},{32,40},{40,48},{48,56},{56,64},{64,7... | collective-permute-start | bytes 36872 | tf_op jit(solution)/shard_map/ppermute | solution.py:333
  14.0 77.7 %copy-start.2 = (bf16[16,2048]{1,0:T(8,128)(2,1)S(1)}, bf16[16,2048]{1,0:T(8,128)(2,1)}, u32[]{:S(2)}) copy-start(bf16[16,2048]{1,0:T(8,128)(2,1)} %skip_ref.3) | copy-start | bytes 196612
  14.1 77.7 %copy-start.3 = (f32[2048]{0:T(1024)S(1)}, f32[2048]{0:T(1024)}, u32[]{:S(2)}) copy-start(f32[2048]{0:T(1024)} %param.31) | copy-start | bytes 24580
Sparse Core Ops, SparseCore 0:
  25.7 80.9 all-gather.1
